TPU v7x, 512 devices: a whole 4x4x16 slice. The times are simulated.
512 devices in a mesh: sp: 32 (over z, core), tp: 16 (over y, x).
Axes of the slice: x: 4, y: 4, z: 16, core: 2. Of those that a mesh axis runs over, the one named last changes fastest.
Arguments:
- cotangent: bfloat16 [4096, 2048], P('sp'), may hold values from -6 to 6
- moe_input: bfloat16 [4096, 2048], P('sp'), may hold values from -6 to 6
- expert_ids: int32 [4096, 2], P('sp'), may hold values from 0 to 31, all different within a row; in each aligned block of 128 rows (0 to 127, 128 to 255, ...) at most 12 rows name the same one
- group_weight: float32 [4096], P('sp'), may hold values from 0.3 to 1
- expert_weight: float32 [4096, 2], P('sp'), may hold values from 0.1 to 0.9
- mixer_out: bfloat16 [4096, 2048], P('sp', 'tp'), may hold values from -6 to 6
- queries: bfloat16 [1024, 4096], P('tp', 'sp'), may hold values from -6 to 6
- key_vectors: bfloat16 [1024, 4096], P('tp', 'sp'), may hold values from -6 to 6
- value_vectors: bfloat16 [2048, 4096], P('tp', 'sp'), may hold values from -6 to 6
- decay_rates: float32 [16, 4096], P('tp', 'sp'), may hold values from 0 to 1, as said below
- proj_weight: bfloat16 [2048, 2048], P(None, 'tp'), may hold values from -0.125 to 0.125
- gate_weight: bfloat16 [32, 2048, 2048], P('sp', None, 'tp'), may hold values from -0.125 to 0.125
- up_weight: bfloat16 [32, 2048, 2048], P('sp', None, 'tp'), may hold values from -0.125 to 0.125
- down_weight: bfloat16 [32, 2048, 2048], P('sp', 'tp'), may hold values from -0.125 to 0.125
Outputs:
- grad_gate: bfloat16 [32, 2048, 2048], P('sp', None, 'tp')
- grad_up: bfloat16 [32, 2048, 2048], P('sp', None, 'tp')
- grad_down: bfloat16 [32, 2048, 2048], P('sp', 'tp')
- grad_proj: float32 [2048, 2048], P('sp', 'tp')
- grad_queries: float32 [1024, 4096], P('tp', 'sp')
- grad_keys: float32 [1024, 4096], P('tp', 'sp')
- grad_values: float32 [2048, 4096], P('tp', 'sp')
Inputs may be any that keep to these rules, and one draw needn't show every extreme that they name: `expert_ids`: in the rows of one device no expert is named by more than 12 entries, a bound that some block reaches; the 2 experts of a row differ. `decay_rates`: Positive.
All inputs are finite; a program needn't handle non-finite values.
Results may differ from a plain program's by a relative error of at most 0.0058.
Values may be sent and summed in bfloat16 or wider, within the bound.
No kernel may reach another device: no remote copies, remote signals or barrier semaphores. Data moves between devices by JAX's collectives and lax.ppermute only.
A program may use at most 64 MiB of HBM per device.

v0:
```python
import jax
import jax.numpy as jnp
from jax import lax
from jax.sharding import Mesh
from jax.sharding import PartitionSpec as P

SP = ("sp_0", "sp_1")


def nothing_yet(shard, identity):
    return jax.tree.map(
        lambda a, e: jnp.broadcast_to(jnp.asarray(e, a.dtype), a.shape), shard, identity
    )


def gathered_once(shard, axis):
    leaves = jax.tree.leaves(shard)
    turns = sorted(range(len(leaves)), key=lambda k: -leaves[k].size)
    width = (1, *leaves[turns[0]].shape)[-1]
    lines = [
        jnp.pad(leaves[k].reshape(-1), (0, -leaves[k].size % width)).reshape(-1, width)
        for k in turns
    ]
    both, at, found = (lax.all_gather(jnp.concatenate(lines), axis), 0, {})
    for k, line in zip(turns, lines):
        section = both[:, at : at + len(line)].reshape(len(both), -1)
        found[k] = section[:, : leaves[k].size].reshape(-1, *leaves[k].shape)
        at += len(line)
    numbers = iter(range(len(leaves)))
    return jax.tree.map(lambda _: found[next(numbers)], shard)


def carried_in(shard, axes, combine, identity):
    before = start = nothing_yet(shard, identity)
    total = shard
    for axis in reversed(axes):
        devices, place = (lax.axis_size(axis), lax.axis_index(axis))
        pieces = gathered_once(total, axis)
        inside, total = (start, start)
        for k in range(devices):
            passed = k < place
            total = combine(total, jax.tree.map(lambda part: part[k], pieces))
            inside = jax.tree.map(lambda new, old: jnp.where(passed, new, old), total, inside)
        before = combine(inside, before)
    return before


def carried_in_2(shard, axes, combine, identity):
    before = start = nothing_yet(shard, identity)
    total = shard
    for axis in reversed(axes):
        devices, place = (lax.axis_size(axis), lax.axis_index(axis))
        pieces = jax.tree.map(lambda part: lax.all_gather(part, axis), total)
        inside, total = (start, start)
        for k in reversed(range(devices)):
            passed = k > place
            total = combine(total, jax.tree.map(lambda part: part[k], pieces))
            inside = jax.tree.map(lambda new, old: jnp.where(passed, new, old), total, inside)
        before = combine(inside, before)
    return before


def sent_together(arrays, axis, split_dim, concat_dim, along):
    both = jnp.concatenate(arrays, axis=along)
    whole, at, gathered = (
        lax.all_to_all(both, axis, split_axis=split_dim, concat_axis=concat_dim, tiled=True),
        0,
        [],
    )
    for a in arrays:
        gathered.append(lax.slice_in_dim(whole, at, at + a.shape[along], axis=along))
        at += a.shape[along]
    return tuple(gathered)


def in_one_piece(arrays, axis, dim, along):
    widths = [a.shape[along] for a in arrays]
    both = jnp.concatenate(arrays, axis=along)
    whole = lax.all_gather(both, axis, axis=dim, tiled=True)
    return tuple(jnp.split(whole, [sum(widths[:k]) for k in range(1, len(widths))], axis=along))


def split_up(shard, dim, devices):
    shape = shard.shape
    pieces = shard.reshape(*shape[:dim], devices, shape[dim] // devices, *shape[dim + 1 :])
    return jnp.moveaxis(pieces, dim, 0)


def sent_and_summed(shard, axis, dim):
    devices = lax.axis_size(axis)
    pieces = lax.all_to_all(split_up(shard, dim, devices), axis, 0, 0, tiled=True)
    return jnp.sum(pieces, axis=0)


def from_everyone(shard, axis):
    copies = jnp.broadcast_to(shard, (lax.axis_size(axis), *shard.shape))
    return lax.all_to_all(copies, axis, split_axis=0, concat_axis=0, tiled=True)


def joined_along(pieces, dim):
    shape = list(pieces.shape[1:])
    shape[dim] *= pieces.shape[0]
    return jnp.moveaxis(pieces, 0, dim).reshape(shape)


def collect(shard, axis, dim):
    pieces = from_everyone(shard, axis)
    return joined_along(pieces, dim)


def slot_table(block_ids, experts_all, capacity):
    flat_ids = block_ids.reshape(-1)
    expert_range = jnp.arange(experts_all, dtype=jnp.int32)
    onehot = (flat_ids[:, None] == expert_range[None, :]).astype(jnp.int32)
    before = jnp.cumsum(onehot, axis=0) - onehot
    rank_in = jnp.sum(before * onehot, axis=1)
    slot_ids = flat_ids * capacity + rank_in
    slot_range = jnp.arange(experts_all * capacity, dtype=jnp.int32)
    entry_numbers = jnp.arange(1, flat_ids.shape[0] + 1, dtype=jnp.int32)
    owners = (
        jnp.sum(
            jnp.where(slot_ids[None, :] == slot_range[:, None], entry_numbers[None, :], 0), axis=1
        )
        - 1
    )
    return (slot_ids, owners)


def pack_rows(cotangent, moe_input, group_weight, expert_weight, expert_ids, experts_all, capacity):
    slot_ids, owners = slot_table(expert_ids, experts_all, capacity)
    present = owners >= 0
    entry_ids = jnp.maximum(owners, 0)
    token_ids = entry_ids // expert_ids.shape[1]
    route_weight = (group_weight[:, None] * expert_weight).reshape(-1)
    row_scale = jnp.where(present, route_weight[entry_ids], 0.0)
    cot_rows = (cotangent[token_ids].astype(jnp.float32) * row_scale[:, None]).astype(jnp.bfloat16)
    inp_rows = jnp.where(present[:, None], moe_input[token_ids], jnp.zeros((), moe_input.dtype))
    return (cot_rows, inp_rows, slot_ids)


def expert_backward(cot_blocks, inp_blocks, gate_weight, up_weight, down_weight):
    gate_pre = jnp.einsum(
        "secd,edf->secf", inp_blocks, gate_weight, preferred_element_type=jnp.float32
    )
    up_pre = jnp.einsum("secd,edf->secf", inp_blocks, up_weight, preferred_element_type=jnp.float32)
    sigmoid_gate = jax.nn.sigmoid(gate_pre)
    hidden = (gate_pre * sigmoid_gate * up_pre).astype(jnp.bfloat16)
    grad_down = jnp.einsum(
        "secf,secd->efd", hidden, cot_blocks, preferred_element_type=jnp.float32
    ).astype(jnp.bfloat16)
    hidden_grad = jnp.einsum(
        "secd,efd->secf", cot_blocks, down_weight, preferred_element_type=jnp.float32
    )
    gate_grad = (
        hidden_grad * up_pre * sigmoid_gate * (1.0 + gate_pre * (1.0 - sigmoid_gate))
    ).astype(jnp.bfloat16)
    up_grad = (hidden_grad * gate_pre * sigmoid_gate).astype(jnp.bfloat16)
    grad_gate = jnp.einsum(
        "secd,secf->edf", inp_blocks, gate_grad, preferred_element_type=jnp.float32
    ).astype(jnp.bfloat16)
    grad_up = jnp.einsum(
        "secd,secf->edf", inp_blocks, up_grad, preferred_element_type=jnp.float32
    ).astype(jnp.bfloat16)
    partial_grad = jnp.einsum(
        "secf,edf->secd", gate_grad, gate_weight, preferred_element_type=jnp.float32
    )
    partial_grad = partial_grad + jnp.einsum(
        "secf,edf->secd", up_grad, up_weight, preferred_element_type=jnp.float32
    )
    return (grad_gate, grad_up, grad_down, partial_grad)


def combine_slots(returned, slot_ids, top_count):
    picked = returned[slot_ids].astype(jnp.float32)
    return jnp.sum(picked.reshape(-1, top_count, returned.shape[1]), axis=1)


def carry_combine(earlier, later):
    earlier_state, earlier_decay = earlier
    later_state, later_decay = later
    return (
        earlier_state * later_decay[:, None, None, None] + later_state,
        earlier_decay * later_decay,
    )


def retention_grads(queries, key_vectors, value_vectors, out_grad, decay_rates):
    exact_result = lax.Precision.HIGHEST
    heads_here = decay_rates.shape[0]
    length = decay_rates.shape[1]
    query_full = queries.astype(jnp.float32).reshape(heads_here, -1, length)
    key_full = key_vectors.astype(jnp.float32).reshape(heads_here, -1, length)
    value_full = value_vectors.astype(jnp.float32).reshape(heads_here, -1, length)
    output_gradient = out_grad.reshape(heads_here, -1, length)
    key_size = query_full.shape[1]
    value_size = value_full.shape[1]
    score_scale = key_size ** (-0.5)
    prefix = jnp.cumsum(decay_rates, axis=1)
    ending = prefix[:, -1:]
    mixing = jnp.exp(-jnp.abs(prefix[:, :, None] - prefix[:, None, :]))
    scores = (
        score_scale
        * jnp.einsum("hkt,hks->hts", query_full, key_full, precision=exact_result)
        * mixing
    )
    score_grad = (
        score_scale
        * jnp.einsum("hvt,hvs->hts", output_gradient, value_full, precision=exact_result)
        * mixing
    )
    query_grad = jnp.einsum("hks,hts->hkt", key_full, score_grad, precision=exact_result)
    key_grad = jnp.einsum("hkt,hts->hks", query_full, score_grad, precision=exact_result)
    value_grad = jnp.einsum("hvt,hts->hvs", output_gradient, scores, precision=exact_result)
    toward_end = jnp.exp(prefix - ending)
    from_start = jnp.exp(-prefix)

    def outgoing(weight_tensors):
        key_value = jnp.einsum(
            "nlq,nyq->nly",
            key_full * weight_tensors[:, None, :],
            value_full,
            precision=exact_result,
        )
        query_cot = jnp.einsum(
            "nlq,nyq->nly",
            query_full * weight_tensors[:, None, :],
            output_gradient,
            precision=exact_result,
        )
        return jnp.stack([key_value, query_cot], axis=1)

    decay_whole = jnp.exp(-ending[:, 0])
    identity_pair = (
        jnp.zeros((heads_here, 2, key_size, value_size), jnp.float32),
        jnp.ones((heads_here,), jnp.float32),
    )
    lower_source = carried_in(
        (outgoing(toward_end), decay_whole), SP, carry_combine, identity_pair
    )[0]
    upper_source = carried_in_2(
        (outgoing(from_start), decay_whole), SP, carry_combine, identity_pair
    )[0]
    low_weight = score_scale * from_start[:, None, :]
    high_weight = score_scale * toward_end[:, None, :]
    query_grad = query_grad + low_weight * jnp.einsum(
        "jsd,jms->jmd", output_gradient, lower_source[:, 0], precision=exact_result
    )
    query_grad = query_grad + high_weight * jnp.einsum(
        "jsd,jms->jmd", output_gradient, upper_source[:, 0], precision=exact_result
    )
    key_grad = key_grad + low_weight * jnp.einsum(
        "cdu,cgd->cgu", value_full, lower_source[:, 1], precision=exact_result
    )
    key_grad = key_grad + high_weight * jnp.einsum(
        "cdu,cgd->cgu", value_full, upper_source[:, 1], precision=exact_result
    )
    value_grad = value_grad + low_weight * jnp.einsum(
        "qnu,qnp->qpu", key_full, lower_source[:, 1], precision=exact_result
    )
    value_grad = value_grad + high_weight * jnp.einsum(
        "qnu,qnp->qpu", key_full, upper_source[:, 1], precision=exact_result
    )
    return (
        query_grad.reshape(heads_here * key_size, length),
        key_grad.reshape(heads_here * key_size, length),
        value_grad.reshape(heads_here * value_size, length),
    )


def on_device(
    cotangent,
    moe_input,
    expert_ids,
    group_weight,
    expert_weight,
    mixer_out,
    queries,
    key_vectors,
    value_vectors,
    decay_rates,
    proj_weight,
    gate_weight,
    up_weight,
    down_weight,
):
    sp_count = lax.axis_size(SP)
    tp_count = lax.axis_size("tp")
    local_experts = gate_weight.shape[0]
    experts_all = local_experts * sp_count
    rows_here = cotangent.shape[0]
    top_count = expert_ids.shape[1]
    capacity = 3 * top_count * rows_here // (2 * experts_all)
    model_width = cotangent.shape[1]
    slice_width = model_width // tp_count
    offset = lax.axis_index("tp") * slice_width
    cot_rows, inp_rows, slot_ids = pack_rows(
        cotangent, moe_input, group_weight, expert_weight, expert_ids, experts_all, capacity
    )
    cot_part = lax.dynamic_slice_in_dim(cot_rows, offset, slice_width, 1)
    inp_part = lax.dynamic_slice_in_dim(inp_rows, offset, slice_width, 1)
    sent_cot, sent_inp = sent_together((cot_part, inp_part), SP, 0, 0, 1)
    got_cot, got_inp = in_one_piece((sent_cot, sent_inp), "tp", 1, 0)
    block_shape = (sp_count, local_experts, capacity, model_width)
    grad_gate, grad_up, grad_down, partial_grad = expert_backward(
        got_cot.reshape(block_shape),
        got_inp.reshape(block_shape),
        gate_weight,
        up_weight,
        down_weight,
    )
    partial_grad = partial_grad.reshape(-1, model_width)
    shared = sent_and_summed(partial_grad, "tp", 1).astype(jnp.bfloat16)
    returned = lax.all_to_all(shared, SP, split_axis=0, concat_axis=0, tiled=True)
    moe_grad = combine_slots(returned, slot_ids, top_count)
    cot_slice = lax.dynamic_slice_in_dim(cotangent, offset, slice_width, 1)
    resid_part = (cot_slice.astype(jnp.float32) + moe_grad).astype(jnp.bfloat16)
    resid_grad = collect(resid_part, "tp", 1)
    grad_proj = sent_and_summed(
        lax.dot_general(
            resid_grad, mixer_out, (((0,), (0,)), ((), ())), preferred_element_type=jnp.float32
        ),
        SP,
        0,
    )
    out_grad = lax.dot_general(
        proj_weight, resid_grad, (((0,), (1,)), ((), ())), preferred_element_type=jnp.float32
    )
    grad_queries, grad_keys, grad_values = retention_grads(
        queries, key_vectors, value_vectors, out_grad, decay_rates
    )
    return (grad_gate, grad_up, grad_down, grad_proj, grad_queries, grad_keys, grad_values)


def solution(mesh):
    finer = Mesh(mesh.devices.reshape(16, 2, mesh.shape["tp"]), ("sp_0", "sp_1", "tp"))
    in_specs = (
        P(SP, None),
        P(SP, None),
        P(SP, None),
        P(SP),
        P(SP, None),
        P(SP, "tp"),
        P("tp", SP),
        P("tp", SP),
        P("tp", SP),
        P("tp", SP),
        P(None, "tp"),
        P(SP, None, "tp"),
        P(SP, None, "tp"),
        P(SP, "tp", None),
    )
    out_specs = (
        P(SP, None, "tp"),
        P(SP, None, "tp"),
        P(SP, "tp", None),
        P(SP, "tp"),
        P("tp", SP),
        P("tp", SP),
        P("tp", SP),
    )
    return jax.shard_map(
        on_device, mesh=finer, in_specs=in_specs, out_specs=out_specs, check_vma=False
    )
```

profile of v0, /device:TPU:32, one launch (start us, length us, event | category | flops | bytes accessed | tf_op | source)
XLA Modules:
  0.0 412.9 jit_solution(8375312899908360244)
XLA Ops:
  7.2 0.9 copy.49
  8.4 0.6 reduce-window.6
  9.6 0.7 broadcast_multiply_fusion.2
  10.5 2.8 gather_fusion.1
  13.4 3.1 gather_fusion.2
  16.5 2.4 gather_fusion
  19.0 1.0 dynamic-slice_select_fusion
  20.2 36.1 %all_to_all.36 = bf16[32,12,256]{2,1,0:T(8,128)(2,1)S(1)} all-to-all(bf16[32,12,256]{2,1,0:T(8,128)(2,1)S(1)} %all_to_all.23), channel_id=1, replica_groups=mesh['sp_0'=16,'sp_1'=2,'tp'=16] {'sp_0','sp_1'}, dimensions={0} | all-to-all | bytes 393216 | tf_op jit(solution)/shard_map/all_to_all | solution.py:66
  56.3 0.7 pad_maximum_fusion.1
  57.1 60.2 %all-gather.10.cloned.1.call-done = bf16[768,2048]{1,0:T(8,128)(2,1)} async-done(((bf16[768,128]{1,0:T(8,128)(2,1)}), bf16[768,2048]{1,0:T(8,128)(2,1)}) %all-gather.10.cloned.1.call-update) | async-done | bytes 3145744 | tf_op jit(solution)/shard_map/all_gather | solution.py:79
  117.2 3.3 fusion.63
  120.6 1.6 reshape.1338
  122.2 2.9 convolution_bitcast_fusion.3
  125.1 1.1 convolution_bitcast_fusion.4
  126.3 2.4 reshape.1339
  128.7 2.2 multiply_convert_fusion.1
  131.0 0.6 fusion.16
  132.7 3.8 copy.59
  136.5 4.8 %reshape_reshape.2 = f32[384,16,128]{2,1,0:T(8,128)} reshape(f32[32,1,12,2048]{3,2,0,1:T(8,128)} %copy.59) | data formatting | bytes 6291456 | tf_op jit(solution)/shard_map/reshape;reshape | solution.py:85
  141.3 2.9 copy.60
  144.2 44.3 %all_to_all.37 = f32[16,384,128]{2,1,0:T(8,128)} all-to-all(f32[16,384,128]{2,1,0:T(8,128)S(1)} %copy.60), channel_id=1, replica_groups=mesh['sp_0'=16,'sp_1'=2,'tp'=16] {'tp'}, dimensions={0} | all-to-all | bytes 6291456 | tf_op jit(solution)/shard_map/all_to_all | solution.py:91
  188.5 2.1 reduce_sum.49
  190.6 0.7 convert_element_type.85
  191.3 12.9 %all-to-all-start.2 = ((bf16[32,12,128]{2,1,0:T(8,128)(2,1)}), bf16[32,12,128]{2,1,0:T(8,128)(2,1)S(1)}, u32[]{:S(2)}, u32[]{:S(2)}) async-start(bf16[32,12,128]{2,1,0:T(8,128)(2,1)} %convert_element_type.85), calls=%async_computation.2 | async-start | bytes 262144 | tf_op jit(solution)/shard_map/all_to_all | solution.py:313
  204.5 15.4 %all-to-all-done.2 = bf16[32,12,128]{2,1,0:T(8,128)(2,1)S(1)} async-done(((bf16[32,12,128]{2,1,0:T(8,128)(2,1)}), bf16[32,12,128]{2,1,0:T(8,128)(2,1)S(1)}, u32[]{:S(2)}, u32[]{:S(2)}) %all-to-all-start.2) | async-done | bytes 98336 | tf_op jit(solution)/shard_map/all_to_all | solution.py:313
  220.0 0.9 gather_fusion.3
  221.1 0.9 broadcast_in_dim.39
  222.0 3.6 all-to-all-start.3
  226.0 0.6 slice.313
  227.3 1.3 dynamic-slice
  228.6 0.7 bitcast_dynamic-update-slice_fusion
  229.2 2.5 all-reduce.2
  231.7 0.6 slice_multiply_fusion
  233.0 0.7 negate_exponential_fusion.1
  233.8 2.6 all-to-all-done.3
  236.4 1.4 fusion.69
  238.0 1.9 all-gather.3
  239.9 1.3 fusion.42
  241.3 1.3 dynamic-slice.1
  242.6 1.4 dynamic-update-slice.1
  244.0 28.8 %all-reduce.3 = f32[16]{0:T(128)S(1)} all-reduce(f32[16]{0:T(128)S(1)} %dynamic-update-slice.1), channel_id=4, replica_groups=mesh['sp_0'=16,'sp_1'=2,'tp'=16] {'sp_0'}, use_global_device_ids=true, to_apply=%add.3 | all-reduce | flops 16 | bytes 128
  272.9 0.7 fusion.68
  275.7 0.8 fusion.10
  276.8 2.1 all-gather.4
  281.4 1.3 fusion.59
  282.7 0.6 maximum_bitcast_fusion.1
  283.3 3.6 fusion.5
  287.0 1.2 fusion.52
  288.2 6.1 %all-to-all-start.4 = ((f32[32,64,128]{2,1,0:T(8,128)}), f32[32,64,128]{2,1,0:T(8,128)}, u32[]{:S(2)}, u32[]{:S(2)}) async-start(f32[32,64,128]{2,1,0:T(8,128)} %fusion.52), calls=%async_computation.4 | async-start | bytes 2097152 | tf_op jit(solution)/shard_map/all_to_all | solution.py:91
  294.4 1.9 fusion.3
  296.3 2.0 fusion.4
  299.8 6.5 %all-gather.12.cloned.1.call-done = f32[16,1,2,64,128]{4,3,2,1,0:T(8,128)} async-done(((f32[1,1,2,64,128]{4,3,2,1,0:T(8,128)}), f32[16,1,2,64,128]{4,3,2,1,0:T(8,128)}) %all-gather.12.cloned.1.call-update) | async-done | bytes 1048592 | tf_op jit(solution)/shard_map/all_gather | solution.py:53
  306.3 11.5 %fusion.34 = f32[1,2,64,128]{3,2,1,0:T(8,128)S(1)} fusion(f32[16,1,2,64,128]{4,3,2,1,0:T(8,128)} %all-gather.12.cloned.1.call-done, f32[2,2,64,128]{3,2,1,0:T(8,128)S(1)} %all-gather.3, f32[]{:T(128)} %bitcast.108, f32[]{:T(128)} %bitcast.107, f32[]{:T(128)} %bitcast.106, f32[]{:T(128)} %bitcast.105, f32[]{:T(128)} %bitcast.96, f32[]{:T(128)} %bitcast.104, ...), kind=kLoop, calls=%fused_computation.73 | loop fusion | flops 884736 | bytes 1245278 | tf_op jit(solution)/shard_map/add | solution.py:182
  317.8 65.8 %all-gather.14.cloned.1.call-done = f32[16,129,128]{2,1,0:T(8,128)} async-done(((f32[1,129,128]{2,1,0:T(8,128)}), f32[16,129,128]{2,1,0:T(8,128)}) %all-gather.14.cloned.1.call-update) | async-done | bytes 1056784 | tf_op jit(solution)/shard_map/all_gather | solution.py:24
  383.6 0.8 slice.426
  384.4 0.7 fusion.66
  385.6 6.0 %broadcast_multiply_fusion = (f32[1,128,128]{2,1,0:T(8,128)S(1)}, f32[1,128,128]{2,1,0:T(8,128)S(1)}, f32[1,128,128]{2,1,0:T(8,128)S(1)}, f32[1,128,128]{2,1,0:T(8,128)S(1)}, f32[1,128,128]{2,1,0:T(8,128)S(1)}) fusion(f32[]{:T(128)} %bitcast.70, f32[16,129,128]{2,1,0:T(8,128)} %all-gather.14.cloned.1.call-done, f32[]{:T(128)} %bitcast.69, f32[]{:T(128)} %bitcast.68, ...), kind=kLoop, calls=%fused_computation.139 | loop fusion | flops 262144 | bytes 983076 | tf_op jit(solution)/shard_map/mul | solution.py:182
  391.6 4.1 select_select_fusion
  395.7 1.0 fusion.64
  396.7 4.5 %multiply_add_fusion = f32[1,2,64,128]{3,2,1,0:T(8,128)S(1)} fusion(f32[1,2,64,128]{3,2,1,0:T(8,128)S(1)} %bitcast.339, f32[1,2,64,128]{3,2,1,0:T(8,128)S(1)} %bitcast.331, f32[1,2,64,128]{3,2,1,0:T(8,128)S(1)} %bitcast.337, f32[1,2,64,128]{3,2,1,0:T(8,128)S(1)} %bitcast.335, f32[1,2,64,128]{3,2,1,0:T(8,128)S(1)} %bitcast.334, ...), kind=kLoop, calls=%fused_computation.121 | loop fusion | flops 409600 | bytes 786472 | tf_op jit(solution)/shard_map/add | solution.py:182
  401.4 0.8 fusion.12
  402.5 0.9 fusion.14
  403.6 0.9 fusion.8
  404.5 1.9 reduce_sum.52
  (104 shorter events, 6.4 us)
Async XLA Ops:
  7.2 115.0 %copy-start = (bf16[1,2048,128]{2,1,0:T(8,128)(2,1)S(1)}, bf16[1,2048,128]{2,1,0:T(8,128)(2,1)}, u32[]{:S(2)}) copy-start(bf16[1,2048,128]{2,1,0:T(8,128)(2,1)} %param.25) | copy-start | bytes 1572868
  7.2 6.2 %copy-start.2 = (bf16[128,2048]{1,0:T(8,128)(2,1)S(1)}, bf16[128,2048]{1,0:T(8,128)(2,1)}, u32[]{:S(2)}) copy-start(bf16[128,2048]{1,0:T(8,128)(2,1)} %param.15) | copy-start | bytes 1572868
  7.2 110.0 %all-gather.10.cloned.1.call-start = ((), (), s32[]{:S(2)}) async-start(), calls=%async_computation.5 | async-start | bytes 3342336 | tf_op jit(solution)/shard_map/all_gather | solution.py:79
  13.4 3.2 copy-start.1
  122.2 2.9 copy-start.3
  122.2 2.9 copy-start.6
  125.1 3.6 copy-start.10
  126.2 2.5 copy-start.12
  131.0 0.6 copy-start.17
  131.0 0.7 copy-start.15
  131.0 1.1 copy-start.7
  188.5 15.7 %copy-start.20 = (s32[128,2]{0,1:T(2,128)S(1)}, s32[128,2]{0,1:T(2,128)}, u32[]{:S(2)}) copy-start(s32[128,2]{0,1:T(2,128)} %param.16) | copy-start | bytes 3076
  191.2 34.4 %copy-start.21 = (f32[1,128]{1,0:T(1,128)S(1)}, f32[1,128]{1,0:T(1,128)}, u32[]{:S(2)}) copy-start(f32[1,128]{1,0:T(1,128)} %param.23) | copy-start | bytes 1540
  191.2 42.4 %copy-start.5 = (bf16[128,128]{1,0:T(8,128)(2,1)S(1)}, bf16[128,128]{1,0:T(8,128)(2,1)}, u32[]{:S(2)}) copy-start(bf16[128,128]{1,0:T(8,128)(2,1)} %param.22) | copy-start | bytes 98308
  191.3 42.4 %copy-start.8 = (bf16[64,128]{1,0:T(8,128)(2,1)S(1)}, bf16[64,128]{1,0:T(8,128)(2,1)}, u32[]{:S(2)}) copy-start(bf16[64,128]{1,0:T(8,128)(2,1)} %param.21) | copy-start | bytes 49156
  191.3 28.7 %all-to-all-start.2 = ((bf16[32,12,128]{2,1,0:T(8,128)(2,1)}), bf16[32,12,128]{2,1,0:T(8,128)(2,1)S(1)}, u32[]{:S(2)}, u32[]{:S(2)}) async-start(bf16[32,12,128]{2,1,0:T(8,128)(2,1)} %convert_element_type.85), calls=%async_computation.2 | async-start | bytes 262144 | tf_op jit(solution)/shard_map/all_to_all | solution.py:313
  220.8 17.0 %copy-start.14 = (bf16[64,128]{1,0:T(8,128)(2,1)S(1)}, bf16[64,128]{1,0:T(8,128)(2,1)}, u32[]{:S(2)}) copy-start(bf16[64,128]{1,0:T(8,128)(2,1)} %param.20) | copy-start | bytes 49156
  222.0 14.3 %all-to-all-start.3 = ((bf16[16,128,128]{1,2,0:T(8,128)(2,1)}), bf16[16,128,128]{1,2,0:T(8,128)(2,1)S(1)}, u32[]{:S(2)}, u32[]{:S(2)}) async-start(bf16[16,128,128]{1,2,0:T(8,128)(2,1)} %broadcast_in_dim.39), calls=%async_computation.3 | async-start | bytes 1048576 | tf_op jit(solution)/shard_map/all_to_all | solution.py:97
  225.6 80.7 %all-gather.12.cloned.1.call-start = ((), (), s32[]{:S(2)}) async-start(), calls=%async_computation.6 | async-start | bytes 1114112 | tf_op jit(solution)/shard_map/all_gather | solution.py:53
  241.2 142.3 %all-gather.14.cloned.1.call-start = ((), (), s32[]{:S(2)}) async-start(), calls=%async_computation.7 | async-start | bytes 1183744 | tf_op jit(solution)/shard_map/all_gather | solution.py:24
  283.3 3.6 copy-start.19
  288.2 6.1 %copy-start.11 = (f32[32,1,12,128]{3,0,2,1:T(8,128)S(1)}, f32[32,1,12,128]{3,0,2,1:T(8,128)}, u32[]{:S(2)}) copy-start(f32[32,1,12,128]{3,0,2,1:T(8,128)} %copy-done.10) | copy-start | bytes 589828
  288.2 6.1 %copy-start.13 = (f32[32,1,12,128]{3,0,2,1:T(8,128)S(1)}, f32[32,1,12,128]{3,0,2,1:T(8,128)}, u32[]{:S(2)}) copy-start(f32[32,1,12,128]{3,0,2,1:T(8,128)} %copy-done.12) | copy-start | bytes 589828
  288.2 116.3 %all-to-all-start.4 = ((f32[32,64,128]{2,1,0:T(8,128)}), f32[32,64,128]{2,1,0:T(8,128)}, u32[]{:S(2)}, u32[]{:S(2)}) async-start(f32[32,64,128]{2,1,0:T(8,128)} %fusion.52), calls=%async_computation.4 | async-start | bytes 2097152 | tf_op jit(solution)/shard_map/all_to_all | solution.py:91
  294.3 2.0 copy-start.4
  294.4 1.9 copy-start.16
  296.3 3.2 copy-start.18
  317.8 78.9 %copy-start.9 = (f32[1,128,128]{2,1,0:T(8,128)S(1)}, f32[1,128,128]{2,1,0:T(8,128)}, u32[]{:S(2)}) copy-start(f32[1,128,128]{2,1,0:T(8,128)} %get-tuple-element.29) | copy-start | bytes 196612
Sparse Core Ops, SparseCore 0:
  57.2 60.0 all-gather.9
  241.3 64.9 all-gather.11
  308.4 75.0 all-gather.13
where the time goes:
time: 415 us; the launch traced here: 413 us
  waiting for transfers between devices  150 us (36%)
  blocking collectives  116 us (28%)
  local copies, waits for them, and re-layouts  41.5 us (10%)
  other arithmetic  38.5 us (9%)
  matrix products  23.1 us (6%)
  starting transfers between devices  22.8 us (5%)
  between operations  20.9 us (5%)
    all_gather x1, waiting for transfers between devices, gathered_once(): both, at, found = (lax.all_gather(jnp.concatenate(lines), axis), 0, {})  65.8 us
    all_gather x1, waiting for transfers between devices, in_one_piece(): whole = lax.all_gather(both, axis, axis=dim, tiled=True)  60.2 us
    all_to_all x1, blocking collectives, sent_and_summed(): lax.all_to_all(split_up(shard, dim, devices), axis, 0, 0, tiled=True)  44.3 us
    all_to_all x1, blocking collectives, sent_together(): lax.all_to_all(both, axis, split_axis=split_dim, concat_axis=concat_dim,...  36.1 us
    unnamed x2, blocking collectives  31.3 us
    add x4, other arithmetic, carry_combine(): earlier_state * later_decay[:, None, None, None] + later_state  18.6 us
    all_to_all x1, waiting for transfers between devices, on_device(): lax.all_to_all(shared, SP, split_axis=0, concat_axis=0, tiled=True)  15.4 us
    all_to_all x1, starting transfers between devices, on_device(): lax.all_to_all(shared, SP, split_axis=0, concat_axis=0, tiled=True)  12.9 us
  transfers between devices with their start and end apart: 6, of which 5 were waited for; matrix products, arithmetic and copies ran while one was open for 13% of the time, Pallas kernels for 0%

commit v1 on v0

v1 whole, which is shorter than its diff:
```python
import jax
import jax.numpy as jnp
from jax import lax
from jax.experimental import pallas as pl
from jax.experimental.pallas import tpu as pltpu
from jax.sharding import Mesh
from jax.sharding import PartitionSpec as P

BF = jnp.bfloat16
F32 = jnp.float32
NZ = 16
NT = 16
CAP = 12
TOK = 128
COL = 128
KD = 64
VD = 128
SP = ("z", "c")
HIGHEST = lax.Precision.HIGHEST
SWAP = [(0, 1), (1, 0)]

NN = (((1,), (0,)), ((), ()))
NTR = (((1,), (1,)), ((), ()))
TN = (((0,), (0,)), ((), ()))


def mm(a, b, dims=NN):
    return lax.dot_general(a, b, dims, preferred_element_type=F32)


def exact(a, b, dims=NN):
    return lax.dot_general(a, b, dims, precision=HIGHEST, preferred_element_type=F32)


def vmem():
    return pl.BlockSpec(memory_space=pltpu.VMEM)


def smem():
    return pl.BlockSpec(memory_space=pltpu.SMEM)


def call(kernel, outs, args, name, flops=1 << 27):
    return pl.pallas_call(
        kernel,
        out_shape=outs,
        in_specs=[smem()] + [vmem()] * (len(args) - 1),
        out_specs=jax.tree.map(lambda _: vmem(), outs),
        name=name,
        cost_estimate=pl.CostEstimate(flops=flops, bytes_accessed=1 << 20, transcendentals=0),
    )(*args)


def arr(shape, dtype):
    return jax.ShapeDtypeStruct(shape, dtype)


def placement(ids, wanted, rank):
    first = ids[0:1, :] == wanted
    match = first | (ids[1:2, :] == wanted)
    tok = TOK
    before = lax.broadcasted_iota(jnp.int32, (tok, tok), 0) < lax.broadcasted_iota(
        jnp.int32, (tok, tok), 1
    )
    ranks = mm(jnp.where(match, 1.0, 0.0).astype(BF), jnp.where(before, 1.0, 0.0).astype(BF))
    return match & (ranks == rank.astype(F32)), first


def rows_of(stride, shift, mul, core):
    n = lax.broadcasted_iota(jnp.int32, (NZ * stride, TOK), 0)
    z = lax.shift_right_logical(n * mul, shift)
    q = n - stride * z
    keep = jnp.where(q < CAP, 2 * z + core, -1)
    send = jnp.where((q >= CAP) & (q < 2 * CAP), 2 * z + 1 - core, -1)
    return keep, q, send, q - CAP


def pack_kernel(s_ref, ids_ref, gw_ref, ew_ref, cot_ref, inp_ref, keep_ref, send_ref):
    ids = ids_ref[...]
    weights = gw_ref[...] * ew_ref[...]
    cot, inp = cot_ref[...], inp_ref[...]
    ek, rk, es, rs = rows_of(2 * CAP, 16, 2731, s_ref[1])
    for wanted, rank, out in ((ek, rk, keep_ref), (es, rs, send_ref)):
        hit, first = placement(ids, wanted, rank)
        scale = jnp.sum(
            jnp.where(hit, jnp.where(first, weights[0:1, :], weights[1:2, :]), 0.0),
            axis=1,
            keepdims=True,
        )
        take = jnp.where(hit, 1.0, 0.0).astype(BF)
        out[:, 0 : 2 * CAP, :] = mm(take, inp).reshape(NZ, 2 * CAP, COL).astype(BF)
        out[:, 2 * CAP : 4 * CAP, :] = (
            (mm(take, cot) * scale).reshape(NZ, 2 * CAP, COL).astype(BF)
        )


def early_kernel(
    s_ref, ids_ref, rate_ref, q_ref, k_ref, v_ref,
    keep_ref, send_ref, piece_ref, weight_ref, mixed_ref, scores_ref, kv_ref,
):
    ek, rk, es, rs = rows_of(32, 5, 1, s_ref[1])
    ids = ids_ref[...]
    for wanted, rank, out in ((ek, rk, keep_ref), (es, rs, send_ref)):
        hit, _ = placement(ids, wanted, rank)
        out[...] = jnp.where(hit, 1.0, 0.0).astype(BF)
    rates = rate_ref[...]
    upto = lax.broadcasted_iota(jnp.int32, (TOK, TOK), 1) <= lax.broadcasted_iota(
        jnp.int32, (TOK, TOK), 0
    )
    col = jnp.broadcast_to(
        jnp.sum(jnp.where(upto, rates, 0.0), axis=1, keepdims=True), (TOK, TOK)
    )
    row = col.T
    total = jnp.sum(rates, axis=1, keepdims=True)
    prefix = row[0:1, :]
    start = jnp.exp(-prefix)
    end = jnp.exp(jnp.minimum(prefix - total, 0.0))
    mixed = KD ** (-0.5) * jnp.exp(-jnp.abs(col - row))
    mixed_ref[...] = mixed
    query, key, value = q_ref[...], k_ref[...], v_ref[...]
    scores_ref[...] = mm(query, key, TN) * mixed
    weight_ref[...] = jnp.concatenate(
        [start, end, jnp.broadcast_to(total, (1, TOK)), jnp.zeros((5, TOK), F32)], axis=0
    )
    keys = key.astype(F32)
    values = value.astype(F32)
    kv_ref[0] = exact(keys * end, values, NTR)
    kv_ref[1] = exact(keys * start, values, NTR)
    hi = jnp.broadcast_to(total, (8, TOK)).astype(BF).astype(F32)
    mid = (total - hi).astype(BF).astype(F32)
    low = total - hi - mid
    number = lax.broadcasted_iota(jnp.int32, (8, TOK), 0)
    piece_ref[...] = jnp.where(
        number == 0, hi, jnp.where(number == 1, mid, jnp.where(number == 2, low, 0.0))
    ).astype(BF)


def expert_kernel(s_ref, x_ref, gw_ref, uw_ref, dw_ref, part_ref, hid_ref, both_ref):
    inp = jnp.concatenate([x_ref[t, 0] for t in range(NT)], axis=1)
    cot = jnp.concatenate([x_ref[t, 1] for t in range(NT)], axis=1)
    both_w = jnp.concatenate([gw_ref[...], uw_ref[...]], axis=1)
    pre = mm(inp, both_w)
    gate, up = pre[:, :128], pre[:, 128:]
    hidden_grad = mm(cot, dw_ref[...], NTR)
    sig = jax.nn.sigmoid(gate)
    act = gate * sig
    hid_ref[...] = (act * up).astype(BF)
    gate_grad = (hidden_grad * up * sig * (1.0 + gate * (1.0 - sig))).astype(BF)
    up_grad = (hidden_grad * act).astype(BF)
    both = jnp.concatenate([gate_grad, up_grad], axis=1)
    both_ref[...] = both
    for t in range(0, NT, 2):
        out = mm(both, both_w[t * COL : (t + 2) * COL], NTR).astype(BF)
        part_ref[t] = out[:, :COL]
        part_ref[t + 1] = out[:, COL:]


def weight_kernel(s_ref, x_ref, hid_ref, both_ref, gg_ref, gu_ref, gd_ref):
    both = both_ref[...]
    hidden = hid_ref[...]
    for t in range(0, NT, 2):
        rows = slice(t * COL, (t + 2) * COL)
        inp = jnp.concatenate([x_ref[t, 0], x_ref[t + 1, 0]], axis=1)
        cot = jnp.concatenate([x_ref[t, 1], x_ref[t + 1, 1]], axis=1)
        out = mm(inp, both, TN).astype(BF)
        gg_ref[rows, :] = out[:, :128]
        gu_ref[rows, :] = out[:, 128:]
        gd_ref[:, rows] = mm(hidden, cot, TN).astype(BF)


def sum_kernel(s_ref, part_ref, piece_ref, out_ref):
    total = part_ref[0].astype(F32)
    for t in range(1, NT):
        total = total + part_ref[t].astype(F32)
    out_ref[:, 0 : 2 * CAP, :] = total.reshape(NZ, 2 * CAP, COL).astype(BF)
    out_ref[:, 2 * CAP : 32, :] = jnp.broadcast_to(piece_ref[...][None], (NZ, 8, COL))


def resid_kernel(s_ref, keep_ref, send_ref, own_ref, other_ref, cot_ref, out_ref):
    moe = mm(keep_ref[...], own_ref[...], TN) + mm(send_ref[...], other_ref[...], TN)
    resid = (cot_ref[...].astype(F32) + moe).astype(BF)
    for t in range(NT):
        out_ref[t] = resid


def proj_kernel(
    s_ref, r_ref, p_ref, mixer_ref, q_ref, weight_ref, kv_ref,
    og_ref, keep_ref, send_ref, state_ref,
):
    core = s_ref[1]
    resid = jnp.concatenate([r_ref[t] for t in range(NT)], axis=1)
    out_grad = mm(resid, p_ref[...])
    og_ref[...] = out_grad
    query = q_ref[...].astype(F32)
    early = exact(query * weight_ref[1:2, :], out_grad)
    late = exact(query * weight_ref[0:1, :], out_grad)
    state_ref[0] = early
    state_ref[1] = late
    send_ref[16] = early.astype(BF)
    send_ref[17] = late.astype(BF)
    send_ref[18] = kv_ref[0].astype(BF)
    send_ref[19] = kv_ref[1].astype(BF)
    mixer = mixer_ref[...]
    for t in range(NT):
        share = mm(r_ref[t], mixer, TN)
        low, high = share[:64], share[64:]
        keep_ref[t] = jnp.where(core == 0, low, high)
        send_ref[t] = jnp.where(core == 0, high, low).astype(BF)


def decays(own_ref, other_ref):
    def total(ref):
        rows = ref[:, 2 * CAP : 32, :].astype(F32)
        return rows[:, 0, :] + rows[:, 1, :] + rows[:, 2, :]

    return total(own_ref), total(other_ref)


def row_at(table, place):
    number = lax.broadcasted_iota(jnp.int32, table.shape, 0)
    return jnp.sum(jnp.where(number == place, table, 0.0), axis=0, keepdims=True)


def chip_kernel(s_ref, keep_ref, got_ref, state_ref, kv_ref, own_ref, other_ref, out_ref):
    place, core = s_ref[0], s_ref[1]
    own, other = decays(own_ref, other_ref)
    mine = jnp.exp(-row_at(own, place))
    theirs = jnp.exp(-row_at(other, place))
    is_first = core == 0
    early_own, early_other = jnp.where(is_first, theirs, 1.0), jnp.where(is_first, 1.0, mine)
    late_own, late_other = jnp.where(is_first, 1.0, theirs), jnp.where(is_first, mine, 1.0)

    def halves(mine_ref, at):
        early = mine_ref[0] * early_own + got_ref[at].astype(F32) * early_other
        late = mine_ref[1] * late_own + got_ref[at + 1].astype(F32) * late_other
        return [jnp.where(is_first, a[:32], a[32:]) for a in (early, late)]

    pairs = [jnp.concatenate(p, axis=0).astype(BF) for p in zip(halves(state_ref, 16), halves(kv_ref, 18))]
    for z in range(NZ):
        out_ref[z, 0:64, :] = (keep_ref[z] + got_ref[z].astype(F32)).astype(BF)
        out_ref[z, 64:128, :] = jnp.where(z > place, pairs[0], pairs[1])


def gather_kernel(s_ref, got_ref, own_ref, other_ref, proj_ref, state_ref):
    place = s_ref[0]
    own, other = decays(own_ref, other_ref)
    chip = own + other
    number = lax.broadcasted_iota(jnp.int32, (NZ, COL), 0)
    between = jnp.zeros((NZ, COL), F32)
    for u in range(NZ):
        inside = ((number < u) & (u < place)) | ((number > u) & (u > place))
        between = between + jnp.where(inside, chip[u : u + 1, :], 0.0)
    weight = jnp.exp(-between)
    early_w = jnp.where(number < place, weight, 0.0)
    late_w = jnp.where(number > place, weight, 0.0)
    share = got_ref[0, 0:64, :].astype(F32)
    state = got_ref[0, 64:128, :].astype(F32)
    early, late = state * early_w[0:1, :], state * late_w[0:1, :]
    for z in range(1, NZ):
        share = share + got_ref[z, 0:64, :].astype(F32)
        state = got_ref[z, 64:128, :].astype(F32)
        early = early + state * early_w[z : z + 1, :]
        late = late + state * late_w[z : z + 1, :]
    proj_ref[...] = share
    state_ref[0] = early
    state_ref[1] = late


def final_kernel(
    s_ref, far_ref, got_ref, og_ref, mixed_ref, scores_ref, weight_ref, q_ref, k_ref, v_ref,
    own_ref, other_ref, gq_ref, gk_ref, gv_ref,
):
    place, core = s_ref[0], s_ref[1]
    is_first = core == 0
    _, other = decays(own_ref, other_ref)
    theirs = jnp.exp(-row_at(other, place))
    early_w, late_w = jnp.where(is_first, 1.0, theirs), jnp.where(is_first, theirs, 1.0)
    early_add, late_add = jnp.where(is_first, 0.0, 1.0), jnp.where(is_first, 1.0, 0.0)

    def state(way, at, w, add):
        far = jnp.concatenate([far_ref[0, way, at : at + 32], far_ref[1, way, at : at + 32]], axis=0)
        near = got_ref[(16 if at == 0 else 18) + way].astype(F32)
        return far * w + near * add

    qd_early, kv_early = [state(0, at, early_w, early_add) for at in (0, 32)]
    qd_late, kv_late = [state(1, at, late_w, late_add) for at in (0, 32)]
    scale = KD ** (-0.5)
    low = scale * weight_ref[0:1, :]
    high = scale * weight_ref[1:2, :]
    out_grad = og_ref[...]
    query, key, value = [r[...].astype(F32) for r in (q_ref, k_ref, v_ref)]
    score_grad = exact(out_grad, value) * mixed_ref[...]
    gq_ref[...] = (
        exact(key, score_grad, NTR)
        + low * exact(kv_early, out_grad, NTR)
        + high * exact(kv_late, out_grad, NTR)
    )
    gk_ref[...] = (
        exact(query, score_grad) + low * exact(qd_early, value) + high * exact(qd_late, value)
    )
    gv_ref[...] = (
        exact(out_grad, scores_ref[...], TN)
        + low * exact(qd_early, key, TN)
        + high * exact(qd_late, key, TN)
    )


def to_all(shard, axis):
    copies = jnp.broadcast_to(shard, (lax.axis_size(axis), *shard.shape))
    return exchange(copies, axis)


def exchange(blocks, axis):
    return lax.all_to_all(blocks, axis, split_axis=0, concat_axis=0, tiled=True)


def on_device(
    cotangent, moe_input, expert_ids, group_weight, expert_weight, mixer_out,
    queries, key_vectors, value_vectors, decay_rates, proj_weight,
    gate_weight, up_weight, down_weight,
):
    place, core, part = [lax.axis_index(a).astype(jnp.int32) for a in ("z", "c", "tp")]
    where = jnp.stack([place, core, part])
    ids = expert_ids.T
    cot = lax.dynamic_slice_in_dim(cotangent, part * COL, COL, 1)
    inp = lax.dynamic_slice_in_dim(moe_input, part * COL, COL, 1)

    keep, send = call(
        pack_kernel,
        [arr((NZ, 4 * CAP, COL), BF)] * 2,
        (where, ids, group_weight.reshape(1, TOK), expert_weight.T, cot, inp),
        "pack",
    )
    rows = keep + lax.ppermute(send, "c", SWAP)
    rows = exchange(rows, "z")
    rows = rows.reshape(NZ, 2, 2 * CAP, COL).transpose(1, 0, 2, 3).reshape(2, NZ * 2 * CAP, COL)
    rows = to_all(rows, "tp")

    pick_keep, pick_send, piece, weight, mixed, scores, kv = call(
        early_kernel,
        [
            arr((NZ * 32, TOK), BF), arr((NZ * 32, TOK), BF), arr((8, TOK), BF), arr((8, TOK), F32),
            arr((TOK, TOK), F32), arr((TOK, TOK), F32), arr((2, KD, VD), F32),
        ],
        (where, ids, decay_rates, queries, key_vectors, value_vectors),
        "early",
    )

    shares, hidden, both = call(
        expert_kernel,
        [arr((NT, 384, COL), BF), arr((384, 128), BF), arr((384, 256), BF)],
        (where, rows, gate_weight[0], up_weight[0], down_weight[0]),
        "expert",
    )
    grad_gate, grad_up, grad_down = call(
        weight_kernel,
        [arr((2048, 128), BF), arr((2048, 128), BF), arr((128, 2048), BF)],
        (where, rows, hidden, both),
        "weights",
        1 << 29,
    )
    shares = exchange(shares, "tp")
    back = call(sum_kernel, arr((NZ, 32, COL), BF), (where, shares, piece), "sums")
    own = exchange(back, "z")
    other = lax.ppermute(own, "c", SWAP)
    resid = call(
        resid_kernel,
        arr((NT, TOK, COL), BF),
        (
            where, pick_keep, pick_send,
            own.reshape(NZ * 32, COL), other.reshape(NZ * 32, COL), cot,
        ),
        "resid",
    )
    resid = exchange(resid, "tp")
    out_grad, proj_keep, proj_send, state = call(
        proj_kernel,
        [
            arr((TOK, VD), F32), arr((NZ, 64, COL), F32), arr((20, 64, COL), BF),
            arr((2, KD, VD), F32),
        ],
        (where, resid, proj_weight, mixer_out, queries, weight, kv),
        "proj",
    )
    got = lax.ppermute(proj_send, "c", SWAP)
    chip = call(
        chip_kernel,
        arr((NZ, 128, COL), BF),
        (where, proj_keep, got, state, kv, own, other),
        "chip",
    )
    chip = exchange(chip, "z")
    grad_proj, far = call(
        gather_kernel,
        [arr((64, COL), F32), arr((2, 64, COL), F32)],
        (where, chip, own, other),
        "gather",
    )
    far = lax.all_gather(far, "c")
    grad_queries, grad_keys, grad_values = call(
        final_kernel,
        [arr((KD, TOK), F32), arr((KD, TOK), F32), arr((VD, TOK), F32)],
        (
            where, far, got, out_grad, mixed, scores, weight,
            queries, key_vectors, value_vectors, own, other,
        ),
        "final",
    )
    return (
        grad_gate[None], grad_up[None], grad_down[None],
        grad_proj, grad_queries, grad_keys, grad_values,
    )


def solution(mesh):
    finer = Mesh(mesh.devices.reshape(NZ, 2, NT), ("z", "c", "tp"))
    in_specs = (
        P(SP, None), P(SP, None), P(SP, None), P(SP), P(SP, None), P(SP, "tp"),
        P("tp", SP), P("tp", SP), P("tp", SP), P("tp", SP), P(None, "tp"),
        P(SP, None, "tp"), P(SP, None, "tp"), P(SP, "tp", None),
    )
    out_specs = (
        P(SP, None, "tp"), P(SP, None, "tp"), P(SP, "tp", None), P(SP, "tp"),
        P("tp", SP), P("tp", SP), P("tp", SP),
    )
    return jax.shard_map(
        on_device, mesh=finer, in_specs=in_specs, out_specs=out_specs, check_vma=False
    )
```

time: 415 us -> 217 us (0.52)
  the two profiles are of different devices: /device:TPU:32 before, /device:TPU:1 now
where the time goes in v1:
time: 217 us; the launch traced here: 216 us
  blocking collectives  115 us (53%)
  waiting for transfers between devices  38.8 us (18%)
  Pallas kernels  27.3 us (13%)
  starting transfers between devices  27 us (12%)
  local copies, waits for them, and re-layouts  5.46 us (3%)
    all_to_all x4, blocking collectives, exchange(): return lax.all_to_all(blocks, axis, split_axis=0, concat_axis=0, tiled=True)  105 us
    all_to_all x2, waiting for transfers between devices, exchange(): return lax.all_to_all(blocks, axis, split_axis=0, concat_axis=0, tiled=True)  35.1 us
    pallas_call x10, Pallas kernels, call(): pl.pallas_call(kernel, out_shape=outs, in_specs=[smem()] + [vmem()] * (le...  27.3 us
    all_gather x1, blocking collectives, on_device(): far = lax.all_gather(far, 'c')  10.3 us
    ppermute x1, starting transfers between devices, on_device(): rows = keep + lax.ppermute(send, 'c', SWAP)  8.73 us
    all_to_all x2, starting transfers between devices, exchange(): return lax.all_to_all(blocks, axis, split_axis=0, concat_axis=0, tiled=True)  7.47 us
    ppermute x1, starting transfers between devices, on_device(): other = lax.ppermute(own, 'c', SWAP)  7.19 us
  transfers between devices with their start and end apart: 5, of which 5 were waited for; matrix products, arithmetic and copies ran while one was open for 0% of the time, Pallas kernels for 3%

profile of v1, /device:TPU:1, one launch (start us, length us, event | category | flops | bytes accessed | tf_op | source)
XLA Modules:
  0.0 216.2 jit_solution(1173198968550632564)
XLA Ops:
  0.6 0.6 pad_add_fusion.s_ref
  1.2 1.4 constant_dynamic-slice_fusion
  2.7 2.1 pack.1
  4.7 8.7 %collective-permute-start = (bf16[16,48,128]{2,1,0:T(8,128)(2,1)}, bf16[16,48,128]{2,1,0:T(8,128)(2,1)S(1)}, u32[]{:S(2)}, u32[]{:S(2)}) collective-permute-start(bf16[16,48,128]{2,1,0:T(8,128)(2,1)} %get-tuple-element.32), channel_id=1, source_target_pairs={{0,16},{16,0},{1,17},{17,1},{2,18},{18,2},{3,19},{19,3},{4,20},{20... | collective-permute-start | bytes 589832 | tf_op jit(solution)/shard_map/ppermute | solution.py:334
  13.4 1.3 collective-permute-done
  14.7 1.0 add.8
  15.7 22.2 %all_to_all.30 = bf16[16,48,128]{2,1,0:T(8,128)(2,1)S(1)} all-to-all(bf16[16,48,128]{2,1,0:T(8,128)(2,1)S(1)} %add.8), channel_id=1, replica_groups=mesh['z'=16,'c'=2,'tp'=16] {'z'}, dimensions={0} | all-to-all | bytes 393216 | tf_op jit(solution)/shard_map/all_to_all | solution.py:314
  37.9 0.7 broadcast_in_dim.12
  38.6 42.5 %all_to_all.31.x_ref = bf16[16,2,384,128]{3,2,1,0:T(8,128)(2,1)} all-to-all(bf16[16,2,384,128]{3,2,1,0:T(8,128)(2,1)S(1)} %broadcast_in_dim.12), channel_id=1, replica_groups=mesh['z'=16,'c'=2,'tp'=16] {'tp'}, dimensions={0} | all-to-all | bytes 6291456 | tf_op jit(solution)/shard_map/all_to_all | solution.py:314
  81.1 4.9 %expert.1 = (bf16[16,384,128]{2,1,0:T(8,128)(2,1)}, bf16[384,128]{1,0:T(8,128)(2,1)}, bf16[384,256]{1,0:T(8,128)(2,1)}) custom-call(s32[3]{0:T(128)} %pad_add_fusion.s_ref, bf16[16,2,384,128]{3,2,1,0:T(8,128)(2,1)} %all_to_all.31.x_ref, bf16[2048,128]{1,0:T(8,128)(2,1)} %bitcast.23, bf16[2048,128]{1,0:T(8,128)(2,1)} %bitcast.24, bf16[128,2048]{1,0:T(8,128)(2,1)} %bitcast.25), custom_call_target="tpu_custom_call" | custom-call | flops 134217728 | bytes 1048576 | tf_op jit(solution)/shard_map/expert/pallas_call | solution.py:44
  86.0 3.7 %all-to-all-start.2 = ((bf16[16,384,128]{2,1,0:T(8,128)(2,1)}), bf16[16,384,128]{2,1,0:T(8,128)(2,1)S(1)}, u32[]{:S(2)}, u32[]{:S(2)}) async-start(bf16[16,384,128]{2,1,0:T(8,128)(2,1)} %get-tuple-element.40), calls=%async_computation.2 | async-start | bytes 3145728 | tf_op jit(solution)/shard_map/all_to_all | solution.py:314
  89.7 2.0 early.1
  91.8 16.5 %all-to-all-done.2.part_ref = bf16[16,384,128]{2,1,0:T(8,128)(2,1)S(1)} async-done(((bf16[16,384,128]{2,1,0:T(8,128)(2,1)}), bf16[16,384,128]{2,1,0:T(8,128)(2,1)S(1)}, u32[]{:S(2)}, u32[]{:S(2)}) %all-to-all-start.2) | async-done | bytes 1572896 | tf_op jit(solution)/shard_map/all_to_all | solution.py:314
  108.3 0.0 copy-start
  108.3 1.2 copy-done
  109.4 2.3 %sums.1 = bf16[16,32,128]{2,1,0:T(8,128)(2,1)} custom-call(s32[3]{0:T(128)} %pad_add_fusion.s_ref, bf16[16,384,128]{2,1,0:T(8,128)(2,1)} %copy-done, bf16[8,128]{1,0:T(8,128)(2,1)} %get-tuple-element.41.piece_ref), custom_call_target="tpu_custom_call" | custom-call | flops 134217728 | bytes 1048576 | tf_op jit(solution)/shard_map/sums/pallas_call | solution.py:44
  111.7 25.4 %all_to_all.32.own_ref = bf16[16,32,128]{2,1,0:T(8,128)(2,1)S(1)} all-to-all(bf16[16,32,128]{2,1,0:T(8,128)(2,1)} %sums.1), channel_id=1, replica_groups=mesh['z'=16,'c'=2,'tp'=16] {'z'}, dimensions={0} | all-to-all | bytes 262144 | tf_op jit(solution)/shard_map/all_to_all | solution.py:314
  137.1 0.0 copy-start.1
  137.1 7.2 %collective-permute-start.1 = (bf16[16,32,128]{2,1,0:T(8,128)(2,1)S(1)}, bf16[16,32,128]{2,1,0:T(8,128)(2,1)S(1)}, u32[]{:S(2)}, u32[]{:S(2)}) collective-permute-start(bf16[16,32,128]{2,1,0:T(8,128)(2,1)S(1)} %all_to_all.32.own_ref), channel_id=1, source_target_pairs={{0,16},{16,0},{1,17},{17,1},{2,18},{18,2},{3,19},{19,3},{4,20},{20... | collective-permute-start | bytes 393224 | tf_op jit(solution)/shard_map/ppermute | solution.py:365
  144.3 1.0 collective-permute-done.1.other_ref
  145.2 0.0 copy-start.3
  145.2 0.0 copy-done.1
  145.2 0.6 copy-done.3
  145.9 2.2 %resid.1 = bf16[16,128,128]{2,1,0:T(8,128)(2,1)} custom-call(s32[3]{0:T(128)} %pad_add_fusion.s_ref, bf16[512,128]{1,0:T(8,128)(2,1)} %get-tuple-element.38.keep_ref, bf16[512,128]{1,0:T(8,128)(2,1)} %get-tuple-element.39.send_ref, bf16[512,128]{1,0:T(8,128)(2,1)} %bitcast.19, bf16[512,128]{1,0:T(8,128)(2,1)} %bitcast.20, ...), custom_call_target="tpu_custom_call" | custom-call | flops 134217728 | bytes 1048576 | tf_op jit(solution)/shard_map/resid/pallas_call | solution.py:44
  148.1 15.0 %all_to_all.33.r_ref = bf16[16,128,128]{2,1,0:T(8,128)(2,1)} all-to-all(bf16[16,128,128]{2,1,0:T(8,128)(2,1)} %resid.1), channel_id=1, replica_groups=mesh['z'=16,'c'=2,'tp'=16] {'tp'}, dimensions={0} | all-to-all | bytes 1048576 | tf_op jit(solution)/shard_map/all_to_all | solution.py:314
  163.1 2.8 %proj.1 = (f32[128,128]{1,0:T(8,128)}, f32[16,64,128]{2,1,0:T(8,128)}, bf16[20,64,128]{2,1,0:T(8,128)(2,1)}, f32[2,64,128]{2,1,0:T(8,128)}) custom-call(s32[3]{0:T(128)} %pad_add_fusion.s_ref, bf16[16,128,128]{2,1,0:T(8,128)(2,1)} %all_to_all.33.r_ref, bf16[2048,128]{1,0:T(8,128)(2,1)} %p_ref.1, bf16[128,128]{1,0:T(8,128)(2,1)} %mixer_ref.1, ...), custom_call_target="tpu_custom_call" | custom-call | flops 134217728 | bytes 1048576 | tf_op jit(solution)/shard_map/proj/pallas_call | solution.py:44
  165.9 3.6 %collective-permute-start.2 = (bf16[20,64,128]{2,1,0:T(8,128)(2,1)}, bf16[20,64,128]{2,1,0:T(8,128)(2,1)S(1)}, u32[]{:S(2)}, u32[]{:S(2)}) collective-permute-start(bf16[20,64,128]{2,1,0:T(8,128)(2,1)} %get-tuple-element.45), channel_id=1, source_target_pairs={{0,16},{16,0},{1,17},{17,1},{2,18},{18,2},{3,19},{19,3},{4,20},{20... | collective-permute-start | bytes 983048 | tf_op jit(solution)/shard_map/ppermute | solution.py:385
  169.5 1.4 collective-permute-done.2.got_ref
  170.9 0.0 copy-start.4
  170.9 0.7 copy-done.4
  171.7 2.2 %chip.1 = bf16[16,128,128]{2,1,0:T(8,128)(2,1)} custom-call(s32[3]{0:T(128)} %pad_add_fusion.s_ref, f32[16,64,128]{2,1,0:T(8,128)} %get-tuple-element.44.keep_ref, bf16[20,64,128]{2,1,0:T(8,128)(2,1)} %copy-done.4, f32[2,64,128]{2,1,0:T(8,128)} %get-tuple-element.46.state_ref, f32[2,64,128]{2,1,0:T(8,128)} %get-tuple-element.43.kv_ref, ...), custom_call_target="tpu_custom_call" | custom-call | flops 134217728 | bytes 1048576 | tf_op jit(solution)/shard_map/chip/pallas_call | solution.py:44
  173.8 3.8 %all-to-all-start.5 = ((bf16[16,128,128]{2,1,0:T(8,128)(2,1)}), bf16[16,128,128]{2,1,0:T(8,128)(2,1)S(1)}, u32[]{:S(2)}, u32[]{:S(2)}) async-start(bf16[16,128,128]{2,1,0:T(8,128)(2,1)} %chip.1), calls=%async_computation.5 | async-start | bytes 1048576 | tf_op jit(solution)/shard_map/all_to_all | solution.py:314
  177.6 4.1 %weights.1 = (bf16[2048,128]{1,0:T(8,128)(2,1)}, bf16[2048,128]{1,0:T(8,128)(2,1)}, bf16[128,2048]{1,0:T(8,128)(2,1)}) custom-call(s32[3]{0:T(128)} %pad_add_fusion.s_ref, bf16[16,2,384,128]{3,2,1,0:T(8,128)(2,1)} %all_to_all.31.x_ref, bf16[384,128]{1,0:T(8,128)(2,1)} %get-tuple-element.33.hid_ref, bf16[384,256]{1,0:T(8,128)(2,1)} %get-tuple-element.34.both_ref), custom_call_target="tpu_custom_call" | custom-call | flops 536870912 | bytes 1048576 | tf_op jit(solution)/shard_map/weights/pallas_call | solution.py:44
  181.7 18.6 %all-to-all-done.5.got_ref = bf16[16,128,128]{2,1,0:T(8,128)(2,1)S(1)} async-done(((bf16[16,128,128]{2,1,0:T(8,128)(2,1)}), bf16[16,128,128]{2,1,0:T(8,128)(2,1)S(1)}, u32[]{:S(2)}, u32[]{:S(2)}) %all-to-all-start.5) | async-done | bytes 524320 | tf_op jit(solution)/shard_map/all_to_all | solution.py:314
  200.4 0.0 copy-start.2
  200.4 0.8 copy-done.2
  201.2 2.0 gather.1
  203.1 10.3 %all-gather = f32[4,64,128]{2,1,0:T(8,128)} all-gather(f32[2,64,128]{2,1,0:T(8,128)} %get-tuple-element.48), channel_id=2, replica_groups=mesh['z'=16,'c'=2,'tp'=16] {'c'}, dimensions={0}, use_global_device_ids=true | all-gather | bytes 196608 | tf_op jit(solution)/shard_map/all_gather | solution.py:399
  213.4 2.8 %final.1 = (f32[64,128]{1,0:T(8,128)}, f32[64,128]{1,0:T(8,128)}, f32[128,128]{1,0:T(8,128)}) custom-call(s32[3]{0:T(128)} %pad_add_fusion.s_ref, f32[2,2,64,128]{3,2,1,0:T(8,128)} %bitcast.26, bf16[20,64,128]{2,1,0:T(8,128)(2,1)} %copy-done.4, f32[128,128]{1,0:T(8,128)} %get-tuple-element.49.og_ref, f32[128,128]{1,0:T(8,128)} %get-tuple-element.50.mixed_ref, ...), custom_call_target="tpu_custom_call" | custom-call | flops 134217728 | bytes 1048576 | tf_op jit(solution)/shard_map/final/pallas_call | solution.py:44
  (1 shorter events, 0.0 us)
Async XLA Ops:
  4.7 10.0 %collective-permute-start = (bf16[16,48,128]{2,1,0:T(8,128)(2,1)}, bf16[16,48,128]{2,1,0:T(8,128)(2,1)S(1)}, u32[]{:S(2)}, u32[]{:S(2)}) collective-permute-start(bf16[16,48,128]{2,1,0:T(8,128)(2,1)} %get-tuple-element.32), channel_id=1, source_target_pairs={{0,16},{16,0},{1,17},{17,1},{2,18},{18,2},{3,19},{19,3},{4,20},{20... | collective-permute-start | bytes 589832 | tf_op jit(solution)/shard_map/ppermute | solution.py:334
  86.0 22.3 %all-to-all-start.2 = ((bf16[16,384,128]{2,1,0:T(8,128)(2,1)}), bf16[16,384,128]{2,1,0:T(8,128)(2,1)S(1)}, u32[]{:S(2)}, u32[]{:S(2)}) async-start(bf16[16,384,128]{2,1,0:T(8,128)(2,1)} %get-tuple-element.40), calls=%async_computation.2 | async-start | bytes 3145728 | tf_op jit(solution)/shard_map/all_to_all | solution.py:314
  108.3 1.2 copy-start
  137.1 8.2 %copy-start.1 = (bf16[16,32,128]{2,1,0:T(8,128)(2,1)}, bf16[16,32,128]{2,1,0:T(8,128)(2,1)S(1)}, u32[]{:S(2)}) copy-start(bf16[16,32,128]{2,1,0:T(8,128)(2,1)S(1)} %all_to_all.32.own_ref) | copy-start | bytes 393220
  137.1 8.2 %collective-permute-start.1 = (bf16[16,32,128]{2,1,0:T(8,128)(2,1)S(1)}, bf16[16,32,128]{2,1,0:T(8,128)(2,1)S(1)}, u32[]{:S(2)}, u32[]{:S(2)}) collective-permute-start(bf16[16,32,128]{2,1,0:T(8,128)(2,1)S(1)} %all_to_all.32.own_ref), channel_id=1, source_target_pairs={{0,16},{16,0},{1,17},{17,1},{2,18},{18,2},{3,19},{19,3},{4,20},{20... | collective-permute-start | bytes 393224 | tf_op jit(solution)/shard_map/ppermute | solution.py:365
  145.2 0.6 copy-start.3
  165.9 5.1 %collective-permute-start.2 = (bf16[20,64,128]{2,1,0:T(8,128)(2,1)}, bf16[20,64,128]{2,1,0:T(8,128)(2,1)S(1)}, u32[]{:S(2)}, u32[]{:S(2)}) collective-permute-start(bf16[20,64,128]{2,1,0:T(8,128)(2,1)} %get-tuple-element.45), channel_id=1, source_target_pairs={{0,16},{16,0},{1,17},{17,1},{2,18},{18,2},{3,19},{19,3},{4,20},{20... | collective-permute-start | bytes 983048 | tf_op jit(solution)/shard_map/ppermute | solution.py:385
  170.9 0.7 copy-start.4
  173.8 26.5 %all-to-all-start.5 = ((bf16[16,128,128]{2,1,0:T(8,128)(2,1)}), bf16[16,128,128]{2,1,0:T(8,128)(2,1)S(1)}, u32[]{:S(2)}, u32[]{:S(2)}) async-start(bf16[16,128,128]{2,1,0:T(8,128)(2,1)} %chip.1), calls=%async_computation.5 | async-start | bytes 1048576 | tf_op jit(solution)/shard_map/all_to_all | solution.py:314
  200.4 0.8 copy-start.2

commit v2 on v1

--- a/solution.py
+++ b/solution.py
@@ -36,19 +36,20 @@
     return pl.BlockSpec(memory_space=pltpu.VMEM)
 
 
-def smem():
-    return pl.BlockSpec(memory_space=pltpu.SMEM)
-
-
-def call(kernel, outs, args, name, flops=1 << 27):
+def call(kernel, outs, args, name, mib=4, flops=1 << 27):
     return pl.pallas_call(
         kernel,
         out_shape=outs,
-        in_specs=[smem()] + [vmem()] * (len(args) - 1),
+        in_specs=[vmem()] * len(args),
         out_specs=jax.tree.map(lambda _: vmem(), outs),
         name=name,
+        compiler_params=pltpu.CompilerParams(vmem_limit_bytes=mib << 20),
         cost_estimate=pl.CostEstimate(flops=flops, bytes_accessed=1 << 20, transcendentals=0),
     )(*args)
+
+
+def spot(axis):
+    return lax.axis_index(axis).astype(jnp.int32)
 
 
 def arr(shape, dtype):
@@ -75,11 +76,13 @@
     return keep, q, send, q - CAP
 
 
-def pack_kernel(s_ref, ids_ref, gw_ref, ew_ref, cot_ref, inp_ref, keep_ref, send_ref):
+def pack_kernel(ids_ref, gw_ref, ew_ref, cot_ref, inp_ref, keep_ref, send_ref, cols_ref):
     ids = ids_ref[...]
     weights = gw_ref[...] * ew_ref[...]
-    cot, inp = cot_ref[...], inp_ref[...]
-    ek, rk, es, rs = rows_of(2 * CAP, 16, 2731, s_ref[1])
+    here = pl.ds(pl.multiple_of(spot("tp") * COL, COL), COL)
+    cot, inp = cot_ref[:, here], inp_ref[:, here]
+    cols_ref[...] = cot
+    ek, rk, es, rs = rows_of(2 * CAP, 16, 2731, spot("c"))
     for wanted, rank, out in ((ek, rk, keep_ref), (es, rs, send_ref)):
         hit, first = placement(ids, wanted, rank)
         scale = jnp.sum(
@@ -95,10 +98,10 @@
 
 
 def early_kernel(
-    s_ref, ids_ref, rate_ref, q_ref, k_ref, v_ref,
+    ids_ref, rate_ref, q_ref, k_ref, v_ref,
     keep_ref, send_ref, piece_ref, weight_ref, mixed_ref, scores_ref, kv_ref,
 ):
-    ek, rk, es, rs = rows_of(32, 5, 1, s_ref[1])
+    ek, rk, es, rs = rows_of(32, 5, 1, spot("c"))
     ids = ids_ref[...]
     for wanted, rank, out in ((ek, rk, keep_ref), (es, rs, send_ref)):
         hit, _ = placement(ids, wanted, rank)
@@ -135,9 +138,9 @@
     ).astype(BF)
 
 
-def expert_kernel(s_ref, x_ref, gw_ref, uw_ref, dw_ref, part_ref, hid_ref, both_ref):
-    inp = jnp.concatenate([x_ref[t, 0] for t in range(NT)], axis=1)
-    cot = jnp.concatenate([x_ref[t, 1] for t in range(NT)], axis=1)
+def expert_kernel(x_ref, gw_ref, uw_ref, dw_ref, part_ref, hid_ref, both_ref):
+    inp = jnp.concatenate([x_ref[held_at(t), 0] for t in range(NT)], axis=1)
+    cot = jnp.concatenate([x_ref[held_at(t), 1] for t in range(NT)], axis=1)
     both_w = jnp.concatenate([gw_ref[...], uw_ref[...]], axis=1)
     pre = mm(inp, both_w)
     gate, up = pre[:, :128], pre[:, 128:]
@@ -155,20 +158,20 @@
         part_ref[t + 1] = out[:, COL:]
 
 
-def weight_kernel(s_ref, x_ref, hid_ref, both_ref, gg_ref, gu_ref, gd_ref):
+def weight_kernel(x_ref, hid_ref, both_ref, gg_ref, gu_ref, gd_ref):
     both = both_ref[...]
     hidden = hid_ref[...]
     for t in range(0, NT, 2):
         rows = slice(t * COL, (t + 2) * COL)
-        inp = jnp.concatenate([x_ref[t, 0], x_ref[t + 1, 0]], axis=1)
-        cot = jnp.concatenate([x_ref[t, 1], x_ref[t + 1, 1]], axis=1)
+        inp = jnp.concatenate([x_ref[held_at(t), 0], x_ref[held_at(t + 1), 0]], axis=1)
+        cot = jnp.concatenate([x_ref[held_at(t), 1], x_ref[held_at(t + 1), 1]], axis=1)
         out = mm(inp, both, TN).astype(BF)
         gg_ref[rows, :] = out[:, :128]
         gu_ref[rows, :] = out[:, 128:]
         gd_ref[:, rows] = mm(hidden, cot, TN).astype(BF)
 
 
-def sum_kernel(s_ref, part_ref, piece_ref, out_ref):
+def sum_kernel(part_ref, piece_ref, out_ref):
     total = part_ref[0].astype(F32)
     for t in range(1, NT):
         total = total + part_ref[t].astype(F32)
@@ -176,7 +179,7 @@
     out_ref[:, 2 * CAP : 32, :] = jnp.broadcast_to(piece_ref[...][None], (NZ, 8, COL))
 
 
-def resid_kernel(s_ref, keep_ref, send_ref, own_ref, other_ref, cot_ref, out_ref):
+def resid_kernel(keep_ref, send_ref, own_ref, other_ref, cot_ref, out_ref):
     moe = mm(keep_ref[...], own_ref[...], TN) + mm(send_ref[...], other_ref[...], TN)
     resid = (cot_ref[...].astype(F32) + moe).astype(BF)
     for t in range(NT):
@@ -184,10 +187,10 @@
 
 
 def proj_kernel(
-    s_ref, r_ref, p_ref, mixer_ref, q_ref, weight_ref, kv_ref,
+    r_ref, p_ref, mixer_ref, q_ref, weight_ref, kv_ref,
     og_ref, keep_ref, send_ref, state_ref,
 ):
-    core = s_ref[1]
+    core = spot("c")
     resid = jnp.concatenate([r_ref[t] for t in range(NT)], axis=1)
     out_grad = mm(resid, p_ref[...])
     og_ref[...] = out_grad
@@ -221,8 +224,8 @@
     return jnp.sum(jnp.where(number == place, table, 0.0), axis=0, keepdims=True)
 
 
-def chip_kernel(s_ref, keep_ref, got_ref, state_ref, kv_ref, own_ref, other_ref, out_ref):
-    place, core = s_ref[0], s_ref[1]
+def chip_kernel(keep_ref, got_ref, state_ref, kv_ref, own_ref, other_ref, out_ref):
+    place, core = spot("z"), spot("c")
     own, other = decays(own_ref, other_ref)
     mine = jnp.exp(-row_at(own, place))
     theirs = jnp.exp(-row_at(other, place))
@@ -241,8 +244,8 @@
         out_ref[z, 64:128, :] = jnp.where(z > place, pairs[0], pairs[1])
 
 
-def gather_kernel(s_ref, got_ref, own_ref, other_ref, proj_ref, state_ref):
-    place = s_ref[0]
+def gather_kernel(got_ref, own_ref, other_ref, proj_ref, state_ref):
+    place = spot("z")
     own, other = decays(own_ref, other_ref)
     chip = own + other
     number = lax.broadcasted_iota(jnp.int32, (NZ, COL), 0)
@@ -267,10 +270,10 @@
 
 
 def final_kernel(
-    s_ref, far_ref, got_ref, og_ref, mixed_ref, scores_ref, weight_ref, q_ref, k_ref, v_ref,
+    far_ref, got_ref, og_ref, mixed_ref, scores_ref, weight_ref, q_ref, k_ref, v_ref,
     own_ref, other_ref, gq_ref, gk_ref, gv_ref,
 ):
-    place, core = s_ref[0], s_ref[1]
+    place, core = spot("z"), spot("c")
     is_first = core == 0
     _, other = decays(own_ref, other_ref)
     theirs = jnp.exp(-row_at(other, place))
@@ -305,13 +308,25 @@
     )
 
 
-def to_all(shard, axis):
-    copies = jnp.broadcast_to(shard, (lax.axis_size(axis), *shard.shape))
-    return exchange(copies, axis)
+def groups(step, stride, step_other, stride_other):
+    first = [[stride * g + step * k for k in range(4)] for g in range(4)]
+    second = [[16 + stride_other * g + step_other * k for k in range(4)] for g in range(4)]
+    return first + second
+
+
+def to_all(shard, axis, sets):
+    copies = jnp.broadcast_to(shard, (len(sets[0]), *shard.shape))
+    return lax.all_to_all(
+        copies, axis, split_axis=0, concat_axis=0, axis_index_groups=sets, tiled=True
+    )
 
 
 def exchange(blocks, axis):
     return lax.all_to_all(blocks, axis, split_axis=0, concat_axis=0, tiled=True)
+
+
+def held_at(t):
+    return jnp.where(spot("c") == 0, (t % 4) * 4 + t // 4, t)
 
 
 def on_device(
@@ -319,22 +334,19 @@
     queries, key_vectors, value_vectors, decay_rates, proj_weight,
     gate_weight, up_weight, down_weight,
 ):
-    place, core, part = [lax.axis_index(a).astype(jnp.int32) for a in ("z", "c", "tp")]
-    where = jnp.stack([place, core, part])
     ids = expert_ids.T
-    cot = lax.dynamic_slice_in_dim(cotangent, part * COL, COL, 1)
-    inp = lax.dynamic_slice_in_dim(moe_input, part * COL, COL, 1)
-
-    keep, send = call(
+    keep, send, cot = call(
         pack_kernel,
-        [arr((NZ, 4 * CAP, COL), BF)] * 2,
-        (where, ids, group_weight.reshape(1, TOK), expert_weight.T, cot, inp),
+        [arr((NZ, 4 * CAP, COL), BF)] * 2 + [arr((TOK, COL), BF)],
+        (ids, group_weight.reshape(1, TOK), expert_weight.T, cotangent, moe_input),
         "pack",
     )
     rows = keep + lax.ppermute(send, "c", SWAP)
     rows = exchange(rows, "z")
     rows = rows.reshape(NZ, 2, 2 * CAP, COL).transpose(1, 0, 2, 3).reshape(2, NZ * 2 * CAP, COL)
-    rows = to_all(rows, "tp")
+    rows = to_all(rows, ("c", "tp"), groups(4, 1, 1, 4))
+    rows = to_all(rows, ("c", "tp"), groups(1, 4, 4, 1))
+    rows = rows.reshape(NT, 2, NZ * 2 * CAP, COL)
 
     pick_keep, pick_send, piece, weight, mixed, scores, kv = call(
         early_kernel,
@@ -342,35 +354,38 @@
             arr((NZ * 32, TOK), BF), arr((NZ * 32, TOK), BF), arr((8, TOK), BF), arr((8, TOK), F32),
             arr((TOK, TOK), F32), arr((TOK, TOK), F32), arr((2, KD, VD), F32),
         ],
-        (where, ids, decay_rates, queries, key_vectors, value_vectors),
+        (ids, decay_rates, queries, key_vectors, value_vectors),
         "early",
     )
 
     shares, hidden, both = call(
         expert_kernel,
         [arr((NT, 384, COL), BF), arr((384, 128), BF), arr((384, 256), BF)],
-        (where, rows, gate_weight[0], up_weight[0], down_weight[0]),
+        (rows, gate_weight[0], up_weight[0], down_weight[0]),
         "expert",
+        20,
     )
     grad_gate, grad_up, grad_down = call(
         weight_kernel,
         [arr((2048, 128), BF), arr((2048, 128), BF), arr((128, 2048), BF)],
-        (where, rows, hidden, both),
+        (rows, hidden, both),
         "weights",
+        16,
         1 << 29,
     )
     shares = exchange(shares, "tp")
-    back = call(sum_kernel, arr((NZ, 32, COL), BF), (where, shares, piece), "sums")
+    back = call(sum_kernel, arr((NZ, 32, COL), BF), (shares, piece), "sums", 6)
     own = exchange(back, "z")
     other = lax.ppermute(own, "c", SWAP)
     resid = call(
         resid_kernel,
         arr((NT, TOK, COL), BF),
         (
-            where, pick_keep, pick_send,
+            pick_keep, pick_send,
             own.reshape(NZ * 32, COL), other.reshape(NZ * 32, COL), cot,
         ),
         "resid",
+        4,
     )
     resid = exchange(resid, "tp")
     out_grad, proj_keep, proj_send, state = call(
@@ -379,21 +394,22 @@
             arr((TOK, VD), F32), arr((NZ, 64, COL), F32), arr((20, 64, COL), BF),
             arr((2, KD, VD), F32),
         ],
-        (where, resid, proj_weight, mixer_out, queries, weight, kv),
+        (resid, proj_weight, mixer_out, queries, weight, kv),
         "proj",
+        8,
     )
     got = lax.ppermute(proj_send, "c", SWAP)
     chip = call(
         chip_kernel,
         arr((NZ, 128, COL), BF),
-        (where, proj_keep, got, state, kv, own, other),
+        (proj_keep, got, state, kv, own, other),
         "chip",
     )
     chip = exchange(chip, "z")
     grad_proj, far = call(
         gather_kernel,
         [arr((64, COL), F32), arr((2, 64, COL), F32)],
-        (where, chip, own, other),
+        (chip, own, other),
         "gather",
     )
     far = lax.all_gather(far, "c")
@@ -401,7 +417,7 @@
         final_kernel,
         [arr((KD, TOK), F32), arr((KD, TOK), F32), arr((VD, TOK), F32)],
         (
-            where, far, got, out_grad, mixed, scores, weight,
+            far, got, out_grad, mixed, scores, weight,
             queries, key_vectors, value_vectors, own, other,
         ),
         "final",

time: 217 us -> 205 us (0.945)
  local copies, waits for them, and re-layouts: 5.46 us -> 22.1 us
  Pallas kernels: 27.3 us -> 10.7 us
  blocking collectives: 115 us -> 103 us
  starting transfers between devices: 27 us -> 29.6 us
    all_to_all x4 -> x3, blocking collectives: 105 us -> 57.6 us  [exchange(): return lax.all_to_all(blocks, axis, split_axis=0, concat_axis=0, tiled=True)]
    all_to_all x0 -> x2, blocking collectives: none -> 37.5 us  [to_all(): lax.all_to_all(copies, axis, split_axis=0, concat_axis=0, axis_index_grou...]
    unnamed x10 -> x76, local copies, waits for them, and re-layouts: 3.33 us -> 21.2 us
    pallas_call x10, Pallas kernels: 27.3 us -> 10.7 us  [call(): pl.pallas_call(kernel, out_shape=outs, in_specs=[vmem()] * len(args), out...]
    all_gather x1, blocking collectives: 10.3 us -> 7.44 us  [on_device(): far = lax.all_gather(far, 'c')]
  transfers between devices with their start and end apart: 5 -> 5, of which waited for: 5 -> 5; matrix products, arithmetic and copies ran while one was open for 0% -> 0% of each run, Pallas kernels for 3% -> 1%
where the time goes in v2:
time: 205 us; the launch traced here: 204 us
  blocking collectives  103 us (50%)
  waiting for transfers between devices  38 us (19%)
  starting transfers between devices  29.6 us (14%)
  local copies, waits for them, and re-layouts  22.1 us (11%)
  Pallas kernels  10.7 us (5%)
    all_to_all x3, blocking collectives, exchange(): return lax.all_to_all(blocks, axis, split_axis=0, concat_axis=0, tiled=True)  57.6 us
    all_to_all x2, blocking collectives, to_all(): lax.all_to_all(copies, axis, split_axis=0, concat_axis=0, axis_index_grou...  37.5 us
    all_to_all x2, waiting for transfers between devices, exchange(): return lax.all_to_all(blocks, axis, split_axis=0, concat_axis=0, tiled=True)  34.7 us
    unnamed x76, local copies, waits for them, and re-layouts  21.2 us
    pallas_call x10, Pallas kernels, call(): pl.pallas_call(kernel, out_shape=outs, in_specs=[vmem()] * len(args), out...  10.7 us
    ppermute x1, starting transfers between devices, on_device(): rows = keep + lax.ppermute(send, 'c', SWAP)  8.75 us
    all_to_all x2, starting transfers between devices, exchange(): return lax.all_to_all(blocks, axis, split_axis=0, concat_axis=0, tiled=True)  8.63 us
    ppermute x1, starting transfers between devices, on_device(): other = lax.ppermute(own, 'c', SWAP)  8.57 us
  transfers between devices with their start and end apart: 5, of which 5 were waited for; matrix products, arithmetic and copies ran while one was open for 0% of the time, Pallas kernels for 1%

profile of v2, /device:TPU:1, one launch (start us, length us, event | category | flops | bytes accessed | tf_op | source)
XLA Modules:
  0.0 203.9 jit_solution(2752879058632235116)
XLA Ops:
  0.6 1.0 copy-done.8
  1.7 1.0 copy-done.9
  2.7 0.7 copy-done.33
  3.4 0.7 copy-done.34
  4.1 0.7 copy-done.36
  4.7 0.5 pack.1
  5.3 0.0 copy-start.26
  5.3 8.7 %collective-permute-start = (bf16[16,48,128]{2,1,0:T(8,128)(2,1)S(1)}, bf16[16,48,128]{2,1,0:T(8,128)(2,1)S(1)}, u32[]{:S(2)}, u32[]{:S(2)}) collective-permute-start(bf16[16,48,128]{2,1,0:T(8,128)(2,1)S(1)} %get-tuple-element.33), channel_id=1, source_target_pairs={{0,16},{16,0},{1,17},{17,1},{2,18},{18,2},{3,19},{19,3},{4,20},{20... | collective-permute-start | bytes 589832 | tf_op jit(solution)/shard_map/ppermute | solution.py:344
  14.1 1.0 collective-permute-done
  15.1 0.1 add.3
  15.2 22.2 %all_to_all.35 = bf16[16,48,128]{2,1,0:T(8,128)(2,1)S(1)} all-to-all(bf16[16,48,128]{2,1,0:T(8,128)(2,1)S(1)} %add.3), channel_id=1, replica_groups=mesh['z'=16,'c'=2,'tp'=16] {'z'}, dimensions={0} | all-to-all | bytes 393216 | tf_op jit(solution)/shard_map/all_to_all | solution.py:325
  37.4 0.1 broadcast_in_dim.15
  37.5 12.1 %all_to_all.36 = bf16[4,2,384,128]{3,2,1,0:T(8,128)(2,1)S(1)} all-to-all(bf16[4,2,384,128]{3,2,1,0:T(8,128)(2,1)S(1)} %broadcast_in_dim.15), channel_id=1, replica_groups={{0,4,8,12},{1,5,9,13},{2,6,10,14},{3,7,11,15},{16,17,18,19},{20,21,22,2..., dimensions={0} | all-to-all | bytes 1572864 | tf_op jit(solution)/shard_map/all_to_all | solution.py:319
  49.7 0.7 broadcast_in_dim.16
  50.4 0.0 copy-start.4
  50.4 0.0 copy-start.5
  50.4 0.0 copy-start.6
  50.4 25.4 %all_to_all.37 = bf16[4,4,2,384,128]{4,3,2,1,0:T(8,128)(2,1)S(1)} all-to-all(bf16[4,4,2,384,128]{4,3,2,1,0:T(8,128)(2,1)S(1)} %broadcast_in_dim.16), channel_id=1, replica_groups={{0,1,2,3},{4,5,6,7},{8,9,10,11},{12,13,14,15},{16,20,24,28},{17,21,25,2..., dimensions={0} | all-to-all | bytes 6291456 | tf_op jit(solution)/shard_map/all_to_all | solution.py:319
  75.8 0.0 copy-start.18
  75.8 0.0 copy-start.24
  75.9 0.0 copy-start.37
  75.9 1.4 expert.1
  77.3 1.2 copy-done.1
  78.5 0.7 copy-done.10
  79.2 0.6 copy-done.16
  79.8 4.4 %all-to-all-start.3 = ((bf16[16,384,128]{2,1,0:T(8,128)(2,1)}), bf16[16,384,128]{2,1,0:T(8,128)(2,1)}, u32[]{:S(2)}, u32[]{:S(2)}) async-start(bf16[16,384,128]{2,1,0:T(8,128)(2,1)} %copy-done.1), calls=%async_computation.3 | async-start | bytes 3145728 | tf_op jit(solution)/shard_map/all_to_all | solution.py:325
  84.3 0.6 early.1
  84.8 0.0 copy-start.12
  84.8 0.6 copy-done.12
  85.5 0.7 copy-done.14
  86.2 0.6 copy-done.19
  86.8 0.6 copy-done.30
  87.4 15.0 %all-to-all-done.3.part_ref = bf16[16,384,128]{2,1,0:T(8,128)(2,1)} async-done(((bf16[16,384,128]{2,1,0:T(8,128)(2,1)}), bf16[16,384,128]{2,1,0:T(8,128)(2,1)}, u32[]{:S(2)}, u32[]{:S(2)}) %all-to-all-start.3) | async-done | bytes 1572896 | tf_op jit(solution)/shard_map/all_to_all | solution.py:325
  102.3 1.7 sums.1
  104.0 21.7 %all_to_all.38.own_ref = bf16[16,32,128]{2,1,0:T(8,128)(2,1)S(1)} all-to-all(bf16[16,32,128]{2,1,0:T(8,128)(2,1)S(1)} %sums.1), channel_id=1, replica_groups=mesh['z'=16,'c'=2,'tp'=16] {'z'}, dimensions={0} | all-to-all | bytes 262144 | tf_op jit(solution)/shard_map/all_to_all | solution.py:325
  125.8 8.6 %collective-permute-start.1 = (bf16[16,32,128]{2,1,0:T(8,128)(2,1)S(1)}, bf16[16,32,128]{2,1,0:T(8,128)(2,1)S(1)}, u32[]{:S(2)}, u32[]{:S(2)}) collective-permute-start(bf16[16,32,128]{2,1,0:T(8,128)(2,1)S(1)} %all_to_all.38.own_ref), channel_id=1, source_target_pairs={{0,16},{16,0},{1,17},{17,1},{2,18},{18,2},{3,19},{19,3},{4,20},{20... | collective-permute-start | bytes 393224 | tf_op jit(solution)/shard_map/ppermute | solution.py:379
  134.3 1.0 collective-permute-done.1.other_ref
  135.3 0.9 copy-done.13
  136.2 0.9 copy-done.15
  137.1 0.8 copy-done.27
  137.9 0.3 resid.1
  138.1 13.6 %all_to_all.39.r_ref = bf16[16,128,128]{2,1,0:T(8,128)(2,1)S(1)} all-to-all(bf16[16,128,128]{2,1,0:T(8,128)(2,1)S(1)} %resid.1), channel_id=1, replica_groups=mesh['z'=16,'c'=2,'tp'=16] {'tp'}, dimensions={0} | all-to-all | bytes 1048576 | tf_op jit(solution)/shard_map/all_to_all | solution.py:325
  151.8 0.8 copy-done.23
  152.6 0.7 proj.1
  153.2 0.6 copy-done.21
  153.9 3.6 %collective-permute-start.2 = (bf16[20,64,128]{2,1,0:T(8,128)(2,1)S(1)}, bf16[20,64,128]{2,1,0:T(8,128)(2,1)S(1)}, u32[]{:S(2)}, u32[]{:S(2)}) collective-permute-start(bf16[20,64,128]{2,1,0:T(8,128)(2,1)S(1)} %get-tuple-element.47), channel_id=1, source_target_pairs={{0,16},{16,0},{1,17},{17,1},{2,18},{18,2},{3,19},{19,3},{4,20},{20... | collective-permute-start | bytes 983048 | tf_op jit(solution)/shard_map/ppermute | solution.py:401
  157.5 1.2 collective-permute-done.2.got_ref
  158.7 0.1 chip.1
  158.9 0.8 copy-done
  159.7 0.7 copy-done.2
  160.4 4.2 %all-to-all-start.6 = ((bf16[16,128,128]{2,1,0:T(8,128)(2,1)}), bf16[16,128,128]{2,1,0:T(8,128)(2,1)}, u32[]{:S(2)}, u32[]{:S(2)}) async-start(bf16[16,128,128]{2,1,0:T(8,128)(2,1)} %copy-done), calls=%async_computation.6 | async-start | bytes 1048576 | tf_op jit(solution)/shard_map/all_to_all | solution.py:325
  164.6 0.9 copy-done.11
  165.6 0.9 copy-done.17
  166.5 2.2 %weights.1 = (bf16[2048,128]{1,0:T(8,128)(2,1)}, bf16[2048,128]{1,0:T(8,128)(2,1)}, bf16[128,2048]{1,0:T(8,128)(2,1)}) custom-call(bf16[16,2,384,128]{3,2,1,0:T(8,128)(2,1)S(1)} %bitcast.18, bf16[384,128]{1,0:T(8,128)(2,1)S(1)} %copy-done.17, bf16[384,256]{1,0:T(8,128)(2,1)S(1)} %copy-done.11), custom_call_target="tpu_custom_call" | custom-call | flops 536870912 | bytes 1048576 | tf_op jit(solution)/shard_map/weights/pallas_call | solution.py:40
  168.6 19.8 %all-to-all-done.6.got_ref = bf16[16,128,128]{2,1,0:T(8,128)(2,1)} async-done(((bf16[16,128,128]{2,1,0:T(8,128)(2,1)}), bf16[16,128,128]{2,1,0:T(8,128)(2,1)}, u32[]{:S(2)}, u32[]{:S(2)}) %all-to-all-start.6) | async-done | bytes 524320 | tf_op jit(solution)/shard_map/all_to_all | solution.py:325
  188.4 1.7 gather.1
  190.1 7.4 %all-gather = f32[4,64,128]{2,1,0:T(8,128)S(1)} all-gather(f32[2,64,128]{2,1,0:T(8,128)S(1)} %get-tuple-element.50), channel_id=2, replica_groups=mesh['z'=16,'c'=2,'tp'=16] {'c'}, dimensions={0}, use_global_device_ids=true | all-gather | bytes 196608 | tf_op jit(solution)/shard_map/all_gather | solution.py:415
  197.6 1.0 copy-done.3
  198.5 0.8 copy-done.20
  199.4 0.8 copy-done.22
  200.2 0.8 copy-done.25
  201.0 0.7 copy-done.29
  201.7 0.7 copy-done.32
  202.4 1.5 final.1
  (42 shorter events, 0.1 us)
Async XLA Ops:
  0.6 1.0 copy-start.8
  1.7 1.0 copy-start.9
  2.7 0.7 copy-start.33
  3.4 0.7 copy-start.34
  4.1 0.7 copy-start.36
  5.3 44.4 %copy-start.26 = (bf16[128,128]{1,0:T(8,128)(2,1)}, bf16[128,128]{1,0:T(8,128)(2,1)S(1)}, u32[]{:S(2)}) copy-start(bf16[128,128]{1,0:T(8,128)(2,1)S(1)} %get-tuple-element.43.cot_ref) | copy-start | bytes 98308
  5.3 9.8 %collective-permute-start = (bf16[16,48,128]{2,1,0:T(8,128)(2,1)S(1)}, bf16[16,48,128]{2,1,0:T(8,128)(2,1)S(1)}, u32[]{:S(2)}, u32[]{:S(2)}) collective-permute-start(bf16[16,48,128]{2,1,0:T(8,128)(2,1)S(1)} %get-tuple-element.33), channel_id=1, source_target_pairs={{0,16},{16,0},{1,17},{17,1},{2,18},{18,2},{3,19},{19,3},{4,20},{20... | collective-permute-start | bytes 589832 | tf_op jit(solution)/shard_map/ppermute | solution.py:344
  50.4 25.4 %copy-start.4 = (bf16[1,2048,128]{2,1,0:T(8,128)(2,1)S(1)}, bf16[1,2048,128]{2,1,0:T(8,128)(2,1)}, u32[]{:S(2)}) copy-start(bf16[1,2048,128]{2,1,0:T(8,128)(2,1)} %param.25) | copy-start | bytes 1572868
  50.4 25.4 %copy-start.5 = (bf16[1,2048,128]{2,1,0:T(8,128)(2,1)S(1)}, bf16[1,2048,128]{2,1,0:T(8,128)(2,1)}, u32[]{:S(2)}) copy-start(bf16[1,2048,128]{2,1,0:T(8,128)(2,1)} %param.26) | copy-start | bytes 1572868
  50.4 25.4 %copy-start.6 = (bf16[1,128,2048]{2,1,0:T(8,128)(2,1)S(1)}, bf16[1,128,2048]{2,1,0:T(8,128)(2,1)}, u32[]{:S(2)}) copy-start(bf16[1,128,2048]{2,1,0:T(8,128)(2,1)} %param.27) | copy-start | bytes 1572868
  75.8 8.4 %copy-start.18 = (bf16[64,128]{1,0:T(8,128)(2,1)S(1)}, bf16[64,128]{1,0:T(8,128)(2,1)}, u32[]{:S(2)}) copy-start(bf16[64,128]{1,0:T(8,128)(2,1)} %q_ref.5) | copy-start | bytes 49156
  75.8 8.4 %copy-start.24 = (bf16[128,128]{1,0:T(8,128)(2,1)S(1)}, bf16[128,128]{1,0:T(8,128)(2,1)}, u32[]{:S(2)}) copy-start(bf16[128,128]{1,0:T(8,128)(2,1)} %v_ref.3) | copy-start | bytes 98308
  75.8 8.4 %copy-start.28 = (bf16[64,128]{1,0:T(8,128)(2,1)S(1)}, bf16[64,128]{1,0:T(8,128)(2,1)}, u32[]{:S(2)}) copy-start(bf16[64,128]{1,0:T(8,128)(2,1)} %k_ref.3) | copy-start | bytes 49156
  75.8 8.4 %copy-start.35 = (s32[128,2]{0,1:T(2,128)S(1)}, s32[128,2]{0,1:T(2,128)}, u32[]{:S(2)}) copy-start(s32[128,2]{0,1:T(2,128)} %param.16) | copy-start | bytes 3076
  75.9 8.4 %copy-start.37 = (f32[1,128]{1,0:T(1,128)S(1)}, f32[1,128]{1,0:T(1,128)}, u32[]{:S(2)}) copy-start(f32[1,128]{1,0:T(1,128)} %rate_ref.1) | copy-start | bytes 1540
  77.3 1.2 copy-start.1
  78.5 0.7 copy-start.10
  79.2 0.6 copy-start.16
  79.8 22.5 %all-to-all-start.3 = ((bf16[16,384,128]{2,1,0:T(8,128)(2,1)}), bf16[16,384,128]{2,1,0:T(8,128)(2,1)}, u32[]{:S(2)}, u32[]{:S(2)}) async-start(bf16[16,384,128]{2,1,0:T(8,128)(2,1)} %copy-done.1), calls=%async_computation.3 | async-start | bytes 3145728 | tf_op jit(solution)/shard_map/all_to_all | solution.py:325
  84.8 0.7 copy-start.12
  85.5 0.7 copy-start.14
  86.2 0.6 copy-start.19
  86.8 0.6 copy-start.30
  102.3 49.5 %copy-start.7 = (bf16[2048,128]{1,0:T(8,128)(2,1)S(1)}, bf16[2048,128]{1,0:T(8,128)(2,1)}, u32[]{:S(2)}) copy-start(bf16[2048,128]{1,0:T(8,128)(2,1)} %p_ref.1) | copy-start | bytes 1572868
  102.3 49.5 %copy-start.31 = (f32[8,128]{1,0:T(8,128)S(1)}, f32[8,128]{1,0:T(8,128)}, u32[]{:S(2)}) copy-start(f32[8,128]{1,0:T(8,128)} %copy-done.30) | copy-start | bytes 12292
  125.8 9.5 %collective-permute-start.1 = (bf16[16,32,128]{2,1,0:T(8,128)(2,1)S(1)}, bf16[16,32,128]{2,1,0:T(8,128)(2,1)S(1)}, u32[]{:S(2)}, u32[]{:S(2)}) collective-permute-start(bf16[16,32,128]{2,1,0:T(8,128)(2,1)S(1)} %all_to_all.38.own_ref), channel_id=1, source_target_pairs={{0,16},{16,0},{1,17},{17,1},{2,18},{18,2},{3,19},{19,3},{4,20},{20... | collective-permute-start | bytes 393224 | tf_op jit(solution)/shard_map/ppermute | solution.py:379
  135.3 0.9 copy-start.13
  136.2 0.9 copy-start.15
  137.1 0.8 copy-start.27
  151.8 0.8 copy-start.23
  153.2 0.6 copy-start.21
  153.9 4.9 %collective-permute-start.2 = (bf16[20,64,128]{2,1,0:T(8,128)(2,1)S(1)}, bf16[20,64,128]{2,1,0:T(8,128)(2,1)S(1)}, u32[]{:S(2)}, u32[]{:S(2)}) collective-permute-start(bf16[20,64,128]{2,1,0:T(8,128)(2,1)S(1)} %get-tuple-element.47), channel_id=1, source_target_pairs={{0,16},{16,0},{1,17},{17,1},{2,18},{18,2},{3,19},{19,3},{4,20},{20... | collective-permute-start | bytes 983048 | tf_op jit(solution)/shard_map/ppermute | solution.py:401
  158.9 0.8 copy-start
  159.7 0.7 copy-start.2
  160.4 28.0 %all-to-all-start.6 = ((bf16[16,128,128]{2,1,0:T(8,128)(2,1)}), bf16[16,128,128]{2,1,0:T(8,128)(2,1)}, u32[]{:S(2)}, u32[]{:S(2)}) async-start(bf16[16,128,128]{2,1,0:T(8,128)(2,1)} %copy-done), calls=%async_computation.6 | async-start | bytes 1048576 | tf_op jit(solution)/shard_map/all_to_all | solution.py:325
  164.6 0.9 copy-start.11
  165.6 0.9 copy-start.17
  197.6 1.0 copy-start.3
  198.5 0.8 copy-start.20
  199.4 0.8 copy-start.22
  200.2 0.8 copy-start.25
  201.0 0.7 copy-start.29
  201.7 0.7 copy-start.32

commit v3 on v2

v3 whole, which is shorter than its diff:
```python
import jax
import jax.numpy as jnp
from jax import lax
from jax.experimental import pallas as pl
from jax.experimental.pallas import tpu as pltpu
from jax.sharding import Mesh
from jax.sharding import PartitionSpec as P

BF = jnp.bfloat16
F32 = jnp.float32
NZ = 16
NT = 16
CAP = 12
TOK = 128
COL = 128
KD = 64
VD = 128
SP = ("z", "c")
HIGHEST = lax.Precision.HIGHEST
SWAP = [(0, 1), (1, 0)]

NN = (((1,), (0,)), ((), ()))
NTR = (((1,), (1,)), ((), ()))
TN = (((0,), (0,)), ((), ()))


def mm(a, b, dims=NN):
    return lax.dot_general(a, b, dims, preferred_element_type=F32)


def exact(a, b, dims=NN):
    return lax.dot_general(a, b, dims, precision=HIGHEST, preferred_element_type=F32)


def vmem():
    return pl.BlockSpec(memory_space=pltpu.VMEM)


def hbm():
    return pl.BlockSpec(memory_space=pltpu.HBM)


def call(kernel, outs, args, name, mib=4, flops=1 << 27, stay=0, scratch=()):
    return pl.pallas_call(
        kernel,
        out_shape=outs,
        in_specs=[hbm()] * stay + [vmem()] * (len(args) - stay),
        out_specs=jax.tree.map(lambda _: vmem(), outs),
        scratch_shapes=scratch,
        name=name,
        compiler_params=pltpu.CompilerParams(vmem_limit_bytes=mib << 20),
        cost_estimate=pl.CostEstimate(flops=flops, bytes_accessed=1 << 20, transcendentals=0),
    )(*args)


def spot(axis):
    return lax.axis_index(axis).astype(jnp.int32)


def fetch(sources, targets, sems):
    copies = [
        pltpu.make_async_copy(src, dst, sems.at[n])
        for n, (src, dst) in enumerate(zip(sources, targets))
    ]
    for copy in copies:
        copy.start()
    for copy in copies:
        copy.wait()


def arr(shape, dtype):
    return jax.ShapeDtypeStruct(shape, dtype)


def placement(ids, wanted, rank):
    first = ids[0:1, :] == wanted
    match = first | (ids[1:2, :] == wanted)
    tok = TOK
    before = lax.broadcasted_iota(jnp.int32, (tok, tok), 0) < lax.broadcasted_iota(
        jnp.int32, (tok, tok), 1
    )
    ranks = mm(jnp.where(match, 1.0, 0.0).astype(BF), jnp.where(before, 1.0, 0.0).astype(BF))
    return match & (ranks == rank.astype(F32)), first


def rows_of(stride, shift, mul, core):
    n = lax.broadcasted_iota(jnp.int32, (NZ * stride, TOK), 0)
    z = lax.shift_right_logical(n * mul, shift)
    q = n - stride * z
    keep = jnp.where(q < CAP, 2 * z + core, -1)
    send = jnp.where((q >= CAP) & (q < 2 * CAP), 2 * z + 1 - core, -1)
    return keep, q, send, q - CAP


def decay_parts(rates):
    upto = lax.broadcasted_iota(jnp.int32, (TOK, TOK), 1) <= lax.broadcasted_iota(
        jnp.int32, (TOK, TOK), 0
    )
    col = jnp.broadcast_to(
        jnp.sum(jnp.where(upto, rates, 0.0), axis=1, keepdims=True), (TOK, TOK)
    )
    row = col.T
    total = jnp.sum(rates, axis=1, keepdims=True)
    prefix = row[0:1, :]
    start = jnp.exp(-prefix)
    end = jnp.exp(jnp.minimum(prefix - total, 0.0))
    return col, row, start, end, jnp.broadcast_to(total, (1, TOK))


def in_pieces(total):
    hi = jnp.broadcast_to(total, (8, TOK)).astype(BF).astype(F32)
    mid = (total - hi).astype(BF).astype(F32)
    low = total - hi - mid
    number = lax.broadcasted_iota(jnp.int32, (8, TOK), 0)
    return jnp.where(
        number == 0, hi, jnp.where(number == 1, mid, jnp.where(number == 2, low, 0.0))
    ).astype(BF)


def pack_kernel(
    ids_in, gw_in, ew_in, cot_in, inp_in, rate_in, k_in, v_in,
    keep_ref, send_ref, cols_ref, mine_ref,
    ids_ref, gw_ref, ew_ref, inp_ref, rate_ref, k_ref, v_ref, sems,
):
    here = pl.ds(pl.multiple_of(spot("tp") * COL, COL), COL)
    fetch(
        (ids_in, gw_in, ew_in, cot_in.at[:, here], inp_in.at[:, here], rate_in, k_in, v_in),
        (ids_ref, gw_ref, ew_ref, cols_ref, inp_ref, rate_ref, k_ref, v_ref),
        sems,
    )
    ids = ids_ref[...]
    weights = gw_ref[...] * ew_ref[...]
    cot, inp = cols_ref[...], inp_ref[...]
    ek, rk, es, rs = rows_of(2 * CAP, 16, 2731, spot("c"))
    for wanted, rank, out in ((ek, rk, keep_ref), (es, rs, send_ref)):
        hit, first = placement(ids, wanted, rank)
        scale = jnp.sum(
            jnp.where(hit, jnp.where(first, weights[0:1, :], weights[1:2, :]), 0.0),
            axis=1,
            keepdims=True,
        )
        take = jnp.where(hit, 1.0, 0.0).astype(BF)
        inp_rows = mm(take, inp)
        cot_rows = mm(take, cot) * scale
        for z in range(NZ):
            part = slice(2 * CAP * z, 2 * CAP * (z + 1))
            at = 4 * CAP * z
            out[at : at + 2 * CAP, :] = inp_rows[part].astype(BF)
            out[at + 2 * CAP : at + 4 * CAP, :] = cot_rows[part].astype(BF)
    _, _, start, end, total = decay_parts(rate_ref[...])
    keys, values = k_ref[...].astype(F32), v_ref[...].astype(F32)
    early = exact(keys * end, values, NTR)
    late = exact(keys * start, values, NTR)
    mine_ref[0:64, :] = early
    mine_ref[64:128, :] = late
    mine_ref[128:136, :] = jnp.broadcast_to(total, (8, TOK))
    send_ref[768:832, :] = early.astype(BF)
    send_ref[832:896, :] = late.astype(BF)
    send_ref[896:904, :] = in_pieces(total)
    send_ref[904:912, :] = jnp.zeros((8, TOK), BF)


def table_kernel(ids_in, rate_in, q_in, k_in, picks_ref, table_ref, ids_ref, rate_ref, q_ref, k_ref, sems):
    fetch((ids_in, rate_in, q_in, k_in), (ids_ref, rate_ref, q_ref, k_ref), sems)
    ek, rk, es, rs = rows_of(32, 5, 1, spot("c"))
    ids = ids_ref[...]
    for wanted, rank, at in ((ek, rk, 0), (es, rs, 512)):
        hit, _ = placement(ids, wanted, rank)
        picks_ref[at : at + 512, :] = jnp.where(hit, 1.0, 0.0).astype(BF)
    col, row, start, end, _ = decay_parts(rate_ref[...])
    mixed = KD ** (-0.5) * jnp.exp(-jnp.abs(col - row))
    table_ref[0:128, :] = mixed
    table_ref[128:256, :] = mm(q_ref[...], k_ref[...], TN) * mixed
    table_ref[256:264, :] = jnp.concatenate([start, end, jnp.zeros((6, TOK), F32)], axis=0)


def expert_kernel(x_ref, gw_ref, uw_ref, dw_ref, part_ref, hid_ref, both_ref):
    inp = jnp.concatenate([x_ref[held_at(t), 0] for t in range(NT)], axis=1)
    cot = jnp.concatenate([x_ref[held_at(t), 1] for t in range(NT)], axis=1)
    both_w = jnp.concatenate([gw_ref[...], uw_ref[...]], axis=1)
    pre = mm(inp, both_w)
    gate, up = pre[:, :128], pre[:, 128:]
    hidden_grad = mm(cot, dw_ref[...], NTR)
    sig = jax.nn.sigmoid(gate)
    act = gate * sig
    hid_ref[...] = (act * up).astype(BF)
    gate_grad = (hidden_grad * up * sig * (1.0 + gate * (1.0 - sig))).astype(BF)
    up_grad = (hidden_grad * act).astype(BF)
    both = jnp.concatenate([gate_grad, up_grad], axis=1)
    both_ref[...] = both
    for t in range(0, NT, 2):
        out = mm(both, both_w[t * COL : (t + 2) * COL], NTR).astype(BF)
        part_ref[t] = out[:, :COL]
        part_ref[t + 1] = out[:, COL:]


def weight_kernel(x_ref, hid_ref, both_ref, gg_ref, gu_ref, gd_ref):
    both = both_ref[...]
    hidden = hid_ref[...]
    for t in range(0, NT, 2):
        rows = slice(t * COL, (t + 2) * COL)
        inp = jnp.concatenate([x_ref[held_at(t), 0], x_ref[held_at(t + 1), 0]], axis=1)
        cot = jnp.concatenate([x_ref[held_at(t), 1], x_ref[held_at(t + 1), 1]], axis=1)
        out = mm(inp, both, TN).astype(BF)
        gg_ref[rows, :] = out[:, :128]
        gu_ref[rows, :] = out[:, 128:]
        gd_ref[:, rows] = mm(hidden, cot, TN).astype(BF)


def chip_states(early, late, early_other, late_other, mine, theirs):
    is_first = spot("c") == 0
    both_early = early * jnp.where(is_first, theirs, 1.0) + early_other * jnp.where(
        is_first, 1.0, mine
    )
    both_late = late * jnp.where(is_first, 1.0, theirs) + late_other * jnp.where(
        is_first, mine, 1.0
    )
    return [jnp.where(is_first, a[:32], a[32:]).astype(BF) for a in (both_early, both_late)]


def sum_kernel(part_ref, mine_ref, extra_ref, out_ref):
    total = part_ref[0].astype(F32)
    for t in range(1, NT):
        total = total + part_ref[t].astype(F32)
    out_ref[:, 0 : 2 * CAP, :] = total.reshape(NZ, 2 * CAP, COL).astype(BF)
    decay = mine_ref[128:129, :]
    out_ref[:, 2 * CAP : 32, :] = jnp.broadcast_to(in_pieces(decay)[None], (NZ, 8, COL))
    pieces = extra_ref[128:136, :].astype(F32)
    theirs = pieces[0:1, :] + pieces[1:2, :] + pieces[2:3, :]
    early, late = chip_states(
        mine_ref[0:64, :], mine_ref[64:128, :],
        extra_ref[0:64, :].astype(F32), extra_ref[64:128, :].astype(F32),
        jnp.exp(-decay), jnp.exp(-theirs),
    )
    place = spot("z")
    for z in range(NZ):
        out_ref[z, 32:64, :] = jnp.where(z > place, early, late)


def resid_kernel(picks_ref, own_ref, other_ref, cols_ref, out_ref):
    own = own_ref[:, 0:32, :].reshape(512, COL)
    other = other_ref[:, 0:32, :].reshape(512, COL)
    moe = mm(picks_ref[0:512, :], own, TN) + mm(picks_ref[512:1024, :], other, TN)
    resid = (cols_ref[...].astype(F32) + moe).astype(BF)
    for t in range(NT):
        out_ref[t] = resid


def proj_kernel(r_ref, p_ref, mixer_ref, q_ref, table_ref, og_ref, keep_ref, send_ref, state_ref):
    core = spot("c")
    resid = jnp.concatenate([r_ref[t] for t in range(NT)], axis=1)
    out_grad = mm(resid, p_ref[...])
    og_ref[...] = out_grad
    query = q_ref[...].astype(F32)
    early = exact(query * table_ref[257:258, :], out_grad)
    late = exact(query * table_ref[256:257, :], out_grad)
    state_ref[0] = early
    state_ref[1] = late
    send_ref[16] = early.astype(BF)
    send_ref[17] = late.astype(BF)
    mixer = mixer_ref[...]
    for t in range(NT):
        share = mm(r_ref[t], mixer, TN)
        low, high = share[:64], share[64:]
        keep_ref[t] = jnp.where(core == 0, low, high)
        send_ref[t] = jnp.where(core == 0, high, low).astype(BF)


def decays(own_ref, other_ref):
    def total(ref):
        rows = ref[:, 2 * CAP : 32, :].astype(F32)
        return rows[:, 0, :] + rows[:, 1, :] + rows[:, 2, :]

    return total(own_ref), total(other_ref)


def row_at(table, place):
    number = lax.broadcasted_iota(jnp.int32, table.shape, 0)
    return jnp.sum(jnp.where(number == place, table, 0.0), axis=0, keepdims=True)


def at_block(far_early, far_late, near, theirs):
    is_first = spot("c") == 0
    early = far_early * jnp.where(is_first, 1.0, theirs) + jnp.where(is_first, 0.0, near)
    late = far_late * jnp.where(is_first, theirs, 1.0) + jnp.where(is_first, near, 0.0)
    return early, late


def intra_kernel(
    og_ref, table_ref, q_ref, k_ref, v_ref, own_ref, other_ref, extra_ref,
    gq_ref, part_ref, weight_ref,
):
    place, core = spot("z"), spot("c")
    own, other = decays(own_ref, other_ref)
    chip = own + other
    number = lax.broadcasted_iota(jnp.int32, (NZ, COL), 0)
    between = jnp.zeros((NZ, COL), F32)
    for u in range(NZ):
        inside = ((number < u) & (u < place)) | ((number > u) & (u > place))
        between = between + jnp.where(inside, chip[u : u + 1, :], 0.0)
    weight = jnp.exp(-between)
    early_w = jnp.where(number < place, weight, 0.0)
    late_w = jnp.where(number > place, weight, 0.0)
    weight_ref[0:16, :] = early_w
    weight_ref[16:32, :] = late_w

    def far(ref):
        early = late = jnp.zeros((32, COL), F32)
        for z in range(NZ):
            state = ref[z, 32:64, :].astype(F32)
            early = early + state * early_w[z : z + 1, :]
            late = late + state * late_w[z : z + 1, :]
        return early, late

    is_first = core == 0
    here, there = far(own_ref), far(other_ref)
    far_early, far_late = [
        jnp.concatenate([jnp.where(is_first, a, b), jnp.where(is_first, b, a)], axis=0)
        for a, b in zip(here, there)
    ]
    near = jnp.where(is_first, extra_ref[64:128, :], extra_ref[0:64, :]).astype(F32)
    theirs = jnp.exp(-row_at(other, place))
    kv_early, kv_late = at_block(far_early, far_late, near, theirs)
    scale = KD ** (-0.5)
    low = scale * table_ref[256:257, :]
    high = scale * table_ref[257:258, :]
    out_grad = og_ref[...]
    query, key, value = [r[...].astype(F32) for r in (q_ref, k_ref, v_ref)]
    score_grad = exact(out_grad, value) * table_ref[0:128, :]
    gq_ref[...] = (
        exact(key, score_grad, NTR)
        + low * exact(kv_early, out_grad, NTR)
        + high * exact(kv_late, out_grad, NTR)
    )
    part_ref[0:64, :] = exact(query, score_grad)
    part_ref[64:192, :] = exact(out_grad, table_ref[128:256, :], TN)
    part_ref[192:256, :] = key
    part_ref[256:384, :] = value
    part_ref[384:392, :] = jnp.concatenate([low, high, theirs, jnp.zeros((5, TOK), F32)], axis=0)


def chip_kernel(keep_ref, got_ref, state_ref, own_ref, other_ref, out_ref, near_ref):
    place, core = spot("z"), spot("c")
    own, other = decays(own_ref, other_ref)
    mine = jnp.exp(-row_at(own, place))
    theirs = jnp.exp(-row_at(other, place))
    early_other, late_other = got_ref[16].astype(F32), got_ref[17].astype(F32)
    early, late = chip_states(state_ref[0], state_ref[1], early_other, late_other, mine, theirs)
    near_ref[...] = jnp.where(core == 0, late_other, early_other)
    for z in range(NZ):
        out_ref[z, 0:64, :] = (keep_ref[z] + got_ref[z].astype(F32)).astype(BF)
        out_ref[z, 64:96, :] = jnp.where(z > place, early, late)


def gather_kernel(got_ref, weight_ref, proj_ref, state_ref):
    share = jnp.zeros((64, COL), F32)
    early = late = jnp.zeros((32, COL), F32)
    for z in range(NZ):
        share = share + got_ref[z, 0:64, :].astype(F32)
        state = got_ref[z, 64:96, :].astype(F32)
        early = early + state * weight_ref[z : z + 1, :]
        late = late + state * weight_ref[16 + z : 17 + z, :]
    proj_ref[...] = share
    state_ref[0] = early
    state_ref[1] = late


def final_kernel(far_ref, near_ref, part_ref, gk_ref, gv_ref):
    early, late = at_block(
        jnp.concatenate([far_ref[0, 0], far_ref[1, 0]], axis=0),
        jnp.concatenate([far_ref[0, 1], far_ref[1, 1]], axis=0),
        near_ref[...],
        part_ref[386:387, :],
    )
    low, high = part_ref[384:385, :], part_ref[385:386, :]
    key, value = part_ref[192:256, :], part_ref[256:384, :]
    gk_ref[...] = part_ref[0:64, :] + low * exact(early, value) + high * exact(late, value)
    gv_ref[...] = part_ref[64:192, :] + low * exact(early, key, TN) + high * exact(late, key, TN)


def groups(step, stride, step_other, stride_other):
    first = [[stride * g + step * k for k in range(4)] for g in range(4)]
    second = [[16 + stride_other * g + step_other * k for k in range(4)] for g in range(4)]
    return first + second


def to_all(shard, axis, sets):
    copies = jnp.broadcast_to(shard, (len(sets[0]), *shard.shape))
    return lax.all_to_all(
        copies, axis, split_axis=0, concat_axis=0, axis_index_groups=sets, tiled=True
    )


def exchange(blocks, axis):
    return lax.all_to_all(blocks, axis, split_axis=0, concat_axis=0, tiled=True)


def held_at(t):
    return jnp.where(spot("c") == 0, (t % 4) * 4 + t // 4, t)


def on_device(
    cotangent, moe_input, expert_ids, group_weight, expert_weight, mixer_out,
    queries, key_vectors, value_vectors, decay_rates, proj_weight,
    gate_weight, up_weight, down_weight,
):
    ids = expert_ids.T
    keep, send, cols, mine = call(
        pack_kernel,
        [arr((768, COL), BF), arr((912, COL), BF), arr((TOK, COL), BF), arr((136, TOK), F32)],
        (
            ids, group_weight.reshape(1, TOK), expert_weight.T, cotangent, moe_input,
            decay_rates, key_vectors, value_vectors,
        ),
        "pack",
        60,
        stay=8,
        scratch=[
            pltpu.VMEM((2, TOK), jnp.int32), pltpu.VMEM((1, TOK), F32), pltpu.VMEM((2, TOK), F32),
            pltpu.VMEM((TOK, COL), BF), pltpu.VMEM((1, TOK), F32), pltpu.VMEM((KD, TOK), BF),
            pltpu.VMEM((VD, TOK), BF), pltpu.SemaphoreType.DMA((8,)),
        ],
    )
    picks, table = call(
        table_kernel,
        [arr((1024, TOK), BF), arr((264, TOK), F32)],
        (ids, decay_rates, queries, key_vectors),
        "table",
        60,
        stay=4,
        scratch=[
            pltpu.VMEM((2, TOK), jnp.int32), pltpu.VMEM((1, TOK), F32), pltpu.VMEM((KD, TOK), BF),
            pltpu.VMEM((KD, TOK), BF), pltpu.SemaphoreType.DMA((4,)),
        ],
    )
    swapped = lax.ppermute(send, "c", SWAP)
    extra = swapped[768:]
    rows = (keep + swapped[:768]).reshape(NZ, 4 * CAP, COL)
    rows, picks, table, extra = lax.optimization_barrier((rows, picks, table, extra))
    rows = exchange(rows, "z")
    rows = rows.reshape(NZ, 2, 2 * CAP, COL).transpose(1, 0, 2, 3).reshape(2, NZ * 2 * CAP, COL)
    rows = to_all(rows, ("c", "tp"), groups(4, 1, 1, 4))
    rows = to_all(rows, ("c", "tp"), groups(1, 4, 4, 1))
    rows = rows.reshape(NT, 2, NZ * 2 * CAP, COL)
    shares, hidden, both = call(
        expert_kernel,
        [arr((NT, 384, COL), BF), arr((384, 128), BF), arr((384, 256), BF)],
        (rows, gate_weight[0], up_weight[0], down_weight[0]),
        "expert",
        20,
    )
    shares = exchange(shares, "tp")
    back = call(sum_kernel, arr((NZ, 64, COL), BF), (shares, mine, extra), "sums", 6)
    own = exchange(back, "z")
    own, rows, hidden, both = lax.optimization_barrier((own, rows, hidden, both))
    other = lax.ppermute(own, "c", SWAP)
    grad_gate, grad_up, grad_down = call(
        weight_kernel,
        [arr((2048, 128), BF), arr((2048, 128), BF), arr((128, 2048), BF)],
        (rows, hidden, both),
        "weights",
        16,
        1 << 29,
    )
    resid = call(resid_kernel, arr((NT, TOK, COL), BF), (picks, own, other, cols), "resid")
    resid, grad_gate, grad_up, grad_down = lax.optimization_barrier(
        (resid, grad_gate, grad_up, grad_down)
    )
    resid = exchange(resid, "tp")
    out_grad, proj_keep, proj_send, state = call(
        proj_kernel,
        [
            arr((TOK, VD), F32), arr((NZ, 64, COL), F32), arr((18, 64, COL), BF),
            arr((2, KD, VD), F32),
        ],
        (resid, proj_weight, mixer_out, queries, table),
        "proj",
        8,
    )
    got = lax.ppermute(proj_send, "c", SWAP)
    grad_queries, part, weight = call(
        intra_kernel,
        [arr((KD, TOK), F32), arr((392, TOK), F32), arr((32, TOK), F32)],
        (out_grad, table, queries, key_vectors, value_vectors, own, other, extra),
        "intra",
    )
    chip, near = call(
        chip_kernel,
        [arr((NZ, 96, COL), BF), arr((KD, VD), F32)],
        (proj_keep, got, state, own, other),
        "chip",
    )
    chip, grad_queries, part, weight = lax.optimization_barrier((chip, grad_queries, part, weight))
    chip = exchange(chip, "z")
    grad_proj, far = call(
        gather_kernel,
        [arr((64, COL), F32), arr((2, 32, COL), F32)],
        (chip, weight),
        "gather",
    )
    far = lax.all_gather(far, "c")
    grad_keys, grad_values = call(
        final_kernel,
        [arr((KD, TOK), F32), arr((VD, TOK), F32)],
        (far, near, part),
        "final",
    )
    return (
        grad_gate[None], grad_up[None], grad_down[None],
        grad_proj, grad_queries, grad_keys, grad_values,
    )


def solution(mesh):
    finer = Mesh(mesh.devices.reshape(NZ, 2, NT), ("z", "c", "tp"))
    in_specs = (
        P(SP, None), P(SP, None), P(SP, None), P(SP), P(SP, None), P(SP, "tp"),
        P("tp", SP), P("tp", SP), P("tp", SP), P("tp", SP), P(None, "tp"),
        P(SP, None, "tp"), P(SP, None, "tp"), P(SP, "tp", None),
    )
    out_specs = (
        P(SP, None, "tp"), P(SP, None, "tp"), P(SP, "tp", None), P(SP, "tp"),
        P("tp", SP), P("tp", SP), P("tp", SP),
    )
    return jax.shard_map(
        on_device, mesh=finer, in_specs=in_specs, out_specs=out_specs, check_vma=False
    )
```

time: 205 us -> 185 us (0.902)
  blocking collectives: 103 us -> 147 us
  waiting for transfers between devices: 38 us -> 0.01 us
  local copies, waits for them, and re-layouts: 22.1 us -> 0.89 us
  starting transfers between devices: 29.6 us -> 22.5 us
    all_to_all x3 -> x5, blocking collectives: 57.6 us -> 100 us  [exchange(): return lax.all_to_all(blocks, axis, split_axis=0, concat_axis=0, tiled=True)]
    all_to_all x2 -> x0, waiting for transfers between devices: 34.7 us -> none  [exchange(): return lax.all_to_all(blocks, axis, split_axis=0, concat_axis=0, tiled=True)]
    unnamed x76 -> x24, local copies, waits for them, and re-layouts: 21.2 us -> 0.06 us
    all_to_all x2 -> x0, starting transfers between devices: 8.63 us -> none  [exchange(): return lax.all_to_all(blocks, axis, split_axis=0, concat_axis=0, tiled=True)]
    ppermute x1, starting transfers between devices: 8.57 us -> 10.7 us  [on_device(): other = lax.ppermute(own, 'c', SWAP)]
    pallas_call x10 -> x11, Pallas kernels: 10.7 us -> 12.2 us  [call(): pl.pallas_call(kernel, out_shape=outs, in_specs=[hbm()] * stay + [vmem()]...]
  transfers between devices with their start and end apart: 5 -> 3, of which waited for: 5 -> 0; matrix products, arithmetic and copies ran while one was open for 0% -> 0% of each run, Pallas kernels for 1% -> 3%
where the time goes in v3:
time: 185 us
  blocking collectives  147 us (79%)
  starting transfers between devices  22.5 us (12%)
  Pallas kernels  12.2 us (7%)
    all_to_all x5, blocking collectives, exchange(): return lax.all_to_all(blocks, axis, split_axis=0, concat_axis=0, tiled=True)  100 us
    all_to_all x2, blocking collectives, to_all(): lax.all_to_all(copies, axis, split_axis=0, concat_axis=0, axis_index_grou...  37.6 us
    pallas_call x11, Pallas kernels, call(): pl.pallas_call(kernel, out_shape=outs, in_specs=[hbm()] * stay + [vmem()]...  12.2 us
    ppermute x1, starting transfers between devices, on_device(): other = lax.ppermute(own, 'c', SWAP)  10.7 us
    all_gather x1, blocking collectives, on_device(): far = lax.all_gather(far, 'c')  9.16 us
    ppermute x1, starting transfers between devices, on_device(): swapped = lax.ppermute(send, 'c', SWAP)  8.75 us
  transfers between devices with their start and end apart: 3, of which 0 were waited for; matrix products, arithmetic and copies ran while one was open for 0% of the time, Pallas kernels for 3%

profile of v3, /device:TPU:1, one launch (start us, length us, event | category | flops | bytes accessed | tf_op | source)
XLA Modules:
  0.0 184.7 jit_solution(1569164298098027820)
XLA Ops:
  0.6 2.5 %pack.1 = (bf16[768,128]{1,0:T(8,128)(2,1)}, bf16[912,128]{1,0:T(8,128)(2,1)}, bf16[128,128]{1,0:T(8,128)(2,1)}, f32[136,128]{1,0:T(8,128)}) custom-call(s32[2,128]{1,0:T(2,128)} %bitcast.26, f32[1,128]{1,0:T(1,128)} %bitcast.28, f32[2,128]{1,0:T(2,128)} %bitcast.25, bf16[128,2048]{1,0:T(8,128)(2,1)} %cot_in.1, bf16[128,2048]{1,0:T(8,128)(2,1)} %inp_in.1, ...), custom_call_target="tpu_custom_call" | custom-call | flops 134217728 | bytes 1048576 | tf_op jit(solution)/shard_map/pack/pallas_call | solution.py:44
  3.1 8.7 %collective-permute-start = (bf16[912,128]{1,0:T(8,128)(2,1)}, bf16[912,128]{1,0:T(8,128)(2,1)S(1)}, u32[]{:S(2)}, u32[]{:S(2)}) collective-permute-start(bf16[912,128]{1,0:T(8,128)(2,1)} %get-tuple-element.49), channel_id=1, source_target_pairs={{0,16},{16,0},{1,17},{17,1},{2,18},{18,2},{3,19},{19,3},{4,20},{20... | collective-permute-start | bytes 700424 | tf_op jit(solution)/shard_map/ppermute | solution.py:436
  11.9 1.9 %table.1 = (bf16[1024,128]{1,0:T(8,128)(2,1)}, f32[264,128]{1,0:T(8,128)}) custom-call(s32[2,128]{1,0:T(2,128)} %bitcast.27, f32[1,128]{1,0:T(1,128)} %rate_in.3, bf16[64,128]{1,0:T(8,128)(2,1)} %q_ref.3, bf16[64,128]{1,0:T(8,128)(2,1)} %k_ref.1), custom_call_target="tpu_custom_call" | custom-call | flops 134217728 | bytes 1048576 | tf_op jit(solution)/shard_map/table/pallas_call | solution.py:44
  13.8 0.0 collective-permute-done
  13.8 1.0 slice_add_fusion
  14.8 22.6 %all_to_all.35 = bf16[16,48,128]{2,1,0:T(8,128)(2,1)S(1)} all-to-all(bf16[16,48,128]{2,1,0:T(8,128)(2,1)S(1)} %bitcast.23), channel_id=1, replica_groups=mesh['z'=16,'c'=2,'tp'=16] {'z'}, dimensions={0} | all-to-all | bytes 393216 | tf_op jit(solution)/shard_map/all_to_all | solution.py:395
  37.4 0.1 broadcast_in_dim.15
  37.5 12.2 %all_to_all.36 = bf16[4,2,384,128]{3,2,1,0:T(8,128)(2,1)S(1)} all-to-all(bf16[4,2,384,128]{3,2,1,0:T(8,128)(2,1)S(1)} %broadcast_in_dim.15), channel_id=1, replica_groups={{0,4,8,12},{1,5,9,13},{2,6,10,14},{3,7,11,15},{16,17,18,19},{20,21,22,2..., dimensions={0} | all-to-all | bytes 1572864 | tf_op jit(solution)/shard_map/all_to_all | solution.py:389
  49.7 0.7 broadcast_in_dim.16
  50.4 0.0 copy-start.1
  50.4 0.0 copy-start.2
  50.4 0.0 copy-start.3
  50.4 25.4 %all_to_all.37 = bf16[4,4,2,384,128]{4,3,2,1,0:T(8,128)(2,1)S(1)} all-to-all(bf16[4,4,2,384,128]{4,3,2,1,0:T(8,128)(2,1)S(1)} %broadcast_in_dim.16), channel_id=1, replica_groups={{0,1,2,3},{4,5,6,7},{8,9,10,11},{12,13,14,15},{16,20,24,28},{17,21,25,2..., dimensions={0} | all-to-all | bytes 6291456 | tf_op jit(solution)/shard_map/all_to_all | solution.py:389
  75.9 0.0 copy-done.1
  75.9 0.0 copy-done.2
  75.9 0.0 copy-done.3
  75.9 0.0 copy-start.7
  75.9 1.4 expert.1
  77.3 20.1 %all_to_all.38.part_ref = bf16[16,384,128]{2,1,0:T(8,128)(2,1)S(1)} all-to-all(bf16[16,384,128]{2,1,0:T(8,128)(2,1)S(1)} %get-tuple-element.54), channel_id=1, replica_groups=mesh['z'=16,'c'=2,'tp'=16] {'tp'}, dimensions={0} | all-to-all | bytes 3145728 | tf_op jit(solution)/shard_map/all_to_all | solution.py:395
  97.4 0.0 copy-start.5
  97.4 0.0 copy-start.11
  97.4 0.0 copy-done.7
  97.4 0.2 sums.1
  97.6 0.0 copy-start
  97.7 0.0 copy-start.4
  97.7 0.0 copy-start.9
  97.7 0.0 copy-start.10
  97.7 22.6 %all_to_all.39.own_ref = bf16[16,64,128]{2,1,0:T(8,128)(2,1)S(1)} all-to-all(bf16[16,64,128]{2,1,0:T(8,128)(2,1)S(1)} %sums.1), channel_id=1, replica_groups=mesh['z'=16,'c'=2,'tp'=16] {'z'}, dimensions={0} | all-to-all | bytes 524288 | tf_op jit(solution)/shard_map/all_to_all | solution.py:395
  120.3 0.0 copy-start.6
  120.3 0.0 copy-start.8
  120.3 10.7 %collective-permute-start.1 = (bf16[16,64,128]{2,1,0:T(8,128)(2,1)S(1)}, bf16[16,64,128]{2,1,0:T(8,128)(2,1)S(1)}, u32[]{:S(2)}, u32[]{:S(2)}) collective-permute-start(bf16[16,64,128]{2,1,0:T(8,128)(2,1)S(1)} %all_to_all.39.own_ref), channel_id=1, source_target_pairs={{0,16},{16,0},{1,17},{17,1},{2,18},{18,2},{3,19},{19,3},{4,20},{20... | collective-permute-start | bytes 786440 | tf_op jit(solution)/shard_map/ppermute | solution.py:456
  130.9 2.2 %weights.1 = (bf16[2048,128]{1,0:T(8,128)(2,1)}, bf16[2048,128]{1,0:T(8,128)(2,1)}, bf16[128,2048]{1,0:T(8,128)(2,1)}) custom-call(bf16[16,2,384,128]{3,2,1,0:T(8,128)(2,1)S(1)} %bitcast.17, bf16[384,128]{1,0:T(8,128)(2,1)S(1)} %get-tuple-element.62.hid_ref, bf16[384,256]{1,0:T(8,128)(2,1)S(1)} %get-tuple-element.63.both_ref), custom_call_target="tpu_custom_call" | custom-call | flops 536870912 | bytes 1048576 | tf_op jit(solution)/shard_map/weights/pallas_call | solution.py:44
  133.1 0.0 collective-permute-done.1.other_ref
  133.1 0.0 copy-done.5
  133.1 0.0 copy-done.11
  133.1 0.3 resid.1
  133.4 13.9 %all_to_all.40.r_ref = bf16[16,128,128]{2,1,0:T(8,128)(2,1)S(1)} all-to-all(bf16[16,128,128]{2,1,0:T(8,128)(2,1)S(1)} %resid.1), channel_id=1, replica_groups=mesh['z'=16,'c'=2,'tp'=16] {'tp'}, dimensions={0} | all-to-all | bytes 1048576 | tf_op jit(solution)/shard_map/all_to_all | solution.py:395
  147.4 0.0 copy-done
  147.4 0.0 copy-done.4
  147.4 0.0 copy-done.9
  147.4 0.0 copy-done.10
  147.4 0.7 proj.1
  148.1 3.1 %collective-permute-start.2 = (bf16[18,64,128]{2,1,0:T(8,128)(2,1)S(1)}, bf16[18,64,128]{2,1,0:T(8,128)(2,1)S(1)}, u32[]{:S(2)}, u32[]{:S(2)}) collective-permute-start(bf16[18,64,128]{2,1,0:T(8,128)(2,1)S(1)} %get-tuple-element.73), channel_id=1, source_target_pairs={{0,16},{16,0},{1,17},{17,1},{2,18},{18,2},{3,19},{19,3},{4,20},{20... | collective-permute-start | bytes 884744 | tf_op jit(solution)/shard_map/ppermute | solution.py:480
  151.1 0.0 copy-done.6
  151.1 0.0 copy-done.8
  151.2 1.3 intra.1
  152.5 0.0 collective-permute-done.2.got_ref
  152.5 0.1 chip.1
  152.6 21.3 %all_to_all.41.got_ref = bf16[16,96,128]{2,1,0:T(8,128)(2,1)S(1)} all-to-all(bf16[16,96,128]{2,1,0:T(8,128)(2,1)S(1)} %get-tuple-element.80), channel_id=1, replica_groups=mesh['z'=16,'c'=2,'tp'=16] {'z'}, dimensions={0} | all-to-all | bytes 786432 | tf_op jit(solution)/shard_map/all_to_all | solution.py:395
  173.9 0.7 gather.1
  174.5 9.2 %all-gather = f32[4,32,128]{2,1,0:T(8,128)S(1)} all-gather(f32[2,32,128]{2,1,0:T(8,128)S(1)} %get-tuple-element.84), channel_id=2, replica_groups=mesh['z'=16,'c'=2,'tp'=16] {'c'}, dimensions={0}, use_global_device_ids=true | all-gather | bytes 98304 | tf_op jit(solution)/shard_map/all_gather | solution.py:501
  183.7 1.0 final.1
  (2 shorter events, 0.0 us)
Async XLA Ops:
  3.1 10.7 %collective-permute-start = (bf16[912,128]{1,0:T(8,128)(2,1)}, bf16[912,128]{1,0:T(8,128)(2,1)S(1)}, u32[]{:S(2)}, u32[]{:S(2)}) collective-permute-start(bf16[912,128]{1,0:T(8,128)(2,1)} %get-tuple-element.49), channel_id=1, source_target_pairs={{0,16},{16,0},{1,17},{17,1},{2,18},{18,2},{3,19},{19,3},{4,20},{20... | collective-permute-start | bytes 700424 | tf_op jit(solution)/shard_map/ppermute | solution.py:436
  50.4 25.5 %copy-start.1 = (bf16[1,2048,128]{2,1,0:T(8,128)(2,1)S(1)}, bf16[1,2048,128]{2,1,0:T(8,128)(2,1)}, u32[]{:S(2)}) copy-start(bf16[1,2048,128]{2,1,0:T(8,128)(2,1)} %param.25) | copy-start | bytes 1572868
  50.4 25.5 %copy-start.2 = (bf16[1,2048,128]{2,1,0:T(8,128)(2,1)S(1)}, bf16[1,2048,128]{2,1,0:T(8,128)(2,1)}, u32[]{:S(2)}) copy-start(bf16[1,2048,128]{2,1,0:T(8,128)(2,1)} %param.26) | copy-start | bytes 1572868
  50.4 25.5 %copy-start.3 = (bf16[1,128,2048]{2,1,0:T(8,128)(2,1)S(1)}, bf16[1,128,2048]{2,1,0:T(8,128)(2,1)}, u32[]{:S(2)}) copy-start(bf16[1,128,2048]{2,1,0:T(8,128)(2,1)} %param.27) | copy-start | bytes 1572868
  75.9 21.5 %copy-start.7 = (f32[136,128]{1,0:T(8,128)S(1)}, f32[136,128]{1,0:T(8,128)}, u32[]{:S(2)}) copy-start(f32[136,128]{1,0:T(8,128)} %get-tuple-element.55.mine_ref) | copy-start | bytes 208900
  97.4 35.7 %copy-start.5 = (bf16[1024,128]{1,0:T(8,128)(2,1)S(1)}, bf16[1024,128]{1,0:T(8,128)(2,1)}, u32[]{:S(2)}) copy-start(bf16[1024,128]{1,0:T(8,128)(2,1)} %get-tuple-element.52.picks_ref) | copy-start | bytes 786436
  97.4 35.7 %copy-start.11 = (bf16[128,128]{1,0:T(8,128)(2,1)S(1)}, bf16[128,128]{1,0:T(8,128)(2,1)}, u32[]{:S(2)}) copy-start(bf16[128,128]{1,0:T(8,128)(2,1)} %get-tuple-element.60.cols_ref) | copy-start | bytes 98308
  97.6 49.7 %copy-start = (f32[264,128]{1,0:T(8,128)S(1)}, f32[264,128]{1,0:T(8,128)}, u32[]{:S(2)}) copy-start(f32[264,128]{1,0:T(8,128)} %get-tuple-element.71.table_ref) | copy-start | bytes 405508
  97.7 49.7 %copy-start.4 = (bf16[2048,128]{1,0:T(8,128)(2,1)S(1)}, bf16[2048,128]{1,0:T(8,128)(2,1)}, u32[]{:S(2)}) copy-start(bf16[2048,128]{1,0:T(8,128)(2,1)} %p_ref.1) | copy-start | bytes 1572868
  97.7 49.7 %copy-start.9 = (bf16[64,128]{1,0:T(8,128)(2,1)S(1)}, bf16[64,128]{1,0:T(8,128)(2,1)}, u32[]{:S(2)}) copy-start(bf16[64,128]{1,0:T(8,128)(2,1)} %q_ref.3) | copy-start | bytes 49156
  97.7 49.7 %copy-start.10 = (bf16[128,128]{1,0:T(8,128)(2,1)S(1)}, bf16[128,128]{1,0:T(8,128)(2,1)}, u32[]{:S(2)}) copy-start(bf16[128,128]{1,0:T(8,128)(2,1)} %mixer_ref.1) | copy-start | bytes 98308
  120.3 30.9 %copy-start.6 = (bf16[128,128]{1,0:T(8,128)(2,1)S(1)}, bf16[128,128]{1,0:T(8,128)(2,1)}, u32[]{:S(2)}) copy-start(bf16[128,128]{1,0:T(8,128)(2,1)} %v_ref.1) | copy-start | bytes 98308
  120.3 30.9 %copy-start.8 = (bf16[64,128]{1,0:T(8,128)(2,1)S(1)}, bf16[64,128]{1,0:T(8,128)(2,1)}, u32[]{:S(2)}) copy-start(bf16[64,128]{1,0:T(8,128)(2,1)} %k_ref.1) | copy-start | bytes 49156
  120.3 12.9 %collective-permute-start.1 = (bf16[16,64,128]{2,1,0:T(8,128)(2,1)S(1)}, bf16[16,64,128]{2,1,0:T(8,128)(2,1)S(1)}, u32[]{:S(2)}, u32[]{:S(2)}) collective-permute-start(bf16[16,64,128]{2,1,0:T(8,128)(2,1)S(1)} %all_to_all.39.own_ref), channel_id=1, source_target_pairs={{0,16},{16,0},{1,17},{17,1},{2,18},{18,2},{3,19},{19,3},{4,20},{20... | collective-permute-start | bytes 786440 | tf_op jit(solution)/shard_map/ppermute | solution.py:456
  148.1 4.4 %collective-permute-start.2 = (bf16[18,64,128]{2,1,0:T(8,128)(2,1)S(1)}, bf16[18,64,128]{2,1,0:T(8,128)(2,1)S(1)}, u32[]{:S(2)}, u32[]{:S(2)}) collective-permute-start(bf16[18,64,128]{2,1,0:T(8,128)(2,1)S(1)} %get-tuple-element.73), channel_id=1, source_target_pairs={{0,16},{16,0},{1,17},{17,1},{2,18},{18,2},{3,19},{19,3},{4,20},{20... | collective-permute-start | bytes 884744 | tf_op jit(solution)/shard_map/ppermute | solution.py:480

commit v4 on v3

--- a/solution.py
+++ b/solution.py
@@ -16,7 +16,6 @@
 KD = 64
 VD = 128
 SP = ("z", "c")
-HIGHEST = lax.Precision.HIGHEST
 SWAP = [(0, 1), (1, 0)]
 
 NN = (((1,), (0,)), ((), ()))
@@ -28,8 +27,20 @@
     return lax.dot_general(a, b, dims, preferred_element_type=F32)
 
 
+def halves(a):
+    high = a.astype(BF)
+    return high, (a - high.astype(F32)).astype(BF)
+
+
 def exact(a, b, dims=NN):
-    return lax.dot_general(a, b, dims, precision=HIGHEST, preferred_element_type=F32)
+    if a.dtype == BF:
+        high, low = halves(b)
+        return mm(a, high, dims) + mm(a, low, dims)
+    high, low = halves(a)
+    if b.dtype == BF:
+        return mm(high, b, dims) + mm(low, b, dims)
+    other, rest = halves(b)
+    return mm(high, other, dims) + (mm(high, rest, dims) + mm(low, other, dims))
 
 
 def vmem():
@@ -148,30 +159,34 @@
             out[at : at + 2 * CAP, :] = inp_rows[part].astype(BF)
             out[at + 2 * CAP : at + 4 * CAP, :] = cot_rows[part].astype(BF)
     _, _, start, end, total = decay_parts(rate_ref[...])
-    keys, values = k_ref[...].astype(F32), v_ref[...].astype(F32)
+    keys, values = k_ref[...].astype(F32), v_ref[...]
     early = exact(keys * end, values, NTR)
     late = exact(keys * start, values, NTR)
     mine_ref[0:64, :] = early
     mine_ref[64:128, :] = late
-    mine_ref[128:136, :] = jnp.broadcast_to(total, (8, TOK))
+    mine_ref[128:136, :] = jnp.concatenate([total, start, end, jnp.zeros((5, TOK), F32)], axis=0)
     send_ref[768:832, :] = early.astype(BF)
     send_ref[832:896, :] = late.astype(BF)
     send_ref[896:904, :] = in_pieces(total)
     send_ref[904:912, :] = jnp.zeros((8, TOK), BF)
 
 
-def table_kernel(ids_in, rate_in, q_in, k_in, picks_ref, table_ref, ids_ref, rate_ref, q_ref, k_ref, sems):
-    fetch((ids_in, rate_in, q_in, k_in), (ids_ref, rate_ref, q_ref, k_ref), sems)
+def merge_kernel(keep_ref, got_ref, rows_ref, extra_ref):
+    for z in range(NZ):
+        part = slice(4 * CAP * z, 4 * CAP * (z + 1))
+        rows_ref[z] = keep_ref[part, :] + got_ref[part, :]
+    extra_ref[...] = got_ref[768:912, :]
+
+
+def picks_kernel(keep_in, ids_ref, picks_ref, keep_ref, sem):
+    copy = pltpu.make_async_copy(keep_in, keep_ref, sem)
+    copy.start()
     ek, rk, es, rs = rows_of(32, 5, 1, spot("c"))
     ids = ids_ref[...]
     for wanted, rank, at in ((ek, rk, 0), (es, rs, 512)):
         hit, _ = placement(ids, wanted, rank)
         picks_ref[at : at + 512, :] = jnp.where(hit, 1.0, 0.0).astype(BF)
-    col, row, start, end, _ = decay_parts(rate_ref[...])
-    mixed = KD ** (-0.5) * jnp.exp(-jnp.abs(col - row))
-    table_ref[0:128, :] = mixed
-    table_ref[128:256, :] = mm(q_ref[...], k_ref[...], TN) * mixed
-    table_ref[256:264, :] = jnp.concatenate([start, end, jnp.zeros((6, TOK), F32)], axis=0)
+    copy.wait()
 
 
 def expert_kernel(x_ref, gw_ref, uw_ref, dw_ref, part_ref, hid_ref, both_ref):
@@ -246,14 +261,14 @@
         out_ref[t] = resid
 
 
-def proj_kernel(r_ref, p_ref, mixer_ref, q_ref, table_ref, og_ref, keep_ref, send_ref, state_ref):
+def proj_kernel(r_ref, p_ref, mixer_ref, q_ref, mine_ref, og_ref, keep_ref, send_ref, state_ref):
     core = spot("c")
     resid = jnp.concatenate([r_ref[t] for t in range(NT)], axis=1)
     out_grad = mm(resid, p_ref[...])
     og_ref[...] = out_grad
     query = q_ref[...].astype(F32)
-    early = exact(query * table_ref[257:258, :], out_grad)
-    late = exact(query * table_ref[256:257, :], out_grad)
+    early = exact(query * mine_ref[130:131, :], out_grad)
+    late = exact(query * mine_ref[129:130, :], out_grad)
     state_ref[0] = early
     state_ref[1] = late
     send_ref[16] = early.astype(BF)
@@ -287,7 +302,7 @@
 
 
 def intra_kernel(
-    og_ref, table_ref, q_ref, k_ref, v_ref, own_ref, other_ref, extra_ref,
+    og_ref, rate_ref, q_ref, k_ref, v_ref, own_ref, other_ref, extra_ref,
     gq_ref, part_ref, weight_ref,
 ):
     place, core = spot("z"), spot("c")
@@ -322,20 +337,21 @@
     theirs = jnp.exp(-row_at(other, place))
     kv_early, kv_late = at_block(far_early, far_late, near, theirs)
     scale = KD ** (-0.5)
-    low = scale * table_ref[256:257, :]
-    high = scale * table_ref[257:258, :]
+    col, row, start, end, _ = decay_parts(rate_ref[...])
+    low, high = scale * start, scale * end
+    mixed = scale * jnp.exp(-jnp.abs(col - row))
     out_grad = og_ref[...]
-    query, key, value = [r[...].astype(F32) for r in (q_ref, k_ref, v_ref)]
-    score_grad = exact(out_grad, value) * table_ref[0:128, :]
+    query, key, value = q_ref[...], k_ref[...], v_ref[...]
+    score_grad = exact(out_grad, value) * mixed
     gq_ref[...] = (
         exact(key, score_grad, NTR)
         + low * exact(kv_early, out_grad, NTR)
         + high * exact(kv_late, out_grad, NTR)
     )
     part_ref[0:64, :] = exact(query, score_grad)
-    part_ref[64:192, :] = exact(out_grad, table_ref[128:256, :], TN)
-    part_ref[192:256, :] = key
-    part_ref[256:384, :] = value
+    part_ref[64:192, :] = exact(out_grad, mm(query, key, TN) * mixed, TN)
+    part_ref[192:256, :] = key.astype(F32)
+    part_ref[256:384, :] = value.astype(F32)
     part_ref[384:392, :] = jnp.concatenate([low, high, theirs, jnp.zeros((5, TOK), F32)], axis=0)
 
 
@@ -352,20 +368,21 @@
         out_ref[z, 64:96, :] = jnp.where(z > place, early, late)
 
 
-def gather_kernel(got_ref, weight_ref, proj_ref, state_ref):
-    share = jnp.zeros((64, COL), F32)
+def gather_kernel(got_ref, weight_ref, state_ref):
     early = late = jnp.zeros((32, COL), F32)
     for z in range(NZ):
-        share = share + got_ref[z, 0:64, :].astype(F32)
         state = got_ref[z, 64:96, :].astype(F32)
         early = early + state * weight_ref[z : z + 1, :]
         late = late + state * weight_ref[16 + z : 17 + z, :]
-    proj_ref[...] = share
     state_ref[0] = early
     state_ref[1] = late
 
 
-def final_kernel(far_ref, near_ref, part_ref, gk_ref, gv_ref):
+def final_kernel(far_ref, near_ref, part_ref, got_ref, proj_ref, gk_ref, gv_ref):
+    share = jnp.zeros((64, COL), F32)
+    for z in range(NZ):
+        share = share + got_ref[z, 0:64, :].astype(F32)
+    proj_ref[...] = share
     early, late = at_block(
         jnp.concatenate([far_ref[0, 0], far_ref[1, 0]], axis=0),
         jnp.concatenate([far_ref[0, 1], far_ref[1, 1]], axis=0),
@@ -373,7 +390,7 @@
         part_ref[386:387, :],
     )
     low, high = part_ref[384:385, :], part_ref[385:386, :]
-    key, value = part_ref[192:256, :], part_ref[256:384, :]
+    key, value = part_ref[192:256, :].astype(BF), part_ref[256:384, :].astype(BF)
     gk_ref[...] = part_ref[0:64, :] + low * exact(early, value) + high * exact(late, value)
     gv_ref[...] = part_ref[64:192, :] + low * exact(early, key, TN) + high * exact(late, key, TN)
 
@@ -421,22 +438,19 @@
             pltpu.VMEM((VD, TOK), BF), pltpu.SemaphoreType.DMA((8,)),
         ],
     )
-    picks, table = call(
-        table_kernel,
-        [arr((1024, TOK), BF), arr((264, TOK), F32)],
-        (ids, decay_rates, queries, key_vectors),
-        "table",
-        60,
-        stay=4,
-        scratch=[
-            pltpu.VMEM((2, TOK), jnp.int32), pltpu.VMEM((1, TOK), F32), pltpu.VMEM((KD, TOK), BF),
-            pltpu.VMEM((KD, TOK), BF), pltpu.SemaphoreType.DMA((4,)),
-        ],
+    picks, keep = call(
+        picks_kernel,
+        [arr((1024, TOK), BF), arr((768, COL), BF)],
+        (keep, ids),
+        "picks",
+        stay=1,
+        scratch=[pltpu.SemaphoreType.DMA(())],
     )
     swapped = lax.ppermute(send, "c", SWAP)
-    extra = swapped[768:]
-    rows = (keep + swapped[:768]).reshape(NZ, 4 * CAP, COL)
-    rows, picks, table, extra = lax.optimization_barrier((rows, picks, table, extra))
+    rows, extra = call(
+        merge_kernel, [arr((NZ, 4 * CAP, COL), BF), arr((144, COL), BF)], (keep, swapped), "merge"
+    )
+    rows, picks, extra = lax.optimization_barrier((rows, picks, extra))
     rows = exchange(rows, "z")
     rows = rows.reshape(NZ, 2, 2 * CAP, COL).transpose(1, 0, 2, 3).reshape(2, NZ * 2 * CAP, COL)
     rows = to_all(rows, ("c", "tp"), groups(4, 1, 1, 4))
@@ -473,7 +487,7 @@
             arr((TOK, VD), F32), arr((NZ, 64, COL), F32), arr((18, 64, COL), BF),
             arr((2, KD, VD), F32),
         ],
-        (resid, proj_weight, mixer_out, queries, table),
+        (resid, proj_weight, mixer_out, queries, mine),
         "proj",
         8,
     )
@@ -481,7 +495,7 @@
     grad_queries, part, weight = call(
         intra_kernel,
         [arr((KD, TOK), F32), arr((392, TOK), F32), arr((32, TOK), F32)],
-        (out_grad, table, queries, key_vectors, value_vectors, own, other, extra),
+        (out_grad, decay_rates, queries, key_vectors, value_vectors, own, other, extra),
         "intra",
     )
     chip, near = call(
@@ -492,17 +506,12 @@
     )
     chip, grad_queries, part, weight = lax.optimization_barrier((chip, grad_queries, part, weight))
     chip = exchange(chip, "z")
-    grad_proj, far = call(
-        gather_kernel,
-        [arr((64, COL), F32), arr((2, 32, COL), F32)],
-        (chip, weight),
-        "gather",
-    )
+    far = call(gather_kernel, arr((2, 32, COL), F32), (chip, weight), "gather")
     far = lax.all_gather(far, "c")
-    grad_keys, grad_values = call(
+    grad_proj, grad_keys, grad_values = call(
         final_kernel,
-        [arr((KD, TOK), F32), arr((VD, TOK), F32)],
-        (far, near, part),
+        [arr((64, COL), F32), arr((KD, TOK), F32), arr((VD, TOK), F32)],
+        (far, near, part, chip),
         "final",
     )
     return (

time: 185 us -> 183 us (0.989)
  Pallas kernels: 12.2 us -> 9.82 us
    pallas_call x11 -> x12, Pallas kernels: 12.2 us -> 9.82 us  [call(): pl.pallas_call(kernel, out_shape=outs, in_specs=[hbm()] * stay + [vmem()]...]
  transfers between devices with their start and end apart: 3 -> 3, of which waited for: 0 -> 0; matrix products, arithmetic and copies ran while one was open for 0% -> 0% of each run, Pallas kernels for 3% -> 2%
where the time goes in v4:
time: 183 us
  blocking collectives  147 us (80%)
  starting transfers between devices  22.5 us (12%)
  Pallas kernels  9.82 us (5%)
  local copies, waits for them, and re-layouts  2.49 us (1%)
    all_to_all x5, blocking collectives, exchange(): return lax.all_to_all(blocks, axis, split_axis=0, concat_axis=0, tiled=True)  101 us
    all_to_all x2, blocking collectives, to_all(): lax.all_to_all(copies, axis, split_axis=0, concat_axis=0, axis_index_grou...  37.6 us
    ppermute x1, starting transfers between devices, on_device(): other = lax.ppermute(own, 'c', SWAP)  10.7 us
    pallas_call x12, Pallas kernels, call(): pl.pallas_call(kernel, out_shape=outs, in_specs=[hbm()] * stay + [vmem()]...  9.82 us
    all_gather x1, blocking collectives, on_device(): far = lax.all_gather(far, 'c')  8.94 us
    ppermute x1, starting transfers between devices, on_device(): swapped = lax.ppermute(send, 'c', SWAP)  8.75 us
  transfers between devices with their start and end apart: 3, of which 0 were waited for; matrix products, arithmetic and copies ran while one was open for 0% of the time, Pallas kernels for 2%

profile of v4, /device:TPU:1, one launch (start us, length us, event | category | flops | bytes accessed | tf_op | source)
XLA Modules:
  0.0 182.7 jit_solution(5149735816203387127)
XLA Ops:
  0.6 2.3 %pack.1 = (bf16[768,128]{1,0:T(8,128)(2,1)}, bf16[912,128]{1,0:T(8,128)(2,1)}, bf16[128,128]{1,0:T(8,128)(2,1)}, f32[136,128]{1,0:T(8,128)}) custom-call(s32[2,128]{1,0:T(2,128)} %bitcast.21, f32[1,128]{1,0:T(1,128)} %bitcast.26, f32[2,128]{1,0:T(2,128)} %bitcast.25, bf16[128,2048]{1,0:T(8,128)(2,1)} %cot_in.1, bf16[128,2048]{1,0:T(8,128)(2,1)} %inp_in.1, ...), custom_call_target="tpu_custom_call" | custom-call | flops 134217728 | bytes 1048576 | tf_op jit(solution)/shard_map/pack/pallas_call | solution.py:55
  2.9 8.7 %collective-permute-start = (bf16[912,128]{1,0:T(8,128)(2,1)}, bf16[912,128]{1,0:T(8,128)(2,1)S(1)}, u32[]{:S(2)}, u32[]{:S(2)}) collective-permute-start(bf16[912,128]{1,0:T(8,128)(2,1)} %get-tuple-element.50), channel_id=1, source_target_pairs={{0,16},{16,0},{1,17},{17,1},{2,18},{18,2},{3,19},{19,3},{4,20},{20... | collective-permute-start | bytes 700424 | tf_op jit(solution)/shard_map/ppermute | solution.py:449
  11.7 0.0 copy-start.11
  11.7 0.7 copy-done.11
  12.4 0.0 copy-start.12
  12.4 0.9 copy-done.12
  13.3 0.5 picks.1
  13.9 0.0 collective-permute-done.got_ref
  13.9 22.6 %all_to_all.35 = bf16[16,48,128]{2,1,0:T(8,128)(2,1)S(1)} all-to-all(bf16[16,48,128]{2,1,0:T(8,128)(2,1)S(1)} %get-tuple-element.55), channel_id=1, replica_groups=mesh['z'=16,'c'=2,'tp'=16] {'z'}, dimensions={0} | all-to-all | bytes 393216 | tf_op jit(solution)/shard_map/all_to_all | solution.py:412
  36.6 0.1 broadcast_in_dim.15
  36.7 12.2 %all_to_all.36 = bf16[4,2,384,128]{3,2,1,0:T(8,128)(2,1)S(1)} all-to-all(bf16[4,2,384,128]{3,2,1,0:T(8,128)(2,1)S(1)} %broadcast_in_dim.15), channel_id=1, replica_groups={{0,4,8,12},{1,5,9,13},{2,6,10,14},{3,7,11,15},{16,17,18,19},{20,21,22,2..., dimensions={0} | all-to-all | bytes 1572864 | tf_op jit(solution)/shard_map/all_to_all | solution.py:406
  48.8 0.7 broadcast_in_dim.16
  49.5 0.0 copy-start
  49.5 0.0 copy-start.1
  49.6 0.0 copy-start.2
  49.6 25.4 %all_to_all.37 = bf16[4,4,2,384,128]{4,3,2,1,0:T(8,128)(2,1)S(1)} all-to-all(bf16[4,4,2,384,128]{4,3,2,1,0:T(8,128)(2,1)S(1)} %broadcast_in_dim.16), channel_id=1, replica_groups={{0,1,2,3},{4,5,6,7},{8,9,10,11},{12,13,14,15},{16,20,24,28},{17,21,25,2..., dimensions={0} | all-to-all | bytes 6291456 | tf_op jit(solution)/shard_map/all_to_all | solution.py:406
  75.0 0.0 copy-done
  75.0 0.0 copy-done.1
  75.0 0.0 copy-done.2
  75.0 0.0 copy-start.4
  75.0 1.4 expert.1
  76.5 20.1 %all_to_all.38.part_ref = bf16[16,384,128]{2,1,0:T(8,128)(2,1)S(1)} all-to-all(bf16[16,384,128]{2,1,0:T(8,128)(2,1)S(1)} %get-tuple-element.56), channel_id=1, replica_groups=mesh['z'=16,'c'=2,'tp'=16] {'tp'}, dimensions={0} | all-to-all | bytes 3145728 | tf_op jit(solution)/shard_map/all_to_all | solution.py:412
  96.5 0.0 copy-start.9
  96.5 0.0 copy-done.4
  96.6 0.2 sums.1
  96.8 0.0 copy-start.3
  96.8 0.0 copy-start.7
  96.8 0.0 copy-start.8
  96.8 22.6 %all_to_all.39.own_ref = bf16[16,64,128]{2,1,0:T(8,128)(2,1)S(1)} all-to-all(bf16[16,64,128]{2,1,0:T(8,128)(2,1)S(1)} %sums.1), channel_id=1, replica_groups=mesh['z'=16,'c'=2,'tp'=16] {'z'}, dimensions={0} | all-to-all | bytes 524288 | tf_op jit(solution)/shard_map/all_to_all | solution.py:412
  119.4 0.0 copy-start.5
  119.4 0.0 copy-start.6
  119.4 0.0 copy-start.10
  119.4 10.7 %collective-permute-start.1 = (bf16[16,64,128]{2,1,0:T(8,128)(2,1)S(1)}, bf16[16,64,128]{2,1,0:T(8,128)(2,1)S(1)}, u32[]{:S(2)}, u32[]{:S(2)}) collective-permute-start(bf16[16,64,128]{2,1,0:T(8,128)(2,1)S(1)} %all_to_all.39.own_ref), channel_id=1, source_target_pairs={{0,16},{16,0},{1,17},{17,1},{2,18},{18,2},{3,19},{19,3},{4,20},{20... | collective-permute-start | bytes 786440 | tf_op jit(solution)/shard_map/ppermute | solution.py:470
  130.1 2.2 %weights.1 = (bf16[2048,128]{1,0:T(8,128)(2,1)}, bf16[2048,128]{1,0:T(8,128)(2,1)}, bf16[128,2048]{1,0:T(8,128)(2,1)}) custom-call(bf16[16,2,384,128]{3,2,1,0:T(8,128)(2,1)S(1)} %bitcast.16, bf16[384,128]{1,0:T(8,128)(2,1)S(1)} %get-tuple-element.64.hid_ref, bf16[384,256]{1,0:T(8,128)(2,1)S(1)} %get-tuple-element.65.both_ref), custom_call_target="tpu_custom_call" | custom-call | flops 536870912 | bytes 1048576 | tf_op jit(solution)/shard_map/weights/pallas_call | solution.py:55
  132.3 0.0 collective-permute-done.1.other_ref
  132.3 0.0 copy-done.9
  132.3 0.3 resid.1
  132.6 13.9 %all_to_all.40.r_ref = bf16[16,128,128]{2,1,0:T(8,128)(2,1)S(1)} all-to-all(bf16[16,128,128]{2,1,0:T(8,128)(2,1)S(1)} %resid.1), channel_id=1, replica_groups=mesh['z'=16,'c'=2,'tp'=16] {'tp'}, dimensions={0} | all-to-all | bytes 1048576 | tf_op jit(solution)/shard_map/all_to_all | solution.py:412
  146.5 0.0 copy-done.3
  146.5 0.0 copy-done.7
  146.5 0.0 copy-done.8
  146.5 0.6 proj.1
  147.1 3.1 %collective-permute-start.2 = (bf16[18,64,128]{2,1,0:T(8,128)(2,1)S(1)}, bf16[18,64,128]{2,1,0:T(8,128)(2,1)S(1)}, u32[]{:S(2)}, u32[]{:S(2)}) collective-permute-start(bf16[18,64,128]{2,1,0:T(8,128)(2,1)S(1)} %get-tuple-element.74), channel_id=1, source_target_pairs={{0,16},{16,0},{1,17},{17,1},{2,18},{18,2},{3,19},{19,3},{4,20},{20... | collective-permute-start | bytes 884744 | tf_op jit(solution)/shard_map/ppermute | solution.py:494
  150.2 0.0 copy-done.5
  150.2 0.0 copy-done.6
  150.3 0.0 copy-done.10
  150.3 1.1 intra.1
  151.4 0.0 collective-permute-done.2.got_ref
  151.4 0.1 chip.1
  151.5 21.3 %all_to_all.41.got_ref = bf16[16,96,128]{2,1,0:T(8,128)(2,1)S(1)} all-to-all(bf16[16,96,128]{2,1,0:T(8,128)(2,1)S(1)} %get-tuple-element.81), channel_id=1, replica_groups=mesh['z'=16,'c'=2,'tp'=16] {'z'}, dimensions={0} | all-to-all | bytes 786432 | tf_op jit(solution)/shard_map/all_to_all | solution.py:412
  172.8 0.1 gather.1
  172.9 8.9 %all-gather = f32[4,32,128]{2,1,0:T(8,128)S(1)} all-gather(f32[2,32,128]{2,1,0:T(8,128)S(1)} %gather.1), channel_id=2, replica_groups=mesh['z'=16,'c'=2,'tp'=16] {'c'}, dimensions={0}, use_global_device_ids=true | all-gather | bytes 98304 | tf_op jit(solution)/shard_map/all_gather | solution.py:510
  181.8 0.9 final.1
  (2 shorter events, 0.1 us)
Async XLA Ops:
  2.9 10.9 %collective-permute-start = (bf16[912,128]{1,0:T(8,128)(2,1)}, bf16[912,128]{1,0:T(8,128)(2,1)S(1)}, u32[]{:S(2)}, u32[]{:S(2)}) collective-permute-start(bf16[912,128]{1,0:T(8,128)(2,1)} %get-tuple-element.50), channel_id=1, source_target_pairs={{0,16},{16,0},{1,17},{17,1},{2,18},{18,2},{3,19},{19,3},{4,20},{20... | collective-permute-start | bytes 700424 | tf_op jit(solution)/shard_map/ppermute | solution.py:449
  11.7 0.7 copy-start.11
  12.4 0.9 copy-start.12
  49.5 25.5 %copy-start = (bf16[1,2048,128]{2,1,0:T(8,128)(2,1)S(1)}, bf16[1,2048,128]{2,1,0:T(8,128)(2,1)}, u32[]{:S(2)}) copy-start(bf16[1,2048,128]{2,1,0:T(8,128)(2,1)} %param.25) | copy-start | bytes 1572868
  49.5 25.5 %copy-start.1 = (bf16[1,2048,128]{2,1,0:T(8,128)(2,1)S(1)}, bf16[1,2048,128]{2,1,0:T(8,128)(2,1)}, u32[]{:S(2)}) copy-start(bf16[1,2048,128]{2,1,0:T(8,128)(2,1)} %param.26) | copy-start | bytes 1572868
  49.6 25.5 %copy-start.2 = (bf16[1,128,2048]{2,1,0:T(8,128)(2,1)S(1)}, bf16[1,128,2048]{2,1,0:T(8,128)(2,1)}, u32[]{:S(2)}) copy-start(bf16[1,128,2048]{2,1,0:T(8,128)(2,1)} %param.27) | copy-start | bytes 1572868
  75.0 21.5 %copy-start.4 = (f32[136,128]{1,0:T(8,128)S(1)}, f32[136,128]{1,0:T(8,128)}, u32[]{:S(2)}) copy-start(f32[136,128]{1,0:T(8,128)} %get-tuple-element.57.mine_ref) | copy-start | bytes 208900
  96.5 35.7 %copy-start.9 = (bf16[128,128]{1,0:T(8,128)(2,1)S(1)}, bf16[128,128]{1,0:T(8,128)(2,1)}, u32[]{:S(2)}) copy-start(bf16[128,128]{1,0:T(8,128)(2,1)} %get-tuple-element.62.cols_ref) | copy-start | bytes 98308
  96.8 49.7 %copy-start.3 = (bf16[2048,128]{1,0:T(8,128)(2,1)S(1)}, bf16[2048,128]{1,0:T(8,128)(2,1)}, u32[]{:S(2)}) copy-start(bf16[2048,128]{1,0:T(8,128)(2,1)} %p_ref.1) | copy-start | bytes 1572868
  96.8 49.7 %copy-start.7 = (bf16[64,128]{1,0:T(8,128)(2,1)S(1)}, bf16[64,128]{1,0:T(8,128)(2,1)}, u32[]{:S(2)}) copy-start(bf16[64,128]{1,0:T(8,128)(2,1)} %q_ref.3) | copy-start | bytes 49156
  96.8 49.7 %copy-start.8 = (bf16[128,128]{1,0:T(8,128)(2,1)S(1)}, bf16[128,128]{1,0:T(8,128)(2,1)}, u32[]{:S(2)}) copy-start(bf16[128,128]{1,0:T(8,128)(2,1)} %mixer_ref.1) | copy-start | bytes 98308
  119.4 30.8 %copy-start.5 = (bf16[128,128]{1,0:T(8,128)(2,1)S(1)}, bf16[128,128]{1,0:T(8,128)(2,1)}, u32[]{:S(2)}) copy-start(bf16[128,128]{1,0:T(8,128)(2,1)} %v_ref.1) | copy-start | bytes 98308
  119.4 30.8 %copy-start.6 = (bf16[64,128]{1,0:T(8,128)(2,1)S(1)}, bf16[64,128]{1,0:T(8,128)(2,1)}, u32[]{:S(2)}) copy-start(bf16[64,128]{1,0:T(8,128)(2,1)} %k_ref.1) | copy-start | bytes 49156
  119.4 30.9 %copy-start.10 = (f32[1,128]{1,0:T(1,128)S(1)}, f32[1,128]{1,0:T(1,128)}, u32[]{:S(2)}) copy-start(f32[1,128]{1,0:T(1,128)} %rate_ref.1) | copy-start | bytes 1540
  119.4 12.9 %collective-permute-start.1 = (bf16[16,64,128]{2,1,0:T(8,128)(2,1)S(1)}, bf16[16,64,128]{2,1,0:T(8,128)(2,1)S(1)}, u32[]{:S(2)}, u32[]{:S(2)}) collective-permute-start(bf16[16,64,128]{2,1,0:T(8,128)(2,1)S(1)} %all_to_all.39.own_ref), channel_id=1, source_target_pairs={{0,16},{16,0},{1,17},{17,1},{2,18},{18,2},{3,19},{19,3},{4,20},{20... | collective-permute-start | bytes 786440 | tf_op jit(solution)/shard_map/ppermute | solution.py:470
  147.1 4.3 %collective-permute-start.2 = (bf16[18,64,128]{2,1,0:T(8,128)(2,1)S(1)}, bf16[18,64,128]{2,1,0:T(8,128)(2,1)S(1)}, u32[]{:S(2)}, u32[]{:S(2)}) collective-permute-start(bf16[18,64,128]{2,1,0:T(8,128)(2,1)S(1)} %get-tuple-element.74), channel_id=1, source_target_pairs={{0,16},{16,0},{1,17},{17,1},{2,18},{18,2},{3,19},{19,3},{4,20},{20... | collective-permute-start | bytes 884744 | tf_op jit(solution)/shard_map/ppermute | solution.py:494

commit v5 on v4

--- a/solution.py
+++ b/solution.py
@@ -162,31 +162,55 @@
     keys, values = k_ref[...].astype(F32), v_ref[...]
     early = exact(keys * end, values, NTR)
     late = exact(keys * start, values, NTR)
-    mine_ref[0:64, :] = early
-    mine_ref[64:128, :] = late
-    mine_ref[128:136, :] = jnp.concatenate([total, start, end, jnp.zeros((5, TOK), F32)], axis=0)
-    send_ref[768:832, :] = early.astype(BF)
-    send_ref[832:896, :] = late.astype(BF)
-    send_ref[896:904, :] = in_pieces(total)
-    send_ref[904:912, :] = jnp.zeros((8, TOK), BF)
+    mine_ref[...] = jnp.concatenate([total, start, end, jnp.zeros((5, TOK), F32)], axis=0)
+    for out in (keep_ref, send_ref):
+        out[768:832, :] = early.astype(BF)
+        out[832:896, :] = late.astype(BF)
+        out[896:904, :] = in_pieces(total)
+        out[904:912, :] = jnp.concatenate(
+            [ids.astype(F32), jnp.zeros((6, TOK), F32)], axis=0
+        ).astype(BF)
+
+
+def in_one(pieces):
+    pieces = pieces.astype(F32)
+    return pieces[0:1, :] + pieces[1:2, :] + pieces[2:3, :]
 
 
 def merge_kernel(keep_ref, got_ref, rows_ref, extra_ref):
+    extra_ref[...] = got_ref[768:912, :]
+    early, late = chip_states(
+        *[
+            ref[at : at + 64, :].astype(F32)
+            for ref in (keep_ref, got_ref)
+            for at in (768, 832)
+        ],
+        jnp.exp(-in_one(keep_ref[896:904, :])),
+        jnp.exp(-in_one(got_ref[896:904, :])),
+    )
+    place = spot("z")
     for z in range(NZ):
         part = slice(4 * CAP * z, 4 * CAP * (z + 1))
-        rows_ref[z] = keep_ref[part, :] + got_ref[part, :]
-    extra_ref[...] = got_ref[768:912, :]
-
-
-def picks_kernel(keep_in, ids_ref, picks_ref, keep_ref, sem):
-    copy = pltpu.make_async_copy(keep_in, keep_ref, sem)
-    copy.start()
+        rows_ref[z, 0 : 4 * CAP, :] = keep_ref[part, :] + got_ref[part, :]
+        rows_ref[z, 48:80, :] = jnp.where(z > place, early, late)
+        rows_ref[z, 80:88, :] = keep_ref[896:904, :]
+
+
+def picks_kernel(keep_ref, picks_ref):
     ek, rk, es, rs = rows_of(32, 5, 1, spot("c"))
-    ids = ids_ref[...]
+    ids = keep_ref[904:912, :].astype(F32).astype(jnp.int32)
     for wanted, rank, at in ((ek, rk, 0), (es, rs, 512)):
         hit, _ = placement(ids, wanted, rank)
         picks_ref[at : at + 512, :] = jnp.where(hit, 1.0, 0.0).astype(BF)
-    copy.wait()
+
+
+def spread_kernel(got_ref, rows_ref, states_ref):
+    states_ref[...] = got_ref[:, 48:88, :]
+    for z in range(NZ):
+        for kind in range(2):
+            part = got_ref[z, 24 * kind : 24 * (kind + 1), :]
+            for k in range(4):
+                rows_ref[k, kind, 24 * z : 24 * (z + 1), :] = part
 
 
 def expert_kernel(x_ref, gw_ref, uw_ref, dw_ref, part_ref, hid_ref, both_ref):
@@ -233,23 +257,11 @@
     return [jnp.where(is_first, a[:32], a[32:]).astype(BF) for a in (both_early, both_late)]
 
 
-def sum_kernel(part_ref, mine_ref, extra_ref, out_ref):
+def sum_kernel(part_ref, out_ref):
     total = part_ref[0].astype(F32)
     for t in range(1, NT):
         total = total + part_ref[t].astype(F32)
-    out_ref[:, 0 : 2 * CAP, :] = total.reshape(NZ, 2 * CAP, COL).astype(BF)
-    decay = mine_ref[128:129, :]
-    out_ref[:, 2 * CAP : 32, :] = jnp.broadcast_to(in_pieces(decay)[None], (NZ, 8, COL))
-    pieces = extra_ref[128:136, :].astype(F32)
-    theirs = pieces[0:1, :] + pieces[1:2, :] + pieces[2:3, :]
-    early, late = chip_states(
-        mine_ref[0:64, :], mine_ref[64:128, :],
-        extra_ref[0:64, :].astype(F32), extra_ref[64:128, :].astype(F32),
-        jnp.exp(-decay), jnp.exp(-theirs),
-    )
-    place = spot("z")
-    for z in range(NZ):
-        out_ref[z, 32:64, :] = jnp.where(z > place, early, late)
+    out_ref[...] = total.reshape(NZ, 2 * CAP, COL).astype(BF)
 
 
 def resid_kernel(picks_ref, own_ref, other_ref, cols_ref, out_ref):
@@ -267,8 +279,8 @@
     out_grad = mm(resid, p_ref[...])
     og_ref[...] = out_grad
     query = q_ref[...].astype(F32)
-    early = exact(query * mine_ref[130:131, :], out_grad)
-    late = exact(query * mine_ref[129:130, :], out_grad)
+    early = exact(query * mine_ref[2:3, :], out_grad)
+    late = exact(query * mine_ref[1:2, :], out_grad)
     state_ref[0] = early
     state_ref[1] = late
     send_ref[16] = early.astype(BF)
@@ -283,7 +295,7 @@
 
 def decays(own_ref, other_ref):
     def total(ref):
-        rows = ref[:, 2 * CAP : 32, :].astype(F32)
+        rows = ref[:, 56:64, :].astype(F32)
         return rows[:, 0, :] + rows[:, 1, :] + rows[:, 2, :]
 
     return total(own_ref), total(other_ref)
@@ -322,7 +334,7 @@
     def far(ref):
         early = late = jnp.zeros((32, COL), F32)
         for z in range(NZ):
-            state = ref[z, 32:64, :].astype(F32)
+            state = ref[z, 24:56, :].astype(F32)
             early = early + state * early_w[z : z + 1, :]
             late = late + state * late_w[z : z + 1, :]
         return early, late
@@ -401,11 +413,14 @@
     return first + second
 
 
+def within(blocks, axis, sets):
+    return lax.all_to_all(
+        blocks, axis, split_axis=0, concat_axis=0, axis_index_groups=sets, tiled=True
+    )
+
+
 def to_all(shard, axis, sets):
-    copies = jnp.broadcast_to(shard, (len(sets[0]), *shard.shape))
-    return lax.all_to_all(
-        copies, axis, split_axis=0, concat_axis=0, axis_index_groups=sets, tiled=True
-    )
+    return within(jnp.broadcast_to(shard, (len(sets[0]), *shard.shape)), axis, sets)
 
 
 def exchange(blocks, axis):
@@ -424,7 +439,7 @@
     ids = expert_ids.T
     keep, send, cols, mine = call(
         pack_kernel,
-        [arr((768, COL), BF), arr((912, COL), BF), arr((TOK, COL), BF), arr((136, TOK), F32)],
+        [arr((912, COL), BF), arr((912, COL), BF), arr((TOK, COL), BF), arr((8, TOK), F32)],
         (
             ids, group_weight.reshape(1, TOK), expert_weight.T, cotangent, moe_input,
             decay_rates, key_vectors, value_vectors,
@@ -438,23 +453,24 @@
             pltpu.VMEM((VD, TOK), BF), pltpu.SemaphoreType.DMA((8,)),
         ],
     )
-    picks, keep = call(
-        picks_kernel,
-        [arr((1024, TOK), BF), arr((768, COL), BF)],
-        (keep, ids),
-        "picks",
-        stay=1,
-        scratch=[pltpu.SemaphoreType.DMA(())],
-    )
+    picks = call(picks_kernel, arr((1024, TOK), BF), (keep,), "picks")
     swapped = lax.ppermute(send, "c", SWAP)
     rows, extra = call(
-        merge_kernel, [arr((NZ, 4 * CAP, COL), BF), arr((144, COL), BF)], (keep, swapped), "merge"
+        merge_kernel,
+        [arr((NZ, 88, COL), BF), arr((144, COL), BF)],
+        (keep, swapped),
+        "merge",
     )
     rows, picks, extra = lax.optimization_barrier((rows, picks, extra))
     rows = exchange(rows, "z")
-    rows = rows.reshape(NZ, 2, 2 * CAP, COL).transpose(1, 0, 2, 3).reshape(2, NZ * 2 * CAP, COL)
-    rows = to_all(rows, ("c", "tp"), groups(4, 1, 1, 4))
-    rows = to_all(rows, ("c", "tp"), groups(1, 4, 4, 1))
+    copies, states = call(
+        spread_kernel,
+        [arr((4, 2, NZ * 2 * CAP, COL), BF), arr((NZ, 40, COL), BF)],
+        (rows,),
+        "spread",
+    )
+    rows = within(copies, ("c", "tp"), groups(4, 1, 1, 4))
+    rows = to_all(rows.reshape(4, 2, NZ * 2 * CAP, COL), ("c", "tp"), groups(1, 4, 4, 1))
     rows = rows.reshape(NT, 2, NZ * 2 * CAP, COL)
     shares, hidden, both = call(
         expert_kernel,
@@ -464,8 +480,8 @@
         20,
     )
     shares = exchange(shares, "tp")
-    back = call(sum_kernel, arr((NZ, 64, COL), BF), (shares, mine, extra), "sums", 6)
-    own = exchange(back, "z")
+    back = call(sum_kernel, arr((NZ, 2 * CAP, COL), BF), (shares,), "sums", 6)
+    own = jnp.concatenate([exchange(back, "z"), states], axis=1)
     own, rows, hidden, both = lax.optimization_barrier((own, rows, hidden, both))
     other = lax.ppermute(own, "c", SWAP)
     grad_gate, grad_up, grad_down = call(

time: 183 us -> 185 us (1.011)
  blocking collectives: 147 us -> 152 us
  starting transfers between devices: 22.5 us -> 20.1 us
    all_to_all x5, blocking collectives: 101 us -> 105 us  [exchange(): return lax.all_to_all(blocks, axis, split_axis=0, concat_axis=0, tiled=True)]
    ppermute x1, starting transfers between devices: 10.7 us -> 8.02 us  [on_device(): other = lax.ppermute(own, 'c', SWAP)]
    pallas_call x12 -> x13, Pallas kernels: 9.82 us -> 9.75 us  [call(): pl.pallas_call(kernel, out_shape=outs, in_specs=[hbm()] * stay + [vmem()]...]
where the time goes in v5:
time: 185 us; the launch traced here: 184 us
  blocking collectives  152 us (82%)
  starting transfers between devices  20.1 us (11%)
  Pallas kernels  9.75 us (5%)
    all_to_all x5, blocking collectives, exchange(): return lax.all_to_all(blocks, axis, split_axis=0, concat_axis=0, tiled=True)  105 us
    all_to_all x2, blocking collectives, within(): lax.all_to_all(blocks, axis, split_axis=0, concat_axis=0, axis_index_grou...  37.5 us
    pallas_call x13, Pallas kernels, call(): pl.pallas_call(kernel, out_shape=outs, in_specs=[hbm()] * stay + [vmem()]...  9.75 us
    all_gather x1, blocking collectives, on_device(): far = lax.all_gather(far, 'c')  8.94 us
    ppermute x1, starting transfers between devices, on_device(): swapped = lax.ppermute(send, 'c', SWAP)  8.75 us
    ppermute x1, starting transfers between devices, on_device(): other = lax.ppermute(own, 'c', SWAP)  8.02 us
  transfers between devices with their start and end apart: 3, of which 0 were waited for; matrix products, arithmetic and copies ran while one was open for 0% of the time, Pallas kernels for 2%

profile of v5, /device:TPU:1, one launch (start us, length us, event | category | flops | bytes accessed | tf_op | source)
XLA Modules:
  0.0 184.4 jit_solution(5365424375887285582)
XLA Ops:
  0.6 2.3 %pack.1 = (bf16[912,128]{1,0:T(8,128)(2,1)}, bf16[912,128]{1,0:T(8,128)(2,1)}, bf16[128,128]{1,0:T(8,128)(2,1)}, f32[8,128]{1,0:T(8,128)}) custom-call(s32[2,128]{1,0:T(2,128)} %bitcast.17, f32[1,128]{1,0:T(1,128)} %bitcast.19, f32[2,128]{1,0:T(2,128)} %bitcast.18, bf16[128,2048]{1,0:T(8,128)(2,1)} %cot_in.1, bf16[128,2048]{1,0:T(8,128)(2,1)} %inp_in.1, ...), custom_call_target="tpu_custom_call" | custom-call | flops 134217728 | bytes 1048576 | tf_op jit(solution)/shard_map/pack/pallas_call | solution.py:55
  3.0 8.7 %collective-permute-start = (bf16[912,128]{1,0:T(8,128)(2,1)}, bf16[912,128]{1,0:T(8,128)(2,1)S(1)}, u32[]{:S(2)}, u32[]{:S(2)}) collective-permute-start(bf16[912,128]{1,0:T(8,128)(2,1)} %get-tuple-element.49), channel_id=1, source_target_pairs={{0,16},{16,0},{1,17},{17,1},{2,18},{18,2},{3,19},{19,3},{4,20},{20... | collective-permute-start | bytes 700424 | tf_op jit(solution)/shard_map/ppermute | solution.py:457
  11.7 0.0 copy-start.11
  11.8 0.9 copy-done.11
  12.7 0.3 picks.1.picks_ref
  13.0 0.0 collective-permute-done.got_ref
  13.0 0.1 merge.1
  13.1 25.5 %all_to_all.35.got_ref = bf16[16,88,128]{2,1,0:T(8,128)(2,1)S(1)} all-to-all(bf16[16,88,128]{2,1,0:T(8,128)(2,1)S(1)} %get-tuple-element.53), channel_id=1, replica_groups=mesh['z'=16,'c'=2,'tp'=16] {'z'}, dimensions={0} | all-to-all | bytes 720896 | tf_op jit(solution)/shard_map/all_to_all | solution.py:427
  38.6 0.1 spread.1
  38.7 12.2 %all_to_all.36 = bf16[4,2,384,128]{3,2,1,0:T(8,128)(2,1)S(1)} all-to-all(bf16[4,2,384,128]{3,2,1,0:T(8,128)(2,1)S(1)} %get-tuple-element.54), channel_id=1, replica_groups={{0,4,8,12},{1,5,9,13},{2,6,10,14},{3,7,11,15},{16,17,18,19},{20,21,22,2..., dimensions={0} | all-to-all | bytes 1572864 | tf_op jit(solution)/shard_map/all_to_all | solution.py:417
  50.9 0.7 broadcast_in_dim.12
  51.6 0.0 copy-start
  51.6 0.0 copy-start.1
  51.6 0.0 copy-start.2
  51.6 25.4 %all_to_all.37 = bf16[4,4,2,384,128]{4,3,2,1,0:T(8,128)(2,1)S(1)} all-to-all(bf16[4,4,2,384,128]{4,3,2,1,0:T(8,128)(2,1)S(1)} %broadcast_in_dim.12), channel_id=1, replica_groups={{0,1,2,3},{4,5,6,7},{8,9,10,11},{12,13,14,15},{16,20,24,28},{17,21,25,2..., dimensions={0} | all-to-all | bytes 6291456 | tf_op jit(solution)/shard_map/all_to_all | solution.py:417
  77.0 0.0 copy-done
  77.0 0.0 copy-done.1
  77.0 0.0 copy-done.2
  77.0 1.4 expert.1
  78.4 18.9 %all_to_all.38.part_ref = bf16[16,384,128]{2,1,0:T(8,128)(2,1)S(1)} all-to-all(bf16[16,384,128]{2,1,0:T(8,128)(2,1)S(1)} %get-tuple-element.55), channel_id=1, replica_groups=mesh['z'=16,'c'=2,'tp'=16] {'tp'}, dimensions={0} | all-to-all | bytes 3145728 | tf_op jit(solution)/shard_map/all_to_all | solution.py:427
  97.3 0.0 copy-start.8
  97.3 0.2 sums.1
  97.5 27.0 %all_to_all.39 = bf16[16,24,128]{2,1,0:T(8,128)(2,1)S(1)} all-to-all(bf16[16,24,128]{2,1,0:T(8,128)(2,1)S(1)} %sums.1), channel_id=1, replica_groups=mesh['z'=16,'c'=2,'tp'=16] {'z'}, dimensions={0} | all-to-all | bytes 196608 | tf_op jit(solution)/shard_map/all_to_all | solution.py:427
  124.5 0.0 copy-start.3
  124.5 0.0 copy-start.6
  124.5 0.0 copy-start.7
  124.5 0.0 copy-start.9
  124.6 0.0 copy-start.4
  124.6 0.0 copy-start.5
  124.6 0.0 copy-start.10
  124.6 8.0 %collective-permute-start.1 = (bf16[16,64,128]{2,1,0:T(8,128)(2,1)S(1)}, bf16[16,64,128]{2,1,0:T(8,128)(2,1)S(1)}, u32[]{:S(2)}, u32[]{:S(2)}) collective-permute-start(bf16[16,64,128]{2,1,0:T(8,128)(2,1)S(1)} %pad_maximum_fusion.own_ref), channel_id=1, source_target_pairs={{0,16},{16,0},{1,17},{17,1},{2,18},{18,2},{3,19},{19,3},{4,20},{20... | collective-permute-start | bytes 786440 | tf_op jit(solution)/shard_map/ppermute | solution.py:486
  132.6 2.2 %weights.1 = (bf16[2048,128]{1,0:T(8,128)(2,1)}, bf16[2048,128]{1,0:T(8,128)(2,1)}, bf16[128,2048]{1,0:T(8,128)(2,1)}) custom-call(bf16[16,2,384,128]{3,2,1,0:T(8,128)(2,1)S(1)} %bitcast.12, bf16[384,128]{1,0:T(8,128)(2,1)S(1)} %get-tuple-element.62.hid_ref, bf16[384,256]{1,0:T(8,128)(2,1)S(1)} %get-tuple-element.63.both_ref), custom_call_target="tpu_custom_call" | custom-call | flops 536870912 | bytes 1048576 | tf_op jit(solution)/shard_map/weights/pallas_call | solution.py:55
  134.8 0.0 collective-permute-done.1.other_ref
  134.8 0.0 copy-done.8
  134.8 0.3 resid.1
  135.1 13.8 %all_to_all.40.r_ref = bf16[16,128,128]{2,1,0:T(8,128)(2,1)S(1)} all-to-all(bf16[16,128,128]{2,1,0:T(8,128)(2,1)S(1)} %resid.1), channel_id=1, replica_groups=mesh['z'=16,'c'=2,'tp'=16] {'tp'}, dimensions={0} | all-to-all | bytes 1048576 | tf_op jit(solution)/shard_map/all_to_all | solution.py:427
  148.8 0.0 copy-done.3
  148.8 0.0 copy-done.6
  148.8 0.0 copy-done.7
  148.9 0.0 copy-done.9
  148.9 0.6 proj.1
  149.5 3.4 %collective-permute-start.2 = (bf16[18,64,128]{2,1,0:T(8,128)(2,1)S(1)}, bf16[18,64,128]{2,1,0:T(8,128)(2,1)S(1)}, u32[]{:S(2)}, u32[]{:S(2)}) collective-permute-start(bf16[18,64,128]{2,1,0:T(8,128)(2,1)S(1)} %get-tuple-element.73), channel_id=1, source_target_pairs={{0,16},{16,0},{1,17},{17,1},{2,18},{18,2},{3,19},{19,3},{4,20},{20... | collective-permute-start | bytes 884744 | tf_op jit(solution)/shard_map/ppermute | solution.py:510
  152.9 0.0 copy-done.4
  152.9 0.0 copy-done.5
  152.9 0.0 copy-done.10
  152.9 1.1 intra.1
  154.0 0.0 collective-permute-done.2.got_ref
  154.1 0.1 chip.1
  154.2 20.4 %all_to_all.41.got_ref = bf16[16,96,128]{2,1,0:T(8,128)(2,1)S(1)} all-to-all(bf16[16,96,128]{2,1,0:T(8,128)(2,1)S(1)} %get-tuple-element.81), channel_id=1, replica_groups=mesh['z'=16,'c'=2,'tp'=16] {'z'}, dimensions={0} | all-to-all | bytes 786432 | tf_op jit(solution)/shard_map/all_to_all | solution.py:427
  174.5 0.1 gather.1
  174.6 8.9 %all-gather = f32[4,32,128]{2,1,0:T(8,128)S(1)} all-gather(f32[2,32,128]{2,1,0:T(8,128)S(1)} %gather.1), channel_id=2, replica_groups=mesh['z'=16,'c'=2,'tp'=16] {'c'}, dimensions={0}, use_global_device_ids=true | all-gather | bytes 98304 | tf_op jit(solution)/shard_map/all_gather | solution.py:526
  183.5 0.9 final.1
  (1 shorter events, 0.0 us)
Async XLA Ops:
  3.0 10.1 %collective-permute-start = (bf16[912,128]{1,0:T(8,128)(2,1)}, bf16[912,128]{1,0:T(8,128)(2,1)S(1)}, u32[]{:S(2)}, u32[]{:S(2)}) collective-permute-start(bf16[912,128]{1,0:T(8,128)(2,1)} %get-tuple-element.49), channel_id=1, source_target_pairs={{0,16},{16,0},{1,17},{17,1},{2,18},{18,2},{3,19},{19,3},{4,20},{20... | collective-permute-start | bytes 700424 | tf_op jit(solution)/shard_map/ppermute | solution.py:457
  11.7 0.9 copy-start.11
  51.6 25.4 %copy-start = (bf16[1,2048,128]{2,1,0:T(8,128)(2,1)S(1)}, bf16[1,2048,128]{2,1,0:T(8,128)(2,1)}, u32[]{:S(2)}) copy-start(bf16[1,2048,128]{2,1,0:T(8,128)(2,1)} %param.25) | copy-start | bytes 1572868
  51.6 25.4 %copy-start.1 = (bf16[1,2048,128]{2,1,0:T(8,128)(2,1)S(1)}, bf16[1,2048,128]{2,1,0:T(8,128)(2,1)}, u32[]{:S(2)}) copy-start(bf16[1,2048,128]{2,1,0:T(8,128)(2,1)} %param.26) | copy-start | bytes 1572868
  51.6 25.4 %copy-start.2 = (bf16[1,128,2048]{2,1,0:T(8,128)(2,1)S(1)}, bf16[1,128,2048]{2,1,0:T(8,128)(2,1)}, u32[]{:S(2)}) copy-start(bf16[1,128,2048]{2,1,0:T(8,128)(2,1)} %param.27) | copy-start | bytes 1572868
  97.3 37.5 %copy-start.8 = (bf16[128,128]{1,0:T(8,128)(2,1)S(1)}, bf16[128,128]{1,0:T(8,128)(2,1)}, u32[]{:S(2)}) copy-start(bf16[128,128]{1,0:T(8,128)(2,1)} %get-tuple-element.60.cols_ref) | copy-start | bytes 98308
  124.5 24.3 %copy-start.3 = (bf16[2048,128]{1,0:T(8,128)(2,1)S(1)}, bf16[2048,128]{1,0:T(8,128)(2,1)}, u32[]{:S(2)}) copy-start(bf16[2048,128]{1,0:T(8,128)(2,1)} %p_ref.1) | copy-start | bytes 1572868
  124.5 24.3 %copy-start.6 = (bf16[64,128]{1,0:T(8,128)(2,1)S(1)}, bf16[64,128]{1,0:T(8,128)(2,1)}, u32[]{:S(2)}) copy-start(bf16[64,128]{1,0:T(8,128)(2,1)} %q_ref.3) | copy-start | bytes 49156
  124.5 24.3 %copy-start.7 = (bf16[128,128]{1,0:T(8,128)(2,1)S(1)}, bf16[128,128]{1,0:T(8,128)(2,1)}, u32[]{:S(2)}) copy-start(bf16[128,128]{1,0:T(8,128)(2,1)} %mixer_ref.1) | copy-start | bytes 98308
  124.5 24.3 %copy-start.9 = (f32[8,128]{1,0:T(8,128)S(1)}, f32[8,128]{1,0:T(8,128)}, u32[]{:S(2)}) copy-start(f32[8,128]{1,0:T(8,128)} %get-tuple-element.71.mine_ref) | copy-start | bytes 12292
  124.6 28.3 %copy-start.4 = (bf16[128,128]{1,0:T(8,128)(2,1)S(1)}, bf16[128,128]{1,0:T(8,128)(2,1)}, u32[]{:S(2)}) copy-start(bf16[128,128]{1,0:T(8,128)(2,1)} %v_ref.1) | copy-start | bytes 98308
  124.6 28.3 %copy-start.5 = (bf16[64,128]{1,0:T(8,128)(2,1)S(1)}, bf16[64,128]{1,0:T(8,128)(2,1)}, u32[]{:S(2)}) copy-start(bf16[64,128]{1,0:T(8,128)(2,1)} %k_ref.1) | copy-start | bytes 49156
  124.6 28.3 %copy-start.10 = (f32[1,128]{1,0:T(1,128)S(1)}, f32[1,128]{1,0:T(1,128)}, u32[]{:S(2)}) copy-start(f32[1,128]{1,0:T(1,128)} %rate_ref.1) | copy-start | bytes 1540
  124.6 10.2 %collective-permute-start.1 = (bf16[16,64,128]{2,1,0:T(8,128)(2,1)S(1)}, bf16[16,64,128]{2,1,0:T(8,128)(2,1)S(1)}, u32[]{:S(2)}, u32[]{:S(2)}) collective-permute-start(bf16[16,64,128]{2,1,0:T(8,128)(2,1)S(1)} %pad_maximum_fusion.own_ref), channel_id=1, source_target_pairs={{0,16},{16,0},{1,17},{17,1},{2,18},{18,2},{3,19},{19,3},{4,20},{20... | collective-permute-start | bytes 786440 | tf_op jit(solution)/shard_map/ppermute | solution.py:486
  149.5 4.6 %collective-permute-start.2 = (bf16[18,64,128]{2,1,0:T(8,128)(2,1)S(1)}, bf16[18,64,128]{2,1,0:T(8,128)(2,1)S(1)}, u32[]{:S(2)}, u32[]{:S(2)}) collective-permute-start(bf16[18,64,128]{2,1,0:T(8,128)(2,1)S(1)} %get-tuple-element.73), channel_id=1, source_target_pairs={{0,16},{16,0},{1,17},{17,1},{2,18},{18,2},{3,19},{19,3},{4,20},{20... | collective-permute-start | bytes 884744 | tf_op jit(solution)/shard_map/ppermute | solution.py:510

commit v6 on v4

--- a/solution.py
+++ b/solution.py
@@ -94,15 +94,6 @@
     return match & (ranks == rank.astype(F32)), first
 
 
-def rows_of(stride, shift, mul, core):
-    n = lax.broadcasted_iota(jnp.int32, (NZ * stride, TOK), 0)
-    z = lax.shift_right_logical(n * mul, shift)
-    q = n - stride * z
-    keep = jnp.where(q < CAP, 2 * z + core, -1)
-    send = jnp.where((q >= CAP) & (q < 2 * CAP), 2 * z + 1 - core, -1)
-    return keep, q, send, q - CAP
-
-
 def decay_parts(rates):
     upto = lax.broadcasted_iota(jnp.int32, (TOK, TOK), 1) <= lax.broadcasted_iota(
         jnp.int32, (TOK, TOK), 0
@@ -118,75 +109,114 @@
     return col, row, start, end, jnp.broadcast_to(total, (1, TOK))
 
 
-def in_pieces(total):
-    hi = jnp.broadcast_to(total, (8, TOK)).astype(BF).astype(F32)
-    mid = (total - hi).astype(BF).astype(F32)
-    low = total - hi - mid
-    number = lax.broadcasted_iota(jnp.int32, (8, TOK), 0)
-    return jnp.where(
-        number == 0, hi, jnp.where(number == 1, mid, jnp.where(number == 2, low, 0.0))
-    ).astype(BF)
-
-
-def pack_kernel(
+def in_pieces(row):
+    hi = row.astype(BF).astype(F32)
+    mid = (row - hi).astype(BF).astype(F32)
+    return jnp.concatenate([hi, mid, row - hi - mid], axis=0)
+
+
+def in_one(pieces):
+    pieces = pieces.astype(F32)
+    return pieces[0:1, :] + pieces[1:2, :] + pieces[2:3, :]
+
+
+def ids_of(rows):
+    return rows[IDS - ROUTE : IDS - ROUTE + 2, :].astype(jnp.int32)
+
+
+def rates_of(g_ref, block):
+    return in_one(g_ref[block, ROUTE:HELD, :].astype(F32)[RATE - ROUTE : IDS - ROUTE])
+
+
+COT, INP, KEY, VALUE, ROUTE, RATE, IDS, HELD = 0, 128, 256, 320, 448, 456, 459, 464
+
+
+def load_kernel(
     ids_in, gw_in, ew_in, cot_in, inp_in, rate_in, k_in, v_in,
-    keep_ref, send_ref, cols_ref, mine_ref,
-    ids_ref, gw_ref, ew_ref, inp_ref, rate_ref, k_ref, v_ref, sems,
+    out_ref, ids_ref, gw_ref, ew_ref, rate_ref, sems,
 ):
     here = pl.ds(pl.multiple_of(spot("tp") * COL, COL), COL)
     fetch(
         (ids_in, gw_in, ew_in, cot_in.at[:, here], inp_in.at[:, here], rate_in, k_in, v_in),
-        (ids_ref, gw_ref, ew_ref, cols_ref, inp_ref, rate_ref, k_ref, v_ref),
+        (
+            ids_ref, gw_ref, ew_ref, out_ref.at[pl.ds(COT, TOK)], out_ref.at[pl.ds(INP, TOK)],
+            rate_ref, out_ref.at[pl.ds(KEY, KD)], out_ref.at[pl.ds(VALUE, VD)],
+        ),
         sems,
     )
-    ids = ids_ref[...]
     weights = gw_ref[...] * ew_ref[...]
-    cot, inp = cols_ref[...], inp_ref[...]
-    ek, rk, es, rs = rows_of(2 * CAP, 16, 2731, spot("c"))
-    for wanted, rank, out in ((ek, rk, keep_ref), (es, rs, send_ref)):
-        hit, first = placement(ids, wanted, rank)
+    none = jnp.zeros((2, TOK), F32)
+    out_ref[ROUTE:HELD, :] = jnp.concatenate(
+        [in_pieces(weights[0:1, :]), in_pieces(weights[1:2, :]), none]
+        + [in_pieces(rate_ref[...]), ids_ref[...].astype(F32), none, none[0:1, :]],
+        axis=0,
+    ).astype(BF)
+
+
+def pack_kernel(g_ref, rows_ref, picks_ref, small_ref, mine_ref):
+    core = spot("c")
+    number = lax.broadcasted_iota(jnp.int32, (NZ * 2 * CAP, TOK), 0)
+    z = lax.shift_right_logical(number * 2731, 16)
+    q = number - 2 * CAP * z
+    first_half = q < CAP
+    inp_rows = cot_rows = 0.0
+    for block, wanted, rank in (
+        (core, jnp.where(first_half, 2 * z + core, -1), q),
+        (1 - core, jnp.where(first_half, -1, 2 * z + core), q - CAP),
+    ):
+        rows = g_ref[block, ROUTE:HELD, :].astype(F32)
+        hit, first = placement(ids_of(rows), wanted, rank)
         scale = jnp.sum(
-            jnp.where(hit, jnp.where(first, weights[0:1, :], weights[1:2, :]), 0.0),
+            jnp.where(hit, jnp.where(first, in_one(rows[0:3]), in_one(rows[3:6])), 0.0),
             axis=1,
             keepdims=True,
         )
         take = jnp.where(hit, 1.0, 0.0).astype(BF)
-        inp_rows = mm(take, inp)
-        cot_rows = mm(take, cot) * scale
-        for z in range(NZ):
-            part = slice(2 * CAP * z, 2 * CAP * (z + 1))
-            at = 4 * CAP * z
-            out[at : at + 2 * CAP, :] = inp_rows[part].astype(BF)
-            out[at + 2 * CAP : at + 4 * CAP, :] = cot_rows[part].astype(BF)
-    _, _, start, end, total = decay_parts(rate_ref[...])
-    keys, values = k_ref[...].astype(F32), v_ref[...]
-    early = exact(keys * end, values, NTR)
-    late = exact(keys * start, values, NTR)
-    mine_ref[0:64, :] = early
-    mine_ref[64:128, :] = late
-    mine_ref[128:136, :] = jnp.concatenate([total, start, end, jnp.zeros((5, TOK), F32)], axis=0)
-    send_ref[768:832, :] = early.astype(BF)
-    send_ref[832:896, :] = late.astype(BF)
-    send_ref[896:904, :] = in_pieces(total)
-    send_ref[904:912, :] = jnp.zeros((8, TOK), BF)
-
-
-def merge_kernel(keep_ref, got_ref, rows_ref, extra_ref):
+        if block is core:
+            picks_ref[0:384, :] = take
+        inp_rows = inp_rows + mm(take, g_ref[block, INP : INP + TOK, :])
+        cot_rows = cot_rows + mm(take, g_ref[block, COT : COT + TOK, :]) * scale
     for z in range(NZ):
-        part = slice(4 * CAP * z, 4 * CAP * (z + 1))
-        rows_ref[z] = keep_ref[part, :] + got_ref[part, :]
-    extra_ref[...] = got_ref[768:912, :]
-
-
-def picks_kernel(keep_in, ids_ref, picks_ref, keep_ref, sem):
-    copy = pltpu.make_async_copy(keep_in, keep_ref, sem)
-    copy.start()
-    ek, rk, es, rs = rows_of(32, 5, 1, spot("c"))
-    ids = ids_ref[...]
-    for wanted, rank, at in ((ek, rk, 0), (es, rs, 512)):
-        hit, _ = placement(ids, wanted, rank)
-        picks_ref[at : at + 512, :] = jnp.where(hit, 1.0, 0.0).astype(BF)
-    copy.wait()
+        part = slice(2 * CAP * z, 2 * CAP * (z + 1))
+        rows_ref[z, 0 : 2 * CAP, :] = inp_rows[part].astype(BF)
+        rows_ref[z, 2 * CAP : 4 * CAP, :] = cot_rows[part].astype(BF)
+    z = lax.shift_right_logical(number * 2731, 16)
+    hit, _ = placement(
+        ids_of(g_ref[core, ROUTE:HELD, :].astype(F32)),
+        jnp.where(first_half, -1, 2 * z + 1 - core),
+        q - CAP,
+    )
+    picks_ref[384:768, :] = jnp.where(hit, 1.0, 0.0).astype(BF)
+
+    _, _, start_a, end_a, total_a = decay_parts(rates_of(g_ref, 0))
+    _, _, start_b, end_b, total_b = decay_parts(rates_of(g_ref, 1))
+    half = pl.ds(pl.multiple_of(KEY + 32 * core, 32), 32)
+    keys = jnp.concatenate([g_ref[0, half, :], g_ref[1, half, :]], axis=1).astype(F32)
+    values = jnp.concatenate([g_ref[k, VALUE : VALUE + VD, :] for k in (0, 1)], axis=1)
+    early = jnp.concatenate([end_a * jnp.exp(-total_b), end_b], axis=1)
+    late = jnp.concatenate([start_a, start_b * jnp.exp(-total_a)], axis=1)
+    small_ref[0:32, :] = exact(keys * early, values, NTR).astype(BF)
+    small_ref[32:64, :] = exact(keys * late, values, NTR).astype(BF)
+    small_ref[64:72, :] = jnp.concatenate(
+        [in_pieces(total_a + total_b), jnp.zeros((5, TOK), F32)], axis=0
+    ).astype(BF)
+    is_first = core == 0
+    mine_ref[...] = jnp.concatenate(
+        [
+            jnp.where(is_first, start_a, start_b), jnp.where(is_first, end_a, end_b),
+            jnp.where(is_first, total_a, total_b), jnp.where(is_first, total_b, total_a),
+            jnp.zeros((4, TOK), F32),
+        ],
+        axis=0,
+    )
+
+
+def spread_kernel(got_ref, rows_ref):
+    for z in range(NZ):
+        for kind in range(2):
+            part = got_ref[z, 24 * kind : 24 * (kind + 1), :]
+            for k in range(4):
+                rows_ref[k, kind, 24 * z : 24 * (z + 1), :] = part
 
 
 def expert_kernel(x_ref, gw_ref, uw_ref, dw_ref, part_ref, hid_ref, both_ref):
@@ -233,30 +263,25 @@
     return [jnp.where(is_first, a[:32], a[32:]).astype(BF) for a in (both_early, both_late)]
 
 
-def sum_kernel(part_ref, mine_ref, extra_ref, out_ref):
+def sum_kernel(part_ref, small_ref, out_ref):
     total = part_ref[0].astype(F32)
     for t in range(1, NT):
         total = total + part_ref[t].astype(F32)
     out_ref[:, 0 : 2 * CAP, :] = total.reshape(NZ, 2 * CAP, COL).astype(BF)
-    decay = mine_ref[128:129, :]
-    out_ref[:, 2 * CAP : 32, :] = jnp.broadcast_to(in_pieces(decay)[None], (NZ, 8, COL))
-    pieces = extra_ref[128:136, :].astype(F32)
-    theirs = pieces[0:1, :] + pieces[1:2, :] + pieces[2:3, :]
-    early, late = chip_states(
-        mine_ref[0:64, :], mine_ref[64:128, :],
-        extra_ref[0:64, :].astype(F32), extra_ref[64:128, :].astype(F32),
-        jnp.exp(-decay), jnp.exp(-theirs),
-    )
+    early, late, pieces = small_ref[0:32, :], small_ref[32:64, :], small_ref[64:72, :]
     place = spot("z")
     for z in range(NZ):
-        out_ref[z, 32:64, :] = jnp.where(z > place, early, late)
-
-
-def resid_kernel(picks_ref, own_ref, other_ref, cols_ref, out_ref):
-    own = own_ref[:, 0:32, :].reshape(512, COL)
-    other = other_ref[:, 0:32, :].reshape(512, COL)
-    moe = mm(picks_ref[0:512, :], own, TN) + mm(picks_ref[512:1024, :], other, TN)
-    resid = (cols_ref[...].astype(F32) + moe).astype(BF)
+        out_ref[z, 24:56, :] = jnp.where(z > place, early, late)
+        out_ref[z, 56:64, :] = pieces
+
+
+def resid_kernel(picks_ref, own_ref, other_ref, g_ref, out_ref):
+    own, other = [
+        r[:, 0 : 2 * CAP, :].astype(F32).reshape(384, COL).astype(BF) for r in (own_ref, other_ref)
+    ]
+    moe = mm(picks_ref[0:384, :], own, TN) + mm(picks_ref[384:768, :], other, TN)
+    cot = g_ref[spot("c"), COT : COT + TOK, :]
+    resid = (cot.astype(F32) + moe).astype(BF)
     for t in range(NT):
         out_ref[t] = resid
 
@@ -267,8 +292,8 @@
     out_grad = mm(resid, p_ref[...])
     og_ref[...] = out_grad
     query = q_ref[...].astype(F32)
-    early = exact(query * mine_ref[130:131, :], out_grad)
-    late = exact(query * mine_ref[129:130, :], out_grad)
+    early = exact(query * mine_ref[1:2, :], out_grad)
+    late = exact(query * mine_ref[0:1, :], out_grad)
     state_ref[0] = early
     state_ref[1] = late
     send_ref[16] = early.astype(BF)
@@ -281,19 +306,6 @@
         send_ref[t] = jnp.where(core == 0, high, low).astype(BF)
 
 
-def decays(own_ref, other_ref):
-    def total(ref):
-        rows = ref[:, 2 * CAP : 32, :].astype(F32)
-        return rows[:, 0, :] + rows[:, 1, :] + rows[:, 2, :]
-
-    return total(own_ref), total(other_ref)
-
-
-def row_at(table, place):
-    number = lax.broadcasted_iota(jnp.int32, table.shape, 0)
-    return jnp.sum(jnp.where(number == place, table, 0.0), axis=0, keepdims=True)
-
-
 def at_block(far_early, far_late, near, theirs):
     is_first = spot("c") == 0
     early = far_early * jnp.where(is_first, 1.0, theirs) + jnp.where(is_first, 0.0, near)
@@ -302,12 +314,11 @@
 
 
 def intra_kernel(
-    og_ref, rate_ref, q_ref, k_ref, v_ref, own_ref, other_ref, extra_ref,
-    gq_ref, part_ref, weight_ref,
+    og_ref, q_ref, g_ref, mine_ref, own_ref, other_ref, gq_ref, part_ref, weight_ref
 ):
     place, core = spot("z"), spot("c")
-    own, other = decays(own_ref, other_ref)
-    chip = own + other
+    rows = own_ref[:, 56:64, :].astype(F32)
+    chip = rows[:, 0, :] + rows[:, 1, :] + rows[:, 2, :]
     number = lax.broadcasted_iota(jnp.int32, (NZ, COL), 0)
     between = jnp.zeros((NZ, COL), F32)
     for u in range(NZ):
@@ -322,7 +333,7 @@
     def far(ref):
         early = late = jnp.zeros((32, COL), F32)
         for z in range(NZ):
-            state = ref[z, 32:64, :].astype(F32)
+            state = ref[z, 24:56, :].astype(F32)
             early = early + state * early_w[z : z + 1, :]
             late = late + state * late_w[z : z + 1, :]
         return early, late
@@ -333,15 +344,18 @@
         jnp.concatenate([jnp.where(is_first, a, b), jnp.where(is_first, b, a)], axis=0)
         for a, b in zip(here, there)
     ]
-    near = jnp.where(is_first, extra_ref[64:128, :], extra_ref[0:64, :]).astype(F32)
-    theirs = jnp.exp(-row_at(other, place))
+    _, _, start, end, _ = decay_parts(rates_of(g_ref, 1 - core))
+    there = g_ref[1 - core, KEY : KEY + KD, :].astype(F32) * jnp.where(is_first, start, end)
+    near = exact(there, g_ref[1 - core, VALUE : VALUE + VD, :], NTR)
+    theirs = jnp.exp(-mine_ref[3:4, :])
     kv_early, kv_late = at_block(far_early, far_late, near, theirs)
     scale = KD ** (-0.5)
-    col, row, start, end, _ = decay_parts(rate_ref[...])
+    col, row, start, end, _ = decay_parts(rates_of(g_ref, core))
     low, high = scale * start, scale * end
     mixed = scale * jnp.exp(-jnp.abs(col - row))
     out_grad = og_ref[...]
-    query, key, value = q_ref[...], k_ref[...], v_ref[...]
+    query, key = q_ref[...], g_ref[core, KEY : KEY + KD, :]
+    value = g_ref[core, VALUE : VALUE + VD, :]
     score_grad = exact(out_grad, value) * mixed
     gq_ref[...] = (
         exact(key, score_grad, NTR)
@@ -355,11 +369,9 @@
     part_ref[384:392, :] = jnp.concatenate([low, high, theirs, jnp.zeros((5, TOK), F32)], axis=0)
 
 
-def chip_kernel(keep_ref, got_ref, state_ref, own_ref, other_ref, out_ref, near_ref):
+def chip_kernel(keep_ref, got_ref, state_ref, mine_ref, out_ref, near_ref):
     place, core = spot("z"), spot("c")
-    own, other = decays(own_ref, other_ref)
-    mine = jnp.exp(-row_at(own, place))
-    theirs = jnp.exp(-row_at(other, place))
+    mine, theirs = jnp.exp(-mine_ref[2:3, :]), jnp.exp(-mine_ref[3:4, :])
     early_other, late_other = got_ref[16].astype(F32), got_ref[17].astype(F32)
     early, late = chip_states(state_ref[0], state_ref[1], early_other, late_other, mine, theirs)
     near_ref[...] = jnp.where(core == 0, late_other, early_other)
@@ -401,11 +413,14 @@
     return first + second
 
 
+def within(blocks, axis, sets):
+    return lax.all_to_all(
+        blocks, axis, split_axis=0, concat_axis=0, axis_index_groups=sets, tiled=True
+    )
+
+
 def to_all(shard, axis, sets):
-    copies = jnp.broadcast_to(shard, (len(sets[0]), *shard.shape))
-    return lax.all_to_all(
-        copies, axis, split_axis=0, concat_axis=0, axis_index_groups=sets, tiled=True
-    )
+    return within(jnp.broadcast_to(shard, (len(sets[0]), *shard.shape)), axis, sets)
 
 
 def exchange(blocks, axis):
@@ -422,39 +437,35 @@
     gate_weight, up_weight, down_weight,
 ):
     ids = expert_ids.T
-    keep, send, cols, mine = call(
-        pack_kernel,
-        [arr((768, COL), BF), arr((912, COL), BF), arr((TOK, COL), BF), arr((136, TOK), F32)],
+    held = call(
+        load_kernel,
+        arr((HELD, COL), BF),
         (
             ids, group_weight.reshape(1, TOK), expert_weight.T, cotangent, moe_input,
             decay_rates, key_vectors, value_vectors,
         ),
-        "pack",
+        "load",
         60,
         stay=8,
         scratch=[
             pltpu.VMEM((2, TOK), jnp.int32), pltpu.VMEM((1, TOK), F32), pltpu.VMEM((2, TOK), F32),
-            pltpu.VMEM((TOK, COL), BF), pltpu.VMEM((1, TOK), F32), pltpu.VMEM((KD, TOK), BF),
-            pltpu.VMEM((VD, TOK), BF), pltpu.SemaphoreType.DMA((8,)),
+            pltpu.VMEM((1, TOK), F32), pltpu.SemaphoreType.DMA((8,)),
         ],
     )
-    picks, keep = call(
-        picks_kernel,
-        [arr((1024, TOK), BF), arr((768, COL), BF)],
-        (keep, ids),
-        "picks",
-        stay=1,
-        scratch=[pltpu.SemaphoreType.DMA(())],
-    )
-    swapped = lax.ppermute(send, "c", SWAP)
-    rows, extra = call(
-        merge_kernel, [arr((NZ, 4 * CAP, COL), BF), arr((144, COL), BF)], (keep, swapped), "merge"
-    )
-    rows, picks, extra = lax.optimization_barrier((rows, picks, extra))
+    held = lax.all_gather(held, "c")
+    rows, picks, small, mine = call(
+        pack_kernel,
+        [
+            arr((NZ, 4 * CAP, COL), BF), arr((768, TOK), BF), arr((72, COL), BF),
+            arr((8, TOK), F32),
+        ],
+        (held,),
+        "pack",
+    )
     rows = exchange(rows, "z")
-    rows = rows.reshape(NZ, 2, 2 * CAP, COL).transpose(1, 0, 2, 3).reshape(2, NZ * 2 * CAP, COL)
-    rows = to_all(rows, ("c", "tp"), groups(4, 1, 1, 4))
-    rows = to_all(rows, ("c", "tp"), groups(1, 4, 4, 1))
+    copies = call(spread_kernel, arr((4, 2, NZ * 2 * CAP, COL), BF), (rows,), "spread")
+    rows = within(copies, ("c", "tp"), groups(4, 1, 1, 4))
+    rows = to_all(rows.reshape(4, 2, NZ * 2 * CAP, COL), ("c", "tp"), groups(1, 4, 4, 1))
     rows = rows.reshape(NT, 2, NZ * 2 * CAP, COL)
     shares, hidden, both = call(
         expert_kernel,
@@ -464,7 +475,7 @@
         20,
     )
     shares = exchange(shares, "tp")
-    back = call(sum_kernel, arr((NZ, 64, COL), BF), (shares, mine, extra), "sums", 6)
+    back = call(sum_kernel, arr((NZ, 64, COL), BF), (shares, small), "sums", 6)
     own = exchange(back, "z")
     own, rows, hidden, both = lax.optimization_barrier((own, rows, hidden, both))
     other = lax.ppermute(own, "c", SWAP)
@@ -476,7 +487,7 @@
         16,
         1 << 29,
     )
-    resid = call(resid_kernel, arr((NT, TOK, COL), BF), (picks, own, other, cols), "resid")
+    resid = call(resid_kernel, arr((NT, TOK, COL), BF), (picks, own, other, held), "resid")
     resid, grad_gate, grad_up, grad_down = lax.optimization_barrier(
         (resid, grad_gate, grad_up, grad_down)
     )
@@ -495,13 +506,13 @@
     grad_queries, part, weight = call(
         intra_kernel,
         [arr((KD, TOK), F32), arr((392, TOK), F32), arr((32, TOK), F32)],
-        (out_grad, decay_rates, queries, key_vectors, value_vectors, own, other, extra),
+        (out_grad, queries, held, mine, own, other),
         "intra",
     )
     chip, near = call(
         chip_kernel,
         [arr((NZ, 96, COL), BF), arr((KD, VD), F32)],
-        (proj_keep, got, state, own, other),
+        (proj_keep, got, state, mine),
         "chip",
     )
     chip, grad_queries, part, weight = lax.optimization_barrier((chip, grad_queries, part, weight))

time: 183 us -> 181 us (0.989)
  blocking collectives: 147 us -> 156 us
  starting transfers between devices: 22.5 us -> 13.6 us
    ppermute x1 -> x0, starting transfers between devices: 8.75 us -> none  [on_device(): swapped = lax.ppermute(send, 'c', SWAP)]
    all_gather x0 -> x1, blocking collectives: none -> 8.67 us  [on_device(): held = lax.all_gather(held, 'c')]
  transfers between devices with their start and end apart: 3 -> 2, of which waited for: 0 -> 0; matrix products, arithmetic and copies ran while one was open for 0% -> 0% of each run, Pallas kernels for 2% -> 2%
where the time goes in v6:
time: 181 us; the launch traced here: 180 us
  blocking collectives  156 us (86%)
  starting transfers between devices  13.6 us (8%)
  Pallas kernels  9.29 us (5%)
    all_to_all x5, blocking collectives, exchange(): return lax.all_to_all(blocks, axis, split_axis=0, concat_axis=0, tiled=True)  100 us
    all_to_all x2, blocking collectives, within(): lax.all_to_all(blocks, axis, split_axis=0, concat_axis=0, axis_index_grou...  37.5 us
    ppermute x1, starting transfers between devices, on_device(): other = lax.ppermute(own, 'c', SWAP)  10.5 us
    pallas_call x12, Pallas kernels, call(): pl.pallas_call(kernel, out_shape=outs, in_specs=[hbm()] * stay + [vmem()]...  9.29 us
    all_gather x1, blocking collectives, on_device(): far = lax.all_gather(far, 'c')  9.16 us
    all_gather x1, blocking collectives, on_device(): held = lax.all_gather(held, 'c')  8.67 us
  transfers between devices with their start and end apart: 2, of which 0 were waited for; matrix products, arithmetic and copies ran while one was open for 0% of the time, Pallas kernels for 2%

profile of v6, /device:TPU:1, one launch (start us, length us, event | category | flops | bytes accessed | tf_op | source)
XLA Modules:
  0.0 180.2 jit_solution(4464622150391719683)
XLA Ops:
  0.6 1.6 load.1
  2.2 8.7 %all-gather = bf16[928,128]{1,0:T(8,128)(2,1)S(1)} all-gather(bf16[464,128]{1,0:T(8,128)(2,1)} %load.1), channel_id=2, replica_groups=mesh['z'=16,'c'=2,'tp'=16] {'c'}, dimensions={0}, use_global_device_ids=true | all-gather | bytes 356352 | tf_op jit(solution)/shard_map/all_gather | solution.py:455
  10.9 0.5 pack.1
  11.5 22.2 %all_to_all.35.got_ref = bf16[16,48,128]{2,1,0:T(8,128)(2,1)S(1)} all-to-all(bf16[16,48,128]{2,1,0:T(8,128)(2,1)S(1)} %get-tuple-element.42), channel_id=1, replica_groups=mesh['z'=16,'c'=2,'tp'=16] {'z'}, dimensions={0} | all-to-all | bytes 393216 | tf_op jit(solution)/shard_map/all_to_all | solution.py:427
  33.7 0.1 spread.1
  33.8 12.2 %all_to_all.36 = bf16[4,2,384,128]{3,2,1,0:T(8,128)(2,1)S(1)} all-to-all(bf16[4,2,384,128]{3,2,1,0:T(8,128)(2,1)S(1)} %spread.1), channel_id=1, replica_groups={{0,4,8,12},{1,5,9,13},{2,6,10,14},{3,7,11,15},{16,17,18,19},{20,21,22,2..., dimensions={0} | all-to-all | bytes 1572864 | tf_op jit(solution)/shard_map/all_to_all | solution.py:417
  45.9 0.7 broadcast_in_dim.12
  46.7 0.0 copy-start
  46.7 0.0 copy-start.1
  46.7 0.0 copy-start.2
  46.7 25.4 %all_to_all.37 = bf16[4,4,2,384,128]{4,3,2,1,0:T(8,128)(2,1)S(1)} all-to-all(bf16[4,4,2,384,128]{4,3,2,1,0:T(8,128)(2,1)S(1)} %broadcast_in_dim.12), channel_id=1, replica_groups={{0,1,2,3},{4,5,6,7},{8,9,10,11},{12,13,14,15},{16,20,24,28},{17,21,25,2..., dimensions={0} | all-to-all | bytes 6291456 | tf_op jit(solution)/shard_map/all_to_all | solution.py:417
  72.1 0.0 copy-done
  72.1 0.0 copy-done.1
  72.1 0.0 copy-done.2
  72.1 1.4 expert.1
  73.5 19.2 %all_to_all.38.part_ref = bf16[16,384,128]{2,1,0:T(8,128)(2,1)S(1)} all-to-all(bf16[16,384,128]{2,1,0:T(8,128)(2,1)S(1)} %get-tuple-element.43), channel_id=1, replica_groups=mesh['z'=16,'c'=2,'tp'=16] {'tp'}, dimensions={0} | all-to-all | bytes 3145728 | tf_op jit(solution)/shard_map/all_to_all | solution.py:427
  92.7 0.2 sums.1
  92.9 0.0 copy-start.3
  92.9 0.0 copy-start.4
  93.0 0.0 copy-start.5
  93.0 23.9 %all_to_all.39.own_ref = bf16[16,64,128]{2,1,0:T(8,128)(2,1)S(1)} all-to-all(bf16[16,64,128]{2,1,0:T(8,128)(2,1)S(1)} %sums.1), channel_id=1, replica_groups=mesh['z'=16,'c'=2,'tp'=16] {'z'}, dimensions={0} | all-to-all | bytes 524288 | tf_op jit(solution)/shard_map/all_to_all | solution.py:427
  116.9 10.5 %collective-permute-start = (bf16[16,64,128]{2,1,0:T(8,128)(2,1)S(1)}, bf16[16,64,128]{2,1,0:T(8,128)(2,1)S(1)}, u32[]{:S(2)}, u32[]{:S(2)}) collective-permute-start(bf16[16,64,128]{2,1,0:T(8,128)(2,1)S(1)} %all_to_all.39.own_ref), channel_id=1, source_target_pairs={{0,16},{16,0},{1,17},{17,1},{2,18},{18,2},{3,19},{19,3},{4,20},{20... | collective-permute-start | bytes 786440 | tf_op jit(solution)/shard_map/ppermute | solution.py:481
  127.4 2.2 %weights.1 = (bf16[2048,128]{1,0:T(8,128)(2,1)}, bf16[2048,128]{1,0:T(8,128)(2,1)}, bf16[128,2048]{1,0:T(8,128)(2,1)}) custom-call(bf16[16,2,384,128]{3,2,1,0:T(8,128)(2,1)S(1)} %bitcast.13, bf16[384,128]{1,0:T(8,128)(2,1)S(1)} %get-tuple-element.49.hid_ref, bf16[384,256]{1,0:T(8,128)(2,1)S(1)} %get-tuple-element.50.both_ref), custom_call_target="tpu_custom_call" | custom-call | flops 536870912 | bytes 1048576 | tf_op jit(solution)/shard_map/weights/pallas_call | solution.py:55
  129.6 0.0 collective-permute-done.other_ref
  129.6 0.3 resid.1
  129.9 13.9 %all_to_all.40.r_ref = bf16[16,128,128]{2,1,0:T(8,128)(2,1)S(1)} all-to-all(bf16[16,128,128]{2,1,0:T(8,128)(2,1)S(1)} %resid.1), channel_id=1, replica_groups=mesh['z'=16,'c'=2,'tp'=16] {'tp'}, dimensions={0} | all-to-all | bytes 1048576 | tf_op jit(solution)/shard_map/all_to_all | solution.py:427
  143.8 0.0 copy-done.3
  143.8 0.0 copy-done.4
  143.8 0.0 copy-done.5
  143.8 0.6 proj.1
  144.4 3.1 %collective-permute-start.1 = (bf16[18,64,128]{2,1,0:T(8,128)(2,1)S(1)}, bf16[18,64,128]{2,1,0:T(8,128)(2,1)S(1)}, u32[]{:S(2)}, u32[]{:S(2)}) collective-permute-start(bf16[18,64,128]{2,1,0:T(8,128)(2,1)S(1)} %get-tuple-element.60), channel_id=1, source_target_pairs={{0,16},{16,0},{1,17},{17,1},{2,18},{18,2},{3,19},{19,3},{4,20},{20... | collective-permute-start | bytes 884744 | tf_op jit(solution)/shard_map/ppermute | solution.py:505
  147.5 1.3 intra.1
  148.8 0.0 collective-permute-done.1.got_ref
  148.8 0.1 chip.1
  148.9 21.2 %all_to_all.41.got_ref = bf16[16,96,128]{2,1,0:T(8,128)(2,1)S(1)} all-to-all(bf16[16,96,128]{2,1,0:T(8,128)(2,1)S(1)} %get-tuple-element.67), channel_id=1, replica_groups=mesh['z'=16,'c'=2,'tp'=16] {'z'}, dimensions={0} | all-to-all | bytes 786432 | tf_op jit(solution)/shard_map/all_to_all | solution.py:427
  170.1 0.1 gather.1
  170.2 9.2 %all-gather.1 = f32[4,32,128]{2,1,0:T(8,128)S(1)} all-gather(f32[2,32,128]{2,1,0:T(8,128)S(1)} %gather.1), channel_id=3, replica_groups=mesh['z'=16,'c'=2,'tp'=16] {'c'}, dimensions={0}, use_global_device_ids=true | all-gather | bytes 98304 | tf_op jit(solution)/shard_map/all_gather | solution.py:521
  179.4 0.9 final.1
Async XLA Ops:
  46.7 25.4 %copy-start = (bf16[1,2048,128]{2,1,0:T(8,128)(2,1)S(1)}, bf16[1,2048,128]{2,1,0:T(8,128)(2,1)}, u32[]{:S(2)}) copy-start(bf16[1,2048,128]{2,1,0:T(8,128)(2,1)} %param.25) | copy-start | bytes 1572868
  46.7 25.4 %copy-start.1 = (bf16[1,2048,128]{2,1,0:T(8,128)(2,1)S(1)}, bf16[1,2048,128]{2,1,0:T(8,128)(2,1)}, u32[]{:S(2)}) copy-start(bf16[1,2048,128]{2,1,0:T(8,128)(2,1)} %param.26) | copy-start | bytes 1572868
  46.7 25.4 %copy-start.2 = (bf16[1,128,2048]{2,1,0:T(8,128)(2,1)S(1)}, bf16[1,128,2048]{2,1,0:T(8,128)(2,1)}, u32[]{:S(2)}) copy-start(bf16[1,128,2048]{2,1,0:T(8,128)(2,1)} %param.27) | copy-start | bytes 1572868
  92.9 50.9 %copy-start.3 = (bf16[2048,128]{1,0:T(8,128)(2,1)S(1)}, bf16[2048,128]{1,0:T(8,128)(2,1)}, u32[]{:S(2)}) copy-start(bf16[2048,128]{1,0:T(8,128)(2,1)} %p_ref.1) | copy-start | bytes 1572868
  92.9 50.9 %copy-start.4 = (bf16[64,128]{1,0:T(8,128)(2,1)S(1)}, bf16[64,128]{1,0:T(8,128)(2,1)}, u32[]{:S(2)}) copy-start(bf16[64,128]{1,0:T(8,128)(2,1)} %q_ref.3) | copy-start | bytes 49156
  93.0 50.9 %copy-start.5 = (bf16[128,128]{1,0:T(8,128)(2,1)S(1)}, bf16[128,128]{1,0:T(8,128)(2,1)}, u32[]{:S(2)}) copy-start(bf16[128,128]{1,0:T(8,128)(2,1)} %mixer_ref.1) | copy-start | bytes 98308
  116.9 12.7 %collective-permute-start = (bf16[16,64,128]{2,1,0:T(8,128)(2,1)S(1)}, bf16[16,64,128]{2,1,0:T(8,128)(2,1)S(1)}, u32[]{:S(2)}, u32[]{:S(2)}) collective-permute-start(bf16[16,64,128]{2,1,0:T(8,128)(2,1)S(1)} %all_to_all.39.own_ref), channel_id=1, source_target_pairs={{0,16},{16,0},{1,17},{17,1},{2,18},{18,2},{3,19},{19,3},{4,20},{20... | collective-permute-start | bytes 786440 | tf_op jit(solution)/shard_map/ppermute | solution.py:481
  144.4 4.4 %collective-permute-start.1 = (bf16[18,64,128]{2,1,0:T(8,128)(2,1)S(1)}, bf16[18,64,128]{2,1,0:T(8,128)(2,1)S(1)}, u32[]{:S(2)}, u32[]{:S(2)}) collective-permute-start(bf16[18,64,128]{2,1,0:T(8,128)(2,1)S(1)} %get-tuple-element.60), channel_id=1, source_target_pairs={{0,16},{16,0},{1,17},{17,1},{2,18},{18,2},{3,19},{19,3},{4,20},{20... | collective-permute-start | bytes 884744 | tf_op jit(solution)/shard_map/ppermute | solution.py:505

commit v7 on v6

--- a/solution.py
+++ b/solution.py
@@ -51,12 +51,12 @@
     return pl.BlockSpec(memory_space=pltpu.HBM)
 
 
-def call(kernel, outs, args, name, mib=4, flops=1 << 27, stay=0, scratch=()):
+def call(kernel, outs, args, name, mib=4, flops=1 << 27, stay=0, scratch=(), out=None):
     return pl.pallas_call(
         kernel,
         out_shape=outs,
         in_specs=[hbm()] * stay + [vmem()] * (len(args) - stay),
-        out_specs=jax.tree.map(lambda _: vmem(), outs),
+        out_specs=jax.tree.map(lambda _: (out or vmem)(), outs),
         scratch_shapes=scratch,
         name=name,
         compiler_params=pltpu.CompilerParams(vmem_limit_bytes=mib << 20),
@@ -239,17 +239,32 @@
         part_ref[t + 1] = out[:, COL:]
 
 
-def weight_kernel(x_ref, hid_ref, both_ref, gg_ref, gu_ref, gd_ref):
-    both = both_ref[...]
-    hidden = hid_ref[...]
+def weight_kernel(
+    x_ref, hid_ref, both_ref, gg_out, gu_out, gd_out, gg_ref, gu_ref, gd_ref, sems
+):
+    both = both_ref[...].T
+    hidden = hid_ref[...].T
+    copies = []
     for t in range(0, NT, 2):
         rows = slice(t * COL, (t + 2) * COL)
         inp = jnp.concatenate([x_ref[held_at(t), 0], x_ref[held_at(t + 1), 0]], axis=1)
         cot = jnp.concatenate([x_ref[held_at(t), 1], x_ref[held_at(t + 1), 1]], axis=1)
-        out = mm(inp, both, TN).astype(BF)
+        out = mm(both, inp).astype(BF).T
         gg_ref[rows, :] = out[:, :128]
         gu_ref[rows, :] = out[:, 128:]
-        gd_ref[:, rows] = mm(hidden, cot, TN).astype(BF)
+        gd_ref[:, rows] = mm(hidden, cot).astype(BF)
+        if t % 4 == 2:
+            done = pl.ds((t - 2) * COL, 4 * COL)
+            for n, (src, dst) in enumerate(
+                (
+                    (gg_ref.at[done], gg_out.at[done]), (gu_ref.at[done], gu_out.at[done]),
+                    (gd_ref.at[:, done], gd_out.at[:, done]),
+                )
+            ):
+                copies.append(pltpu.make_async_copy(src, dst, sems.at[t // 4, n]))
+                copies[-1].start()
+    for copy in copies:
+        copy.wait()
 
 
 def chip_states(early, late, early_other, late_other, mine, theirs):
@@ -479,13 +494,16 @@
     own = exchange(back, "z")
     own, rows, hidden, both = lax.optimization_barrier((own, rows, hidden, both))
     other = lax.ppermute(own, "c", SWAP)
+    shapes = [arr((2048, 128), BF), arr((2048, 128), BF), arr((128, 2048), BF)]
     grad_gate, grad_up, grad_down = call(
         weight_kernel,
-        [arr((2048, 128), BF), arr((2048, 128), BF), arr((128, 2048), BF)],
+        shapes,
         (rows, hidden, both),
         "weights",
         16,
         1 << 29,
+        scratch=[pltpu.VMEM(a.shape, BF) for a in shapes] + [pltpu.SemaphoreType.DMA((4, 3))],
+        out=hbm,
     )
     resid = call(resid_kernel, arr((NT, TOK, COL), BF), (picks, own, other, held), "resid")
     resid, grad_gate, grad_up, grad_down = lax.optimization_barrier(

time: 181 us -> 180 us (level)
  no operation moved by 1% of the time
where the time goes in v7:
time: 180 us
  blocking collectives  156 us (87%)
  starting transfers between devices  13.6 us (8%)
  Pallas kernels  9.02 us (5%)
    all_to_all x5, blocking collectives, exchange(): return lax.all_to_all(blocks, axis, split_axis=0, concat_axis=0, tiled=True)  100 us
    all_to_all x2, blocking collectives, within(): lax.all_to_all(blocks, axis, split_axis=0, concat_axis=0, axis_index_grou...  37.5 us
    ppermute x1, starting transfers between devices, on_device(): other = lax.ppermute(own, 'c', SWAP)  10.5 us
    all_gather x1, blocking collectives, on_device(): far = lax.all_gather(far, 'c')  9.16 us
    pallas_call x12, Pallas kernels, call(): pl.pallas_call(kernel, out_shape=outs, in_specs=[hbm()] * stay + [vmem()]...  9.02 us
    all_gather x1, blocking collectives, on_device(): held = lax.all_gather(held, 'c')  8.67 us
  transfers between devices with their start and end apart: 2, of which 0 were waited for; matrix products, arithmetic and copies ran while one was open for 0% of the time, Pallas kernels for 2%

profile of v7, /device:TPU:1, one launch (start us, length us, event | category | flops | bytes accessed | tf_op | source)
XLA Modules:
  0.0 180.0 jit_solution(12530904441842854980)
XLA Ops:
  0.6 1.6 load.1
  2.2 8.7 %all-gather = bf16[928,128]{1,0:T(8,128)(2,1)S(1)} all-gather(bf16[464,128]{1,0:T(8,128)(2,1)} %load.1), channel_id=2, replica_groups=mesh['z'=16,'c'=2,'tp'=16] {'c'}, dimensions={0}, use_global_device_ids=true | all-gather | bytes 356352 | tf_op jit(solution)/shard_map/all_gather | solution.py:470
  10.9 0.5 pack.1
  11.5 22.2 %all_to_all.35.got_ref = bf16[16,48,128]{2,1,0:T(8,128)(2,1)S(1)} all-to-all(bf16[16,48,128]{2,1,0:T(8,128)(2,1)S(1)} %get-tuple-element.42), channel_id=1, replica_groups=mesh['z'=16,'c'=2,'tp'=16] {'z'}, dimensions={0} | all-to-all | bytes 393216 | tf_op jit(solution)/shard_map/all_to_all | solution.py:442
  33.7 0.1 spread.1
  33.8 12.2 %all_to_all.36 = bf16[4,2,384,128]{3,2,1,0:T(8,128)(2,1)S(1)} all-to-all(bf16[4,2,384,128]{3,2,1,0:T(8,128)(2,1)S(1)} %spread.1), channel_id=1, replica_groups={{0,4,8,12},{1,5,9,13},{2,6,10,14},{3,7,11,15},{16,17,18,19},{20,21,22,2..., dimensions={0} | all-to-all | bytes 1572864 | tf_op jit(solution)/shard_map/all_to_all | solution.py:432
  45.9 0.7 broadcast_in_dim.12
  46.7 0.0 copy-start
  46.7 0.0 copy-start.1
  46.7 0.0 copy-start.2
  46.7 25.4 %all_to_all.37 = bf16[4,4,2,384,128]{4,3,2,1,0:T(8,128)(2,1)S(1)} all-to-all(bf16[4,4,2,384,128]{4,3,2,1,0:T(8,128)(2,1)S(1)} %broadcast_in_dim.12), channel_id=1, replica_groups={{0,1,2,3},{4,5,6,7},{8,9,10,11},{12,13,14,15},{16,20,24,28},{17,21,25,2..., dimensions={0} | all-to-all | bytes 6291456 | tf_op jit(solution)/shard_map/all_to_all | solution.py:432
  72.1 0.0 copy-done
  72.1 0.0 copy-done.1
  72.1 0.0 copy-done.2
  72.1 1.4 expert.1
  73.5 19.2 %all_to_all.38.part_ref = bf16[16,384,128]{2,1,0:T(8,128)(2,1)S(1)} all-to-all(bf16[16,384,128]{2,1,0:T(8,128)(2,1)S(1)} %get-tuple-element.43), channel_id=1, replica_groups=mesh['z'=16,'c'=2,'tp'=16] {'tp'}, dimensions={0} | all-to-all | bytes 3145728 | tf_op jit(solution)/shard_map/all_to_all | solution.py:442
  92.7 0.2 sums.1
  92.9 0.0 copy-start.3
  92.9 0.0 copy-start.4
  93.0 0.0 copy-start.5
  93.0 23.9 %all_to_all.39.own_ref = bf16[16,64,128]{2,1,0:T(8,128)(2,1)S(1)} all-to-all(bf16[16,64,128]{2,1,0:T(8,128)(2,1)S(1)} %sums.1), channel_id=1, replica_groups=mesh['z'=16,'c'=2,'tp'=16] {'z'}, dimensions={0} | all-to-all | bytes 524288 | tf_op jit(solution)/shard_map/all_to_all | solution.py:442
  116.9 10.5 %collective-permute-start = (bf16[16,64,128]{2,1,0:T(8,128)(2,1)S(1)}, bf16[16,64,128]{2,1,0:T(8,128)(2,1)S(1)}, u32[]{:S(2)}, u32[]{:S(2)}) collective-permute-start(bf16[16,64,128]{2,1,0:T(8,128)(2,1)S(1)} %all_to_all.39.own_ref), channel_id=1, source_target_pairs={{0,16},{16,0},{1,17},{17,1},{2,18},{18,2},{3,19},{19,3},{4,20},{20... | collective-permute-start | bytes 786440 | tf_op jit(solution)/shard_map/ppermute | solution.py:496
  127.4 1.9 %weights.1 = (bf16[2048,128]{1,0:T(8,128)(2,1)}, bf16[2048,128]{1,0:T(8,128)(2,1)}, bf16[128,2048]{1,0:T(8,128)(2,1)}) custom-call(bf16[16,2,384,128]{3,2,1,0:T(8,128)(2,1)S(1)} %bitcast.13, bf16[384,128]{1,0:T(8,128)(2,1)S(1)} %get-tuple-element.49.hid_ref, bf16[384,256]{1,0:T(8,128)(2,1)S(1)} %get-tuple-element.50.both_ref), custom_call_target="tpu_custom_call" | custom-call | flops 536870912 | bytes 1048576 | tf_op jit(solution)/shard_map/weights/pallas_call | solution.py:55
  129.3 0.0 collective-permute-done.other_ref
  129.3 0.3 resid.1
  129.6 14.0 %all_to_all.40.r_ref = bf16[16,128,128]{2,1,0:T(8,128)(2,1)S(1)} all-to-all(bf16[16,128,128]{2,1,0:T(8,128)(2,1)S(1)} %resid.1), channel_id=1, replica_groups=mesh['z'=16,'c'=2,'tp'=16] {'tp'}, dimensions={0} | all-to-all | bytes 1048576 | tf_op jit(solution)/shard_map/all_to_all | solution.py:442
  143.6 0.0 copy-done.3
  143.6 0.0 copy-done.4
  143.6 0.0 copy-done.5
  143.6 0.6 proj.1
  144.2 3.1 %collective-permute-start.1 = (bf16[18,64,128]{2,1,0:T(8,128)(2,1)S(1)}, bf16[18,64,128]{2,1,0:T(8,128)(2,1)S(1)}, u32[]{:S(2)}, u32[]{:S(2)}) collective-permute-start(bf16[18,64,128]{2,1,0:T(8,128)(2,1)S(1)} %get-tuple-element.60), channel_id=1, source_target_pairs={{0,16},{16,0},{1,17},{17,1},{2,18},{18,2},{3,19},{19,3},{4,20},{20... | collective-permute-start | bytes 884744 | tf_op jit(solution)/shard_map/ppermute | solution.py:523
  147.3 1.3 intra.1
  148.6 0.0 collective-permute-done.1.got_ref
  148.6 0.1 chip.1
  148.7 21.2 %all_to_all.41.got_ref = bf16[16,96,128]{2,1,0:T(8,128)(2,1)S(1)} all-to-all(bf16[16,96,128]{2,1,0:T(8,128)(2,1)S(1)} %get-tuple-element.67), channel_id=1, replica_groups=mesh['z'=16,'c'=2,'tp'=16] {'z'}, dimensions={0} | all-to-all | bytes 786432 | tf_op jit(solution)/shard_map/all_to_all | solution.py:442
  169.9 0.1 gather.1
  169.9 9.2 %all-gather.1 = f32[4,32,128]{2,1,0:T(8,128)S(1)} all-gather(f32[2,32,128]{2,1,0:T(8,128)S(1)} %gather.1), channel_id=3, replica_groups=mesh['z'=16,'c'=2,'tp'=16] {'c'}, dimensions={0}, use_global_device_ids=true | all-gather | bytes 98304 | tf_op jit(solution)/shard_map/all_gather | solution.py:539
  179.1 0.9 final.1
Async XLA Ops:
  46.7 25.4 %copy-start = (bf16[1,2048,128]{2,1,0:T(8,128)(2,1)S(1)}, bf16[1,2048,128]{2,1,0:T(8,128)(2,1)}, u32[]{:S(2)}) copy-start(bf16[1,2048,128]{2,1,0:T(8,128)(2,1)} %param.25) | copy-start | bytes 1572868
  46.7 25.4 %copy-start.1 = (bf16[1,2048,128]{2,1,0:T(8,128)(2,1)S(1)}, bf16[1,2048,128]{2,1,0:T(8,128)(2,1)}, u32[]{:S(2)}) copy-start(bf16[1,2048,128]{2,1,0:T(8,128)(2,1)} %param.26) | copy-start | bytes 1572868
  46.7 25.4 %copy-start.2 = (bf16[1,128,2048]{2,1,0:T(8,128)(2,1)S(1)}, bf16[1,128,2048]{2,1,0:T(8,128)(2,1)}, u32[]{:S(2)}) copy-start(bf16[1,128,2048]{2,1,0:T(8,128)(2,1)} %param.27) | copy-start | bytes 1572868
  92.9 50.6 %copy-start.3 = (bf16[2048,128]{1,0:T(8,128)(2,1)S(1)}, bf16[2048,128]{1,0:T(8,128)(2,1)}, u32[]{:S(2)}) copy-start(bf16[2048,128]{1,0:T(8,128)(2,1)} %p_ref.1) | copy-start | bytes 1572868
  92.9 50.6 %copy-start.4 = (bf16[64,128]{1,0:T(8,128)(2,1)S(1)}, bf16[64,128]{1,0:T(8,128)(2,1)}, u32[]{:S(2)}) copy-start(bf16[64,128]{1,0:T(8,128)(2,1)} %q_ref.3) | copy-start | bytes 49156
  93.0 50.6 %copy-start.5 = (bf16[128,128]{1,0:T(8,128)(2,1)S(1)}, bf16[128,128]{1,0:T(8,128)(2,1)}, u32[]{:S(2)}) copy-start(bf16[128,128]{1,0:T(8,128)(2,1)} %mixer_ref.1) | copy-start | bytes 98308
  116.9 12.4 %collective-permute-start = (bf16[16,64,128]{2,1,0:T(8,128)(2,1)S(1)}, bf16[16,64,128]{2,1,0:T(8,128)(2,1)S(1)}, u32[]{:S(2)}, u32[]{:S(2)}) collective-permute-start(bf16[16,64,128]{2,1,0:T(8,128)(2,1)S(1)} %all_to_all.39.own_ref), channel_id=1, source_target_pairs={{0,16},{16,0},{1,17},{17,1},{2,18},{18,2},{3,19},{19,3},{4,20},{20... | collective-permute-start | bytes 786440 | tf_op jit(solution)/shard_map/ppermute | solution.py:496
  144.2 4.4 %collective-permute-start.1 = (bf16[18,64,128]{2,1,0:T(8,128)(2,1)S(1)}, bf16[18,64,128]{2,1,0:T(8,128)(2,1)S(1)}, u32[]{:S(2)}, u32[]{:S(2)}) collective-permute-start(bf16[18,64,128]{2,1,0:T(8,128)(2,1)S(1)} %get-tuple-element.60), channel_id=1, source_target_pairs={{0,16},{16,0},{1,17},{17,1},{2,18},{18,2},{3,19},{19,3},{4,20},{20... | collective-permute-start | bytes 884744 | tf_op jit(solution)/shard_map/ppermute | solution.py:523

commit v8 on v6

--- a/solution.py
+++ b/solution.py
@@ -428,7 +428,7 @@
 
 
 def held_at(t):
-    return jnp.where(spot("c") == 0, (t % 4) * 4 + t // 4, t)
+    return jnp.where(spot("c") == 1, (t % 4) * 4 + t // 4, t)
 
 
 def on_device(
@@ -464,8 +464,8 @@
     )
     rows = exchange(rows, "z")
     copies = call(spread_kernel, arr((4, 2, NZ * 2 * CAP, COL), BF), (rows,), "spread")
-    rows = within(copies, ("c", "tp"), groups(4, 1, 1, 4))
-    rows = to_all(rows.reshape(4, 2, NZ * 2 * CAP, COL), ("c", "tp"), groups(1, 4, 4, 1))
+    rows = within(copies, ("c", "tp"), groups(1, 4, 4, 1))
+    rows = to_all(rows.reshape(4, 2, NZ * 2 * CAP, COL), ("c", "tp"), groups(4, 1, 1, 4))
     rows = rows.reshape(NT, 2, NZ * 2 * CAP, COL)
     shares, hidden, both = call(
         expert_kernel,

time: 181 us -> 181 us (level)
  no operation moved by 1% of the time
where the time goes in v8:
time: 181 us; the launch traced here: 180 us
  blocking collectives  156 us (86%)
  starting transfers between devices  13.6 us (8%)
  Pallas kernels  9.29 us (5%)
    all_to_all x5, blocking collectives, exchange(): return lax.all_to_all(blocks, axis, split_axis=0, concat_axis=0, tiled=True)  100 us
    all_to_all x2, blocking collectives, within(): lax.all_to_all(blocks, axis, split_axis=0, concat_axis=0, axis_index_grou...  37.5 us
    ppermute x1, starting transfers between devices, on_device(): other = lax.ppermute(own, 'c', SWAP)  10.5 us
    pallas_call x12, Pallas kernels, call(): pl.pallas_call(kernel, out_shape=outs, in_specs=[hbm()] * stay + [vmem()]...  9.29 us
    all_gather x1, blocking collectives, on_device(): far = lax.all_gather(far, 'c')  9.16 us
    all_gather x1, blocking collectives, on_device(): held = lax.all_gather(held, 'c')  8.67 us
  transfers between devices with their start and end apart: 2, of which 0 were waited for; matrix products, arithmetic and copies ran while one was open for 0% of the time, Pallas kernels for 2%

profile of v8, /device:TPU:1, one launch (start us, length us, event | category | flops | bytes accessed | tf_op | source)
XLA Modules:
  0.0 180.2 jit_solution(14361226747193844875)
XLA Ops:
  0.6 1.6 load.1
  2.2 8.7 %all-gather = bf16[928,128]{1,0:T(8,128)(2,1)S(1)} all-gather(bf16[464,128]{1,0:T(8,128)(2,1)} %load.1), channel_id=2, replica_groups=mesh['z'=16,'c'=2,'tp'=16] {'c'}, dimensions={0}, use_global_device_ids=true | all-gather | bytes 356352 | tf_op jit(solution)/shard_map/all_gather | solution.py:455
  10.9 0.5 pack.1
  11.5 22.2 %all_to_all.35.got_ref = bf16[16,48,128]{2,1,0:T(8,128)(2,1)S(1)} all-to-all(bf16[16,48,128]{2,1,0:T(8,128)(2,1)S(1)} %get-tuple-element.42), channel_id=1, replica_groups=mesh['z'=16,'c'=2,'tp'=16] {'z'}, dimensions={0} | all-to-all | bytes 393216 | tf_op jit(solution)/shard_map/all_to_all | solution.py:427
  33.7 0.1 spread.1
  33.8 12.3 %all_to_all.36 = bf16[4,2,384,128]{3,2,1,0:T(8,128)(2,1)S(1)} all-to-all(bf16[4,2,384,128]{3,2,1,0:T(8,128)(2,1)S(1)} %spread.1), channel_id=1, replica_groups={{0,1,2,3},{4,5,6,7},{8,9,10,11},{12,13,14,15},{16,20,24,28},{17,21,25,2..., dimensions={0} | all-to-all | bytes 1572864 | tf_op jit(solution)/shard_map/all_to_all | solution.py:417
  46.1 0.7 broadcast_in_dim.12
  46.8 0.0 copy-start
  46.8 0.0 copy-start.1
  46.8 0.0 copy-start.2
  46.9 25.2 %all_to_all.37 = bf16[4,4,2,384,128]{4,3,2,1,0:T(8,128)(2,1)S(1)} all-to-all(bf16[4,4,2,384,128]{4,3,2,1,0:T(8,128)(2,1)S(1)} %broadcast_in_dim.12), channel_id=1, replica_groups={{0,4,8,12},{1,5,9,13},{2,6,10,14},{3,7,11,15},{16,17,18,19},{20,21,22,2..., dimensions={0} | all-to-all | bytes 6291456 | tf_op jit(solution)/shard_map/all_to_all | solution.py:417
  72.1 0.0 copy-done
  72.1 0.0 copy-done.1
  72.1 0.0 copy-done.2
  72.1 1.4 expert.1
  73.5 19.2 %all_to_all.38.part_ref = bf16[16,384,128]{2,1,0:T(8,128)(2,1)S(1)} all-to-all(bf16[16,384,128]{2,1,0:T(8,128)(2,1)S(1)} %get-tuple-element.43), channel_id=1, replica_groups=mesh['z'=16,'c'=2,'tp'=16] {'tp'}, dimensions={0} | all-to-all | bytes 3145728 | tf_op jit(solution)/shard_map/all_to_all | solution.py:427
  92.7 0.2 sums.1
  92.9 0.0 copy-start.3
  92.9 0.0 copy-start.4
  93.0 0.0 copy-start.5
  93.0 23.9 %all_to_all.39.own_ref = bf16[16,64,128]{2,1,0:T(8,128)(2,1)S(1)} all-to-all(bf16[16,64,128]{2,1,0:T(8,128)(2,1)S(1)} %sums.1), channel_id=1, replica_groups=mesh['z'=16,'c'=2,'tp'=16] {'z'}, dimensions={0} | all-to-all | bytes 524288 | tf_op jit(solution)/shard_map/all_to_all | solution.py:427
  116.9 10.5 %collective-permute-start = (bf16[16,64,128]{2,1,0:T(8,128)(2,1)S(1)}, bf16[16,64,128]{2,1,0:T(8,128)(2,1)S(1)}, u32[]{:S(2)}, u32[]{:S(2)}) collective-permute-start(bf16[16,64,128]{2,1,0:T(8,128)(2,1)S(1)} %all_to_all.39.own_ref), channel_id=1, source_target_pairs={{0,16},{16,0},{1,17},{17,1},{2,18},{18,2},{3,19},{19,3},{4,20},{20... | collective-permute-start | bytes 786440 | tf_op jit(solution)/shard_map/ppermute | solution.py:481
  127.4 2.2 %weights.1 = (bf16[2048,128]{1,0:T(8,128)(2,1)}, bf16[2048,128]{1,0:T(8,128)(2,1)}, bf16[128,2048]{1,0:T(8,128)(2,1)}) custom-call(bf16[16,2,384,128]{3,2,1,0:T(8,128)(2,1)S(1)} %bitcast.13, bf16[384,128]{1,0:T(8,128)(2,1)S(1)} %get-tuple-element.49.hid_ref, bf16[384,256]{1,0:T(8,128)(2,1)S(1)} %get-tuple-element.50.both_ref), custom_call_target="tpu_custom_call" | custom-call | flops 536870912 | bytes 1048576 | tf_op jit(solution)/shard_map/weights/pallas_call | solution.py:55
  129.6 0.0 collective-permute-done.other_ref
  129.6 0.3 resid.1
  129.9 13.9 %all_to_all.40.r_ref = bf16[16,128,128]{2,1,0:T(8,128)(2,1)S(1)} all-to-all(bf16[16,128,128]{2,1,0:T(8,128)(2,1)S(1)} %resid.1), channel_id=1, replica_groups=mesh['z'=16,'c'=2,'tp'=16] {'tp'}, dimensions={0} | all-to-all | bytes 1048576 | tf_op jit(solution)/shard_map/all_to_all | solution.py:427
  143.8 0.0 copy-done.3
  143.8 0.0 copy-done.4
  143.8 0.0 copy-done.5
  143.8 0.6 proj.1
  144.4 3.1 %collective-permute-start.1 = (bf16[18,64,128]{2,1,0:T(8,128)(2,1)S(1)}, bf16[18,64,128]{2,1,0:T(8,128)(2,1)S(1)}, u32[]{:S(2)}, u32[]{:S(2)}) collective-permute-start(bf16[18,64,128]{2,1,0:T(8,128)(2,1)S(1)} %get-tuple-element.60), channel_id=1, source_target_pairs={{0,16},{16,0},{1,17},{17,1},{2,18},{18,2},{3,19},{19,3},{4,20},{20... | collective-permute-start | bytes 884744 | tf_op jit(solution)/shard_map/ppermute | solution.py:505
  147.5 1.3 intra.1
  148.8 0.0 collective-permute-done.1.got_ref
  148.8 0.1 chip.1
  148.9 21.2 %all_to_all.41.got_ref = bf16[16,96,128]{2,1,0:T(8,128)(2,1)S(1)} all-to-all(bf16[16,96,128]{2,1,0:T(8,128)(2,1)S(1)} %get-tuple-element.67), channel_id=1, replica_groups=mesh['z'=16,'c'=2,'tp'=16] {'z'}, dimensions={0} | all-to-all | bytes 786432 | tf_op jit(solution)/shard_map/all_to_all | solution.py:427
  170.1 0.1 gather.1
  170.2 9.2 %all-gather.1 = f32[4,32,128]{2,1,0:T(8,128)S(1)} all-gather(f32[2,32,128]{2,1,0:T(8,128)S(1)} %gather.1), channel_id=3, replica_groups=mesh['z'=16,'c'=2,'tp'=16] {'c'}, dimensions={0}, use_global_device_ids=true | all-gather | bytes 98304 | tf_op jit(solution)/shard_map/all_gather | solution.py:521
  179.4 0.9 final.1
Async XLA Ops:
  46.8 25.2 %copy-start = (bf16[1,2048,128]{2,1,0:T(8,128)(2,1)S(1)}, bf16[1,2048,128]{2,1,0:T(8,128)(2,1)}, u32[]{:S(2)}) copy-start(bf16[1,2048,128]{2,1,0:T(8,128)(2,1)} %param.25) | copy-start | bytes 1572868
  46.8 25.2 %copy-start.1 = (bf16[1,2048,128]{2,1,0:T(8,128)(2,1)S(1)}, bf16[1,2048,128]{2,1,0:T(8,128)(2,1)}, u32[]{:S(2)}) copy-start(bf16[1,2048,128]{2,1,0:T(8,128)(2,1)} %param.26) | copy-start | bytes 1572868
  46.8 25.2 %copy-start.2 = (bf16[1,128,2048]{2,1,0:T(8,128)(2,1)S(1)}, bf16[1,128,2048]{2,1,0:T(8,128)(2,1)}, u32[]{:S(2)}) copy-start(bf16[1,128,2048]{2,1,0:T(8,128)(2,1)} %param.27) | copy-start | bytes 1572868
  92.9 50.9 %copy-start.3 = (bf16[2048,128]{1,0:T(8,128)(2,1)S(1)}, bf16[2048,128]{1,0:T(8,128)(2,1)}, u32[]{:S(2)}) copy-start(bf16[2048,128]{1,0:T(8,128)(2,1)} %p_ref.1) | copy-start | bytes 1572868
  92.9 50.9 %copy-start.4 = (bf16[64,128]{1,0:T(8,128)(2,1)S(1)}, bf16[64,128]{1,0:T(8,128)(2,1)}, u32[]{:S(2)}) copy-start(bf16[64,128]{1,0:T(8,128)(2,1)} %q_ref.3) | copy-start | bytes 49156
  93.0 50.9 %copy-start.5 = (bf16[128,128]{1,0:T(8,128)(2,1)S(1)}, bf16[128,128]{1,0:T(8,128)(2,1)}, u32[]{:S(2)}) copy-start(bf16[128,128]{1,0:T(8,128)(2,1)} %mixer_ref.1) | copy-start | bytes 98308
  116.9 12.7 %collective-permute-start = (bf16[16,64,128]{2,1,0:T(8,128)(2,1)S(1)}, bf16[16,64,128]{2,1,0:T(8,128)(2,1)S(1)}, u32[]{:S(2)}, u32[]{:S(2)}) collective-permute-start(bf16[16,64,128]{2,1,0:T(8,128)(2,1)S(1)} %all_to_all.39.own_ref), channel_id=1, source_target_pairs={{0,16},{16,0},{1,17},{17,1},{2,18},{18,2},{3,19},{19,3},{4,20},{20... | collective-permute-start | bytes 786440 | tf_op jit(solution)/shard_map/ppermute | solution.py:481
  144.4 4.4 %collective-permute-start.1 = (bf16[18,64,128]{2,1,0:T(8,128)(2,1)S(1)}, bf16[18,64,128]{2,1,0:T(8,128)(2,1)S(1)}, u32[]{:S(2)}, u32[]{:S(2)}) collective-permute-start(bf16[18,64,128]{2,1,0:T(8,128)(2,1)S(1)} %get-tuple-element.60), channel_id=1, source_target_pairs={{0,16},{16,0},{1,17},{17,1},{2,18},{18,2},{3,19},{19,3},{4,20},{20... | collective-permute-start | bytes 884744 | tf_op jit(solution)/shard_map/ppermute | solution.py:505

commit v9 on v7

--- a/solution.py
+++ b/solution.py
@@ -211,6 +211,14 @@
     )
 
 
+def copies_kernel(got_ref, out_ref):
+    for j in range(4):
+        for kind in range(2):
+            part = got_ref[j, kind]
+            for k in range(4):
+                out_ref[k, j, kind] = part
+
+
 def spread_kernel(got_ref, rows_ref):
     for z in range(NZ):
         for kind in range(2):
@@ -434,10 +442,6 @@
     )
 
 
-def to_all(shard, axis, sets):
-    return within(jnp.broadcast_to(shard, (len(sets[0]), *shard.shape)), axis, sets)
-
-
 def exchange(blocks, axis):
     return lax.all_to_all(blocks, axis, split_axis=0, concat_axis=0, tiled=True)
 
@@ -480,7 +484,9 @@
     rows = exchange(rows, "z")
     copies = call(spread_kernel, arr((4, 2, NZ * 2 * CAP, COL), BF), (rows,), "spread")
     rows = within(copies, ("c", "tp"), groups(4, 1, 1, 4))
-    rows = to_all(rows.reshape(4, 2, NZ * 2 * CAP, COL), ("c", "tp"), groups(1, 4, 4, 1))
+    rows = rows.reshape(4, 2, NZ * 2 * CAP, COL)
+    copies = call(copies_kernel, arr((4, *rows.shape), BF), (rows,), "copies", 12)
+    rows = within(copies, ("c", "tp"), groups(1, 4, 4, 1))
     rows = rows.reshape(NT, 2, NZ * 2 * CAP, COL)
     shares, hidden, both = call(
         expert_kernel,

time: 180 us -> 180 us (level)
    pallas_call x12 -> x13, Pallas kernels: 9.02 us -> 9.4 us  [call(): pl.pallas_call(kernel, out_shape=outs, in_specs=[hbm()] * stay + [vmem()]...]
where the time goes in v9:
time: 180 us
  blocking collectives  156 us (87%)
  starting transfers between devices  13.6 us (8%)
  Pallas kernels  9.4 us (5%)
    all_to_all x5, blocking collectives, exchange(): return lax.all_to_all(blocks, axis, split_axis=0, concat_axis=0, tiled=True)  100 us
    all_to_all x2, blocking collectives, within(): lax.all_to_all(blocks, axis, split_axis=0, concat_axis=0, axis_index_grou...  37.5 us
    ppermute x1, starting transfers between devices, on_device(): other = lax.ppermute(own, 'c', SWAP)  10.5 us
    pallas_call x13, Pallas kernels, call(): pl.pallas_call(kernel, out_shape=outs, in_specs=[hbm()] * stay + [vmem()]...  9.4 us
    all_gather x1, blocking collectives, on_device(): far = lax.all_gather(far, 'c')  9.16 us
    all_gather x1, blocking collectives, on_device(): held = lax.all_gather(held, 'c')  8.67 us
  transfers between devices with their start and end apart: 2, of which 0 were waited for; matrix products, arithmetic and copies ran while one was open for 0% of the time, Pallas kernels for 2%

profile of v9, /device:TPU:1, one launch (start us, length us, event | category | flops | bytes accessed | tf_op | source)
XLA Modules:
  0.0 179.6 jit_solution(17051475940317032715)
XLA Ops:
  0.6 1.6 load.1
  2.2 8.7 %all-gather = bf16[928,128]{1,0:T(8,128)(2,1)S(1)} all-gather(bf16[464,128]{1,0:T(8,128)(2,1)} %load.1), channel_id=2, replica_groups=mesh['z'=16,'c'=2,'tp'=16] {'c'}, dimensions={0}, use_global_device_ids=true | all-gather | bytes 356352 | tf_op jit(solution)/shard_map/all_gather | solution.py:474
  10.9 0.5 pack.1
  11.5 22.2 %all_to_all.35.got_ref = bf16[16,48,128]{2,1,0:T(8,128)(2,1)S(1)} all-to-all(bf16[16,48,128]{2,1,0:T(8,128)(2,1)S(1)} %get-tuple-element.42), channel_id=1, replica_groups=mesh['z'=16,'c'=2,'tp'=16] {'z'}, dimensions={0} | all-to-all | bytes 393216 | tf_op jit(solution)/shard_map/all_to_all | solution.py:446
  33.7 0.1 spread.1
  33.8 12.2 %all_to_all.36.got_ref = bf16[4,2,384,128]{3,2,1,0:T(8,128)(2,1)S(1)} all-to-all(bf16[4,2,384,128]{3,2,1,0:T(8,128)(2,1)S(1)} %spread.1), channel_id=1, replica_groups={{0,4,8,12},{1,5,9,13},{2,6,10,14},{3,7,11,15},{16,17,18,19},{20,21,22,2..., dimensions={0} | all-to-all | bytes 1572864 | tf_op jit(solution)/shard_map/all_to_all | solution.py:440
  45.9 0.4 copies.1
  46.3 0.0 copy-start
  46.4 0.0 copy-start.1
  46.4 0.0 copy-start.2
  46.4 25.4 %all_to_all.37 = bf16[4,4,2,384,128]{4,3,2,1,0:T(8,128)(2,1)S(1)} all-to-all(bf16[4,4,2,384,128]{4,3,2,1,0:T(8,128)(2,1)S(1)} %copies.1), channel_id=1, replica_groups={{0,1,2,3},{4,5,6,7},{8,9,10,11},{12,13,14,15},{16,20,24,28},{17,21,25,2..., dimensions={0} | all-to-all | bytes 6291456 | tf_op jit(solution)/shard_map/all_to_all | solution.py:440
  71.8 0.0 copy-done
  71.8 0.0 copy-done.1
  71.8 0.0 copy-done.2
  71.8 1.4 expert.1
  73.2 19.2 %all_to_all.38.part_ref = bf16[16,384,128]{2,1,0:T(8,128)(2,1)S(1)} all-to-all(bf16[16,384,128]{2,1,0:T(8,128)(2,1)S(1)} %get-tuple-element.43), channel_id=1, replica_groups=mesh['z'=16,'c'=2,'tp'=16] {'tp'}, dimensions={0} | all-to-all | bytes 3145728 | tf_op jit(solution)/shard_map/all_to_all | solution.py:446
  92.4 0.2 sums.1
  92.6 0.0 copy-start.3
  92.6 0.0 copy-start.4
  92.6 0.0 copy-start.5
  92.6 23.9 %all_to_all.39.own_ref = bf16[16,64,128]{2,1,0:T(8,128)(2,1)S(1)} all-to-all(bf16[16,64,128]{2,1,0:T(8,128)(2,1)S(1)} %sums.1), channel_id=1, replica_groups=mesh['z'=16,'c'=2,'tp'=16] {'z'}, dimensions={0} | all-to-all | bytes 524288 | tf_op jit(solution)/shard_map/all_to_all | solution.py:446
  116.6 10.5 %collective-permute-start = (bf16[16,64,128]{2,1,0:T(8,128)(2,1)S(1)}, bf16[16,64,128]{2,1,0:T(8,128)(2,1)S(1)}, u32[]{:S(2)}, u32[]{:S(2)}) collective-permute-start(bf16[16,64,128]{2,1,0:T(8,128)(2,1)S(1)} %all_to_all.39.own_ref), channel_id=1, source_target_pairs={{0,16},{16,0},{1,17},{17,1},{2,18},{18,2},{3,19},{19,3},{4,20},{20... | collective-permute-start | bytes 786440 | tf_op jit(solution)/shard_map/ppermute | solution.py:502
  127.1 1.9 %weights.1 = (bf16[2048,128]{1,0:T(8,128)(2,1)}, bf16[2048,128]{1,0:T(8,128)(2,1)}, bf16[128,2048]{1,0:T(8,128)(2,1)}) custom-call(bf16[16,2,384,128]{3,2,1,0:T(8,128)(2,1)S(1)} %bitcast.13, bf16[384,128]{1,0:T(8,128)(2,1)S(1)} %get-tuple-element.49.hid_ref, bf16[384,256]{1,0:T(8,128)(2,1)S(1)} %get-tuple-element.50.both_ref), custom_call_target="tpu_custom_call" | custom-call | flops 536870912 | bytes 1048576 | tf_op jit(solution)/shard_map/weights/pallas_call | solution.py:55
  129.0 0.0 collective-permute-done.other_ref
  129.0 0.3 resid.1
  129.3 13.9 %all_to_all.40.r_ref = bf16[16,128,128]{2,1,0:T(8,128)(2,1)S(1)} all-to-all(bf16[16,128,128]{2,1,0:T(8,128)(2,1)S(1)} %resid.1), channel_id=1, replica_groups=mesh['z'=16,'c'=2,'tp'=16] {'tp'}, dimensions={0} | all-to-all | bytes 1048576 | tf_op jit(solution)/shard_map/all_to_all | solution.py:446
  143.2 0.0 copy-done.3
  143.2 0.0 copy-done.4
  143.2 0.0 copy-done.5
  143.3 0.6 proj.1
  143.9 3.1 %collective-permute-start.1 = (bf16[18,64,128]{2,1,0:T(8,128)(2,1)S(1)}, bf16[18,64,128]{2,1,0:T(8,128)(2,1)S(1)}, u32[]{:S(2)}, u32[]{:S(2)}) collective-permute-start(bf16[18,64,128]{2,1,0:T(8,128)(2,1)S(1)} %get-tuple-element.60), channel_id=1, source_target_pairs={{0,16},{16,0},{1,17},{17,1},{2,18},{18,2},{3,19},{19,3},{4,20},{20... | collective-permute-start | bytes 884744 | tf_op jit(solution)/shard_map/ppermute | solution.py:529
  147.0 1.3 intra.1
  148.3 0.0 collective-permute-done.1.got_ref
  148.3 0.1 chip.1
  148.4 21.2 %all_to_all.41.got_ref = bf16[16,96,128]{2,1,0:T(8,128)(2,1)S(1)} all-to-all(bf16[16,96,128]{2,1,0:T(8,128)(2,1)S(1)} %get-tuple-element.67), channel_id=1, replica_groups=mesh['z'=16,'c'=2,'tp'=16] {'z'}, dimensions={0} | all-to-all | bytes 786432 | tf_op jit(solution)/shard_map/all_to_all | solution.py:446
  169.6 0.1 gather.1
  169.6 9.2 %all-gather.1 = f32[4,32,128]{2,1,0:T(8,128)S(1)} all-gather(f32[2,32,128]{2,1,0:T(8,128)S(1)} %gather.1), channel_id=3, replica_groups=mesh['z'=16,'c'=2,'tp'=16] {'c'}, dimensions={0}, use_global_device_ids=true | all-gather | bytes 98304 | tf_op jit(solution)/shard_map/all_gather | solution.py:545
  178.8 0.9 final.1
Async XLA Ops:
  46.3 25.4 %copy-start = (bf16[1,2048,128]{2,1,0:T(8,128)(2,1)S(1)}, bf16[1,2048,128]{2,1,0:T(8,128)(2,1)}, u32[]{:S(2)}) copy-start(bf16[1,2048,128]{2,1,0:T(8,128)(2,1)} %param.25) | copy-start | bytes 1572868
  46.4 25.4 %copy-start.1 = (bf16[1,2048,128]{2,1,0:T(8,128)(2,1)S(1)}, bf16[1,2048,128]{2,1,0:T(8,128)(2,1)}, u32[]{:S(2)}) copy-start(bf16[1,2048,128]{2,1,0:T(8,128)(2,1)} %param.26) | copy-start | bytes 1572868
  46.4 25.4 %copy-start.2 = (bf16[1,128,2048]{2,1,0:T(8,128)(2,1)S(1)}, bf16[1,128,2048]{2,1,0:T(8,128)(2,1)}, u32[]{:S(2)}) copy-start(bf16[1,128,2048]{2,1,0:T(8,128)(2,1)} %param.27) | copy-start | bytes 1572868
  92.6 50.6 %copy-start.3 = (bf16[2048,128]{1,0:T(8,128)(2,1)S(1)}, bf16[2048,128]{1,0:T(8,128)(2,1)}, u32[]{:S(2)}) copy-start(bf16[2048,128]{1,0:T(8,128)(2,1)} %p_ref.1) | copy-start | bytes 1572868
  92.6 50.6 %copy-start.4 = (bf16[64,128]{1,0:T(8,128)(2,1)S(1)}, bf16[64,128]{1,0:T(8,128)(2,1)}, u32[]{:S(2)}) copy-start(bf16[64,128]{1,0:T(8,128)(2,1)} %q_ref.3) | copy-start | bytes 49156
  92.6 50.6 %copy-start.5 = (bf16[128,128]{1,0:T(8,128)(2,1)S(1)}, bf16[128,128]{1,0:T(8,128)(2,1)}, u32[]{:S(2)}) copy-start(bf16[128,128]{1,0:T(8,128)(2,1)} %mixer_ref.1) | copy-start | bytes 98308
  116.6 12.4 %collective-permute-start = (bf16[16,64,128]{2,1,0:T(8,128)(2,1)S(1)}, bf16[16,64,128]{2,1,0:T(8,128)(2,1)S(1)}, u32[]{:S(2)}, u32[]{:S(2)}) collective-permute-start(bf16[16,64,128]{2,1,0:T(8,128)(2,1)S(1)} %all_to_all.39.own_ref), channel_id=1, source_target_pairs={{0,16},{16,0},{1,17},{17,1},{2,18},{18,2},{3,19},{19,3},{4,20},{20... | collective-permute-start | bytes 786440 | tf_op jit(solution)/shard_map/ppermute | solution.py:502
  143.9 4.4 %collective-permute-start.1 = (bf16[18,64,128]{2,1,0:T(8,128)(2,1)S(1)}, bf16[18,64,128]{2,1,0:T(8,128)(2,1)S(1)}, u32[]{:S(2)}, u32[]{:S(2)}) collective-permute-start(bf16[18,64,128]{2,1,0:T(8,128)(2,1)S(1)} %get-tuple-element.60), channel_id=1, source_target_pairs={{0,16},{16,0},{1,17},{17,1},{2,18},{18,2},{3,19},{19,3},{4,20},{20... | collective-permute-start | bytes 884744 | tf_op jit(solution)/shard_map/ppermute | solution.py:529

commit v10 on v9

--- a/solution.py
+++ b/solution.py
@@ -133,24 +133,38 @@
 
 def load_kernel(
     ids_in, gw_in, ew_in, cot_in, inp_in, rate_in, k_in, v_in,
-    out_ref, ids_ref, gw_ref, ew_ref, rate_ref, sems,
+    out, held_ref, ids_ref, gw_ref, ew_ref, rate_ref, sems, out_sems,
 ):
     here = pl.ds(pl.multiple_of(spot("tp") * COL, COL), COL)
-    fetch(
-        (ids_in, gw_in, ew_in, cot_in.at[:, here], inp_in.at[:, here], rate_in, k_in, v_in),
-        (
-            ids_ref, gw_ref, ew_ref, out_ref.at[pl.ds(COT, TOK)], out_ref.at[pl.ds(INP, TOK)],
-            rate_ref, out_ref.at[pl.ds(KEY, KD)], out_ref.at[pl.ds(VALUE, VD)],
-        ),
-        sems,
-    )
+    bulk = [pl.ds(COT, TOK), pl.ds(INP, TOK), pl.ds(KEY, KD), pl.ds(VALUE, VD)]
+    sources = (cot_in.at[:, here], inp_in.at[:, here], k_in, v_in, ids_in, gw_in, ew_in, rate_in)
+    targets = [held_ref.at[part] for part in bulk] + [ids_ref, gw_ref, ew_ref, rate_ref]
+    copies = [
+        pltpu.make_async_copy(src, dst, sems.at[n])
+        for n, (src, dst) in enumerate(zip(sources, targets))
+    ]
+    small = pl.ds(ROUTE, HELD - ROUTE)
+    leaving = [
+        pltpu.make_async_copy(held_ref.at[part], out.at[part], out_sems.at[n])
+        for n, part in enumerate(bulk + [small])
+    ]
+    for copy in copies:
+        copy.start()
+    for copy, leave in zip(copies[:4], leaving):
+        copy.wait()
+        leave.start()
+    for copy in copies[4:]:
+        copy.wait()
     weights = gw_ref[...] * ew_ref[...]
     none = jnp.zeros((2, TOK), F32)
-    out_ref[ROUTE:HELD, :] = jnp.concatenate(
+    held_ref[ROUTE:HELD, :] = jnp.concatenate(
         [in_pieces(weights[0:1, :]), in_pieces(weights[1:2, :]), none]
         + [in_pieces(rate_ref[...]), ids_ref[...].astype(F32), none, none[0:1, :]],
         axis=0,
     ).astype(BF)
+    leaving[4].start()
+    for leave in leaving:
+        leave.wait()
 
 
 def pack_kernel(g_ref, rows_ref, picks_ref, small_ref, mine_ref):
@@ -413,11 +427,20 @@
     state_ref[1] = late
 
 
-def final_kernel(far_ref, near_ref, part_ref, got_ref, proj_ref, gk_ref, gv_ref):
+def final_kernel(
+    far_ref, near_ref, part_ref, got_ref, proj_out, gk_out, gv_out, proj_ref, gk_ref, gv_ref, sems
+):
+    copies = [
+        pltpu.make_async_copy(src, dst, sems.at[n])
+        for n, (src, dst) in enumerate(
+            ((proj_ref, proj_out), (gk_ref, gk_out), (gv_ref, gv_out))
+        )
+    ]
     share = jnp.zeros((64, COL), F32)
     for z in range(NZ):
         share = share + got_ref[z, 0:64, :].astype(F32)
     proj_ref[...] = share
+    copies[0].start()
     early, late = at_block(
         jnp.concatenate([far_ref[0, 0], far_ref[1, 0]], axis=0),
         jnp.concatenate([far_ref[0, 1], far_ref[1, 1]], axis=0),
@@ -426,8 +449,12 @@
     )
     low, high = part_ref[384:385, :], part_ref[385:386, :]
     key, value = part_ref[192:256, :].astype(BF), part_ref[256:384, :].astype(BF)
+    gv_ref[...] = part_ref[64:192, :] + low * exact(early, key, TN) + high * exact(late, key, TN)
+    copies[2].start()
     gk_ref[...] = part_ref[0:64, :] + low * exact(early, value) + high * exact(late, value)
-    gv_ref[...] = part_ref[64:192, :] + low * exact(early, key, TN) + high * exact(late, key, TN)
+    copies[1].start()
+    for copy in copies:
+        copy.wait()
 
 
 def groups(step, stride, step_other, stride_other):
@@ -467,9 +494,11 @@
         60,
         stay=8,
         scratch=[
-            pltpu.VMEM((2, TOK), jnp.int32), pltpu.VMEM((1, TOK), F32), pltpu.VMEM((2, TOK), F32),
-            pltpu.VMEM((1, TOK), F32), pltpu.SemaphoreType.DMA((8,)),
+            pltpu.VMEM((HELD, COL), BF), pltpu.VMEM((2, TOK), jnp.int32), pltpu.VMEM((1, TOK), F32),
+            pltpu.VMEM((2, TOK), F32), pltpu.VMEM((1, TOK), F32),
+            pltpu.SemaphoreType.DMA((8,)), pltpu.SemaphoreType.DMA((5,)),
         ],
+        out=hbm,
     )
     held = lax.all_gather(held, "c")
     rows, picks, small, mine = call(
@@ -543,11 +572,14 @@
     chip = exchange(chip, "z")
     far = call(gather_kernel, arr((2, 32, COL), F32), (chip, weight), "gather")
     far = lax.all_gather(far, "c")
+    shapes = [arr((64, COL), F32), arr((KD, TOK), F32), arr((VD, TOK), F32)]
     grad_proj, grad_keys, grad_values = call(
         final_kernel,
-        [arr((64, COL), F32), arr((KD, TOK), F32), arr((VD, TOK), F32)],
+        shapes,
         (far, near, part, chip),
         "final",
+        scratch=[pltpu.VMEM(a.shape, F32) for a in shapes] + [pltpu.SemaphoreType.DMA((3,))],
+        out=hbm,
     )
     return (
         grad_gate[None], grad_up[None], grad_down[None],

time: 180 us -> 180 us (level)
  no operation moved by 1% of the time
where the time goes in v10:
time: 180 us
  blocking collectives  156 us (87%)
  starting transfers between devices  13.6 us (8%)
  Pallas kernels  9.39 us (5%)
    all_to_all x5, blocking collectives, exchange(): return lax.all_to_all(blocks, axis, split_axis=0, concat_axis=0, tiled=True)  100 us
    all_to_all x2, blocking collectives, within(): lax.all_to_all(blocks, axis, split_axis=0, concat_axis=0, axis_index_grou...  37.5 us
    ppermute x1, starting transfers between devices, on_device(): other = lax.ppermute(own, 'c', SWAP)  10.5 us
    pallas_call x13, Pallas kernels, call(): pl.pallas_call(kernel, out_shape=outs, in_specs=[hbm()] * stay + [vmem()]...  9.39 us
    all_gather x1, blocking collectives, on_device(): far = lax.all_gather(far, 'c')  9.16 us
    all_gather x1, blocking collectives, on_device(): held = lax.all_gather(held, 'c')  8.67 us
  transfers between devices with their start and end apart: 2, of which 0 were waited for; matrix products, arithmetic and copies ran while one was open for 0% of the time, Pallas kernels for 2%

profile of v10, /device:TPU:1, one launch (start us, length us, event | category | flops | bytes accessed | tf_op | source)
XLA Modules:
  0.0 179.6 jit_solution(9969448784779019347)
XLA Ops:
  0.6 1.5 load.1
  2.2 8.7 %all-gather = bf16[928,128]{1,0:T(8,128)(2,1)S(1)} all-gather(bf16[464,128]{1,0:T(8,128)(2,1)} %load.1), channel_id=2, replica_groups=mesh['z'=16,'c'=2,'tp'=16] {'c'}, dimensions={0}, use_global_device_ids=true | all-gather | bytes 356352 | tf_op jit(solution)/shard_map/all_gather | solution.py:503
  10.9 0.5 pack.1
  11.4 22.2 %all_to_all.35.got_ref = bf16[16,48,128]{2,1,0:T(8,128)(2,1)S(1)} all-to-all(bf16[16,48,128]{2,1,0:T(8,128)(2,1)S(1)} %get-tuple-element.42), channel_id=1, replica_groups=mesh['z'=16,'c'=2,'tp'=16] {'z'}, dimensions={0} | all-to-all | bytes 393216 | tf_op jit(solution)/shard_map/all_to_all | solution.py:473
  33.6 0.1 spread.1
  33.7 12.2 %all_to_all.36.got_ref = bf16[4,2,384,128]{3,2,1,0:T(8,128)(2,1)S(1)} all-to-all(bf16[4,2,384,128]{3,2,1,0:T(8,128)(2,1)S(1)} %spread.1), channel_id=1, replica_groups={{0,4,8,12},{1,5,9,13},{2,6,10,14},{3,7,11,15},{16,17,18,19},{20,21,22,2..., dimensions={0} | all-to-all | bytes 1572864 | tf_op jit(solution)/shard_map/all_to_all | solution.py:467
  45.9 0.4 copies.1
  46.3 0.0 copy-start
  46.3 0.0 copy-start.1
  46.3 0.0 copy-start.2
  46.3 25.4 %all_to_all.37 = bf16[4,4,2,384,128]{4,3,2,1,0:T(8,128)(2,1)S(1)} all-to-all(bf16[4,4,2,384,128]{4,3,2,1,0:T(8,128)(2,1)S(1)} %copies.1), channel_id=1, replica_groups={{0,1,2,3},{4,5,6,7},{8,9,10,11},{12,13,14,15},{16,20,24,28},{17,21,25,2..., dimensions={0} | all-to-all | bytes 6291456 | tf_op jit(solution)/shard_map/all_to_all | solution.py:467
  71.7 0.0 copy-done
  71.7 0.0 copy-done.1
  71.7 0.0 copy-done.2
  71.7 1.4 expert.1
  73.2 19.2 %all_to_all.38.part_ref = bf16[16,384,128]{2,1,0:T(8,128)(2,1)S(1)} all-to-all(bf16[16,384,128]{2,1,0:T(8,128)(2,1)S(1)} %get-tuple-element.43), channel_id=1, replica_groups=mesh['z'=16,'c'=2,'tp'=16] {'tp'}, dimensions={0} | all-to-all | bytes 3145728 | tf_op jit(solution)/shard_map/all_to_all | solution.py:473
  92.3 0.2 sums.1
  92.5 0.0 copy-start.3
  92.6 0.0 copy-start.4
  92.6 0.0 copy-start.5
  92.6 23.9 %all_to_all.39.own_ref = bf16[16,64,128]{2,1,0:T(8,128)(2,1)S(1)} all-to-all(bf16[16,64,128]{2,1,0:T(8,128)(2,1)S(1)} %sums.1), channel_id=1, replica_groups=mesh['z'=16,'c'=2,'tp'=16] {'z'}, dimensions={0} | all-to-all | bytes 524288 | tf_op jit(solution)/shard_map/all_to_all | solution.py:473
  116.5 10.5 %collective-permute-start = (bf16[16,64,128]{2,1,0:T(8,128)(2,1)S(1)}, bf16[16,64,128]{2,1,0:T(8,128)(2,1)S(1)}, u32[]{:S(2)}, u32[]{:S(2)}) collective-permute-start(bf16[16,64,128]{2,1,0:T(8,128)(2,1)S(1)} %all_to_all.39.own_ref), channel_id=1, source_target_pairs={{0,16},{16,0},{1,17},{17,1},{2,18},{18,2},{3,19},{19,3},{4,20},{20... | collective-permute-start | bytes 786440 | tf_op jit(solution)/shard_map/ppermute | solution.py:531
  127.1 1.9 %weights.1 = (bf16[2048,128]{1,0:T(8,128)(2,1)}, bf16[2048,128]{1,0:T(8,128)(2,1)}, bf16[128,2048]{1,0:T(8,128)(2,1)}) custom-call(bf16[16,2,384,128]{3,2,1,0:T(8,128)(2,1)S(1)} %bitcast.13, bf16[384,128]{1,0:T(8,128)(2,1)S(1)} %get-tuple-element.49.hid_ref, bf16[384,256]{1,0:T(8,128)(2,1)S(1)} %get-tuple-element.50.both_ref), custom_call_target="tpu_custom_call" | custom-call | flops 536870912 | bytes 1048576 | tf_op jit(solution)/shard_map/weights/pallas_call | solution.py:55
  128.9 0.0 collective-permute-done.other_ref
  129.0 0.3 resid.1
  129.2 13.9 %all_to_all.40.r_ref = bf16[16,128,128]{2,1,0:T(8,128)(2,1)S(1)} all-to-all(bf16[16,128,128]{2,1,0:T(8,128)(2,1)S(1)} %resid.1), channel_id=1, replica_groups=mesh['z'=16,'c'=2,'tp'=16] {'tp'}, dimensions={0} | all-to-all | bytes 1048576 | tf_op jit(solution)/shard_map/all_to_all | solution.py:473
  143.2 0.0 copy-done.3
  143.2 0.0 copy-done.4
  143.2 0.0 copy-done.5
  143.2 0.6 proj.1
  143.8 3.1 %collective-permute-start.1 = (bf16[18,64,128]{2,1,0:T(8,128)(2,1)S(1)}, bf16[18,64,128]{2,1,0:T(8,128)(2,1)S(1)}, u32[]{:S(2)}, u32[]{:S(2)}) collective-permute-start(bf16[18,64,128]{2,1,0:T(8,128)(2,1)S(1)} %get-tuple-element.60), channel_id=1, source_target_pairs={{0,16},{16,0},{1,17},{17,1},{2,18},{18,2},{3,19},{19,3},{4,20},{20... | collective-permute-start | bytes 884744 | tf_op jit(solution)/shard_map/ppermute | solution.py:558
  146.9 1.3 intra.1
  148.2 0.0 collective-permute-done.1.got_ref
  148.2 0.1 chip.1
  148.3 21.2 %all_to_all.41.got_ref = bf16[16,96,128]{2,1,0:T(8,128)(2,1)S(1)} all-to-all(bf16[16,96,128]{2,1,0:T(8,128)(2,1)S(1)} %get-tuple-element.67), channel_id=1, replica_groups=mesh['z'=16,'c'=2,'tp'=16] {'z'}, dimensions={0} | all-to-all | bytes 786432 | tf_op jit(solution)/shard_map/all_to_all | solution.py:473
  169.5 0.1 gather.1
  169.6 9.2 %all-gather.1 = f32[4,32,128]{2,1,0:T(8,128)S(1)} all-gather(f32[2,32,128]{2,1,0:T(8,128)S(1)} %gather.1), channel_id=3, replica_groups=mesh['z'=16,'c'=2,'tp'=16] {'c'}, dimensions={0}, use_global_device_ids=true | all-gather | bytes 98304 | tf_op jit(solution)/shard_map/all_gather | solution.py:574
  178.7 0.9 final.1
Async XLA Ops:
  46.3 25.4 %copy-start = (bf16[1,2048,128]{2,1,0:T(8,128)(2,1)S(1)}, bf16[1,2048,128]{2,1,0:T(8,128)(2,1)}, u32[]{:S(2)}) copy-start(bf16[1,2048,128]{2,1,0:T(8,128)(2,1)} %param.25) | copy-start | bytes 1572868
  46.3 25.4 %copy-start.1 = (bf16[1,2048,128]{2,1,0:T(8,128)(2,1)S(1)}, bf16[1,2048,128]{2,1,0:T(8,128)(2,1)}, u32[]{:S(2)}) copy-start(bf16[1,2048,128]{2,1,0:T(8,128)(2,1)} %param.26) | copy-start | bytes 1572868
  46.3 25.4 %copy-start.2 = (bf16[1,128,2048]{2,1,0:T(8,128)(2,1)S(1)}, bf16[1,128,2048]{2,1,0:T(8,128)(2,1)}, u32[]{:S(2)}) copy-start(bf16[1,128,2048]{2,1,0:T(8,128)(2,1)} %param.27) | copy-start | bytes 1572868
  92.5 50.6 %copy-start.3 = (bf16[2048,128]{1,0:T(8,128)(2,1)S(1)}, bf16[2048,128]{1,0:T(8,128)(2,1)}, u32[]{:S(2)}) copy-start(bf16[2048,128]{1,0:T(8,128)(2,1)} %p_ref.1) | copy-start | bytes 1572868
  92.6 50.6 %copy-start.4 = (bf16[64,128]{1,0:T(8,128)(2,1)S(1)}, bf16[64,128]{1,0:T(8,128)(2,1)}, u32[]{:S(2)}) copy-start(bf16[64,128]{1,0:T(8,128)(2,1)} %q_ref.3) | copy-start | bytes 49156
  92.6 50.6 %copy-start.5 = (bf16[128,128]{1,0:T(8,128)(2,1)S(1)}, bf16[128,128]{1,0:T(8,128)(2,1)}, u32[]{:S(2)}) copy-start(bf16[128,128]{1,0:T(8,128)(2,1)} %mixer_ref.1) | copy-start | bytes 98308
  116.5 12.4 %collective-permute-start = (bf16[16,64,128]{2,1,0:T(8,128)(2,1)S(1)}, bf16[16,64,128]{2,1,0:T(8,128)(2,1)S(1)}, u32[]{:S(2)}, u32[]{:S(2)}) collective-permute-start(bf16[16,64,128]{2,1,0:T(8,128)(2,1)S(1)} %all_to_all.39.own_ref), channel_id=1, source_target_pairs={{0,16},{16,0},{1,17},{17,1},{2,18},{18,2},{3,19},{19,3},{4,20},{20... | collective-permute-start | bytes 786440 | tf_op jit(solution)/shard_map/ppermute | solution.py:531
  143.8 4.4 %collective-permute-start.1 = (bf16[18,64,128]{2,1,0:T(8,128)(2,1)S(1)}, bf16[18,64,128]{2,1,0:T(8,128)(2,1)S(1)}, u32[]{:S(2)}, u32[]{:S(2)}) collective-permute-start(bf16[18,64,128]{2,1,0:T(8,128)(2,1)S(1)} %get-tuple-element.60), channel_id=1, source_target_pairs={{0,16},{16,0},{1,17},{17,1},{2,18},{18,2},{3,19},{19,3},{4,20},{20... | collective-permute-start | bytes 884744 | tf_op jit(solution)/shard_map/ppermute | solution.py:558

commit v11 on v10

--- a/solution.py
+++ b/solution.py
@@ -427,20 +427,11 @@
     state_ref[1] = late
 
 
-def final_kernel(
-    far_ref, near_ref, part_ref, got_ref, proj_out, gk_out, gv_out, proj_ref, gk_ref, gv_ref, sems
-):
-    copies = [
-        pltpu.make_async_copy(src, dst, sems.at[n])
-        for n, (src, dst) in enumerate(
-            ((proj_ref, proj_out), (gk_ref, gk_out), (gv_ref, gv_out))
-        )
-    ]
+def final_kernel(far_ref, near_ref, part_ref, got_ref, proj_ref, gk_ref, gv_ref):
     share = jnp.zeros((64, COL), F32)
     for z in range(NZ):
         share = share + got_ref[z, 0:64, :].astype(F32)
     proj_ref[...] = share
-    copies[0].start()
     early, late = at_block(
         jnp.concatenate([far_ref[0, 0], far_ref[1, 0]], axis=0),
         jnp.concatenate([far_ref[0, 1], far_ref[1, 1]], axis=0),
@@ -449,12 +440,8 @@
     )
     low, high = part_ref[384:385, :], part_ref[385:386, :]
     key, value = part_ref[192:256, :].astype(BF), part_ref[256:384, :].astype(BF)
+    gk_ref[...] = part_ref[0:64, :] + low * exact(early, value) + high * exact(late, value)
     gv_ref[...] = part_ref[64:192, :] + low * exact(early, key, TN) + high * exact(late, key, TN)
-    copies[2].start()
-    gk_ref[...] = part_ref[0:64, :] + low * exact(early, value) + high * exact(late, value)
-    copies[1].start()
-    for copy in copies:
-        copy.wait()
 
 
 def groups(step, stride, step_other, stride_other):
@@ -572,14 +559,11 @@
     chip = exchange(chip, "z")
     far = call(gather_kernel, arr((2, 32, COL), F32), (chip, weight), "gather")
     far = lax.all_gather(far, "c")
-    shapes = [arr((64, COL), F32), arr((KD, TOK), F32), arr((VD, TOK), F32)]
     grad_proj, grad_keys, grad_values = call(
         final_kernel,
-        shapes,
+        [arr((64, COL), F32), arr((KD, TOK), F32), arr((VD, TOK), F32)],
         (far, near, part, chip),
         "final",
-        scratch=[pltpu.VMEM(a.shape, F32) for a in shapes] + [pltpu.SemaphoreType.DMA((3,))],
-        out=hbm,
     )
     return (
         grad_gate[None], grad_up[None], grad_down[None],

time: 180 us -> 180 us (level)
  no operation moved by 1% of the time
where the time goes in v11:
time: 180 us
  blocking collectives  156 us (87%)
  starting transfers between devices  13.6 us (8%)
  Pallas kernels  9.35 us (5%)
    all_to_all x5, blocking collectives, exchange(): return lax.all_to_all(blocks, axis, split_axis=0, concat_axis=0, tiled=True)  100 us
    all_to_all x2, blocking collectives, within(): lax.all_to_all(blocks, axis, split_axis=0, concat_axis=0, axis_index_grou...  37.5 us
    ppermute x1, starting transfers between devices, on_device(): other = lax.ppermute(own, 'c', SWAP)  10.5 us
    pallas_call x13, Pallas kernels, call(): pl.pallas_call(kernel, out_shape=outs, in_specs=[hbm()] * stay + [vmem()]...  9.35 us
    all_gather x1, blocking collectives, on_device(): far = lax.all_gather(far, 'c')  9.16 us
    all_gather x1, blocking collectives, on_device(): held = lax.all_gather(held, 'c')  8.67 us
  transfers between devices with their start and end apart: 2, of which 0 were waited for; matrix products, arithmetic and copies ran while one was open for 0% of the time, Pallas kernels for 2%

profile of v11, /device:TPU:1, one launch (start us, length us, event | category | flops | bytes accessed | tf_op | source)
XLA Modules:
  0.0 179.6 jit_solution(178377146641729305)
XLA Ops:
  0.6 1.5 load.1
  2.2 8.7 %all-gather = bf16[928,128]{1,0:T(8,128)(2,1)S(1)} all-gather(bf16[464,128]{1,0:T(8,128)(2,1)} %load.1), channel_id=2, replica_groups=mesh['z'=16,'c'=2,'tp'=16] {'c'}, dimensions={0}, use_global_device_ids=true | all-gather | bytes 356352 | tf_op jit(solution)/shard_map/all_gather | solution.py:490
  10.9 0.5 pack.1
  11.4 22.2 %all_to_all.35.got_ref = bf16[16,48,128]{2,1,0:T(8,128)(2,1)S(1)} all-to-all(bf16[16,48,128]{2,1,0:T(8,128)(2,1)S(1)} %get-tuple-element.42), channel_id=1, replica_groups=mesh['z'=16,'c'=2,'tp'=16] {'z'}, dimensions={0} | all-to-all | bytes 393216 | tf_op jit(solution)/shard_map/all_to_all | solution.py:460
  33.6 0.1 spread.1
  33.7 12.2 %all_to_all.36.got_ref = bf16[4,2,384,128]{3,2,1,0:T(8,128)(2,1)S(1)} all-to-all(bf16[4,2,384,128]{3,2,1,0:T(8,128)(2,1)S(1)} %spread.1), channel_id=1, replica_groups={{0,4,8,12},{1,5,9,13},{2,6,10,14},{3,7,11,15},{16,17,18,19},{20,21,22,2..., dimensions={0} | all-to-all | bytes 1572864 | tf_op jit(solution)/shard_map/all_to_all | solution.py:454
  45.9 0.4 copies.1
  46.3 0.0 copy-start
  46.3 0.0 copy-start.1
  46.3 0.0 copy-start.2
  46.3 25.4 %all_to_all.37 = bf16[4,4,2,384,128]{4,3,2,1,0:T(8,128)(2,1)S(1)} all-to-all(bf16[4,4,2,384,128]{4,3,2,1,0:T(8,128)(2,1)S(1)} %copies.1), channel_id=1, replica_groups={{0,1,2,3},{4,5,6,7},{8,9,10,11},{12,13,14,15},{16,20,24,28},{17,21,25,2..., dimensions={0} | all-to-all | bytes 6291456 | tf_op jit(solution)/shard_map/all_to_all | solution.py:454
  71.7 0.0 copy-done
  71.7 0.0 copy-done.1
  71.7 0.0 copy-done.2
  71.7 1.4 expert.1
  73.2 19.2 %all_to_all.38.part_ref = bf16[16,384,128]{2,1,0:T(8,128)(2,1)S(1)} all-to-all(bf16[16,384,128]{2,1,0:T(8,128)(2,1)S(1)} %get-tuple-element.43), channel_id=1, replica_groups=mesh['z'=16,'c'=2,'tp'=16] {'tp'}, dimensions={0} | all-to-all | bytes 3145728 | tf_op jit(solution)/shard_map/all_to_all | solution.py:460
  92.3 0.2 sums.1
  92.5 0.0 copy-start.3
  92.6 0.0 copy-start.4
  92.6 0.0 copy-start.5
  92.6 23.9 %all_to_all.39.own_ref = bf16[16,64,128]{2,1,0:T(8,128)(2,1)S(1)} all-to-all(bf16[16,64,128]{2,1,0:T(8,128)(2,1)S(1)} %sums.1), channel_id=1, replica_groups=mesh['z'=16,'c'=2,'tp'=16] {'z'}, dimensions={0} | all-to-all | bytes 524288 | tf_op jit(solution)/shard_map/all_to_all | solution.py:460
  116.5 10.5 %collective-permute-start = (bf16[16,64,128]{2,1,0:T(8,128)(2,1)S(1)}, bf16[16,64,128]{2,1,0:T(8,128)(2,1)S(1)}, u32[]{:S(2)}, u32[]{:S(2)}) collective-permute-start(bf16[16,64,128]{2,1,0:T(8,128)(2,1)S(1)} %all_to_all.39.own_ref), channel_id=1, source_target_pairs={{0,16},{16,0},{1,17},{17,1},{2,18},{18,2},{3,19},{19,3},{4,20},{20... | collective-permute-start | bytes 786440 | tf_op jit(solution)/shard_map/ppermute | solution.py:518
  127.1 1.9 %weights.1 = (bf16[2048,128]{1,0:T(8,128)(2,1)}, bf16[2048,128]{1,0:T(8,128)(2,1)}, bf16[128,2048]{1,0:T(8,128)(2,1)}) custom-call(bf16[16,2,384,128]{3,2,1,0:T(8,128)(2,1)S(1)} %bitcast.13, bf16[384,128]{1,0:T(8,128)(2,1)S(1)} %get-tuple-element.49.hid_ref, bf16[384,256]{1,0:T(8,128)(2,1)S(1)} %get-tuple-element.50.both_ref), custom_call_target="tpu_custom_call" | custom-call | flops 536870912 | bytes 1048576 | tf_op jit(solution)/shard_map/weights/pallas_call | solution.py:55
  128.9 0.0 collective-permute-done.other_ref
  129.0 0.3 resid.1
  129.2 13.9 %all_to_all.40.r_ref = bf16[16,128,128]{2,1,0:T(8,128)(2,1)S(1)} all-to-all(bf16[16,128,128]{2,1,0:T(8,128)(2,1)S(1)} %resid.1), channel_id=1, replica_groups=mesh['z'=16,'c'=2,'tp'=16] {'tp'}, dimensions={0} | all-to-all | bytes 1048576 | tf_op jit(solution)/shard_map/all_to_all | solution.py:460
  143.2 0.0 copy-done.3
  143.2 0.0 copy-done.4
  143.2 0.0 copy-done.5
  143.2 0.6 proj.1
  143.8 3.1 %collective-permute-start.1 = (bf16[18,64,128]{2,1,0:T(8,128)(2,1)S(1)}, bf16[18,64,128]{2,1,0:T(8,128)(2,1)S(1)}, u32[]{:S(2)}, u32[]{:S(2)}) collective-permute-start(bf16[18,64,128]{2,1,0:T(8,128)(2,1)S(1)} %get-tuple-element.60), channel_id=1, source_target_pairs={{0,16},{16,0},{1,17},{17,1},{2,18},{18,2},{3,19},{19,3},{4,20},{20... | collective-permute-start | bytes 884744 | tf_op jit(solution)/shard_map/ppermute | solution.py:545
  146.9 1.3 intra.1
  148.2 0.0 collective-permute-done.1.got_ref
  148.2 0.1 chip.1
  148.3 21.2 %all_to_all.41.got_ref = bf16[16,96,128]{2,1,0:T(8,128)(2,1)S(1)} all-to-all(bf16[16,96,128]{2,1,0:T(8,128)(2,1)S(1)} %get-tuple-element.67), channel_id=1, replica_groups=mesh['z'=16,'c'=2,'tp'=16] {'z'}, dimensions={0} | all-to-all | bytes 786432 | tf_op jit(solution)/shard_map/all_to_all | solution.py:460
  169.5 0.1 gather.1
  169.6 9.2 %all-gather.1 = f32[4,32,128]{2,1,0:T(8,128)S(1)} all-gather(f32[2,32,128]{2,1,0:T(8,128)S(1)} %gather.1), channel_id=3, replica_groups=mesh['z'=16,'c'=2,'tp'=16] {'c'}, dimensions={0}, use_global_device_ids=true | all-gather | bytes 98304 | tf_op jit(solution)/shard_map/all_gather | solution.py:561
  178.7 0.9 final.1
Async XLA Ops:
  46.3 25.4 %copy-start = (bf16[1,2048,128]{2,1,0:T(8,128)(2,1)S(1)}, bf16[1,2048,128]{2,1,0:T(8,128)(2,1)}, u32[]{:S(2)}) copy-start(bf16[1,2048,128]{2,1,0:T(8,128)(2,1)} %param.25) | copy-start | bytes 1572868
  46.3 25.4 %copy-start.1 = (bf16[1,2048,128]{2,1,0:T(8,128)(2,1)S(1)}, bf16[1,2048,128]{2,1,0:T(8,128)(2,1)}, u32[]{:S(2)}) copy-start(bf16[1,2048,128]{2,1,0:T(8,128)(2,1)} %param.26) | copy-start | bytes 1572868
  46.3 25.4 %copy-start.2 = (bf16[1,128,2048]{2,1,0:T(8,128)(2,1)S(1)}, bf16[1,128,2048]{2,1,0:T(8,128)(2,1)}, u32[]{:S(2)}) copy-start(bf16[1,128,2048]{2,1,0:T(8,128)(2,1)} %param.27) | copy-start | bytes 1572868
  92.5 50.6 %copy-start.3 = (bf16[2048,128]{1,0:T(8,128)(2,1)S(1)}, bf16[2048,128]{1,0:T(8,128)(2,1)}, u32[]{:S(2)}) copy-start(bf16[2048,128]{1,0:T(8,128)(2,1)} %p_ref.1) | copy-start | bytes 1572868
  92.6 50.6 %copy-start.4 = (bf16[64,128]{1,0:T(8,128)(2,1)S(1)}, bf16[64,128]{1,0:T(8,128)(2,1)}, u32[]{:S(2)}) copy-start(bf16[64,128]{1,0:T(8,128)(2,1)} %q_ref.3) | copy-start | bytes 49156
  92.6 50.6 %copy-start.5 = (bf16[128,128]{1,0:T(8,128)(2,1)S(1)}, bf16[128,128]{1,0:T(8,128)(2,1)}, u32[]{:S(2)}) copy-start(bf16[128,128]{1,0:T(8,128)(2,1)} %mixer_ref.1) | copy-start | bytes 98308
  116.5 12.4 %collective-permute-start = (bf16[16,64,128]{2,1,0:T(8,128)(2,1)S(1)}, bf16[16,64,128]{2,1,0:T(8,128)(2,1)S(1)}, u32[]{:S(2)}, u32[]{:S(2)}) collective-permute-start(bf16[16,64,128]{2,1,0:T(8,128)(2,1)S(1)} %all_to_all.39.own_ref), channel_id=1, source_target_pairs={{0,16},{16,0},{1,17},{17,1},{2,18},{18,2},{3,19},{19,3},{4,20},{20... | collective-permute-start | bytes 786440 | tf_op jit(solution)/shard_map/ppermute | solution.py:518
  143.8 4.4 %collective-permute-start.1 = (bf16[18,64,128]{2,1,0:T(8,128)(2,1)S(1)}, bf16[18,64,128]{2,1,0:T(8,128)(2,1)S(1)}, u32[]{:S(2)}, u32[]{:S(2)}) collective-permute-start(bf16[18,64,128]{2,1,0:T(8,128)(2,1)S(1)} %get-tuple-element.60), channel_id=1, source_target_pairs={{0,16},{16,0},{1,17},{17,1},{2,18},{18,2},{3,19},{19,3},{4,20},{20... | collective-permute-start | bytes 884744 | tf_op jit(solution)/shard_map/ppermute | solution.py:545
